TPU v7x, 512 devices: a whole 4x4x16 slice. The times are simulated.
512 devices in a mesh: sp: 16 (over z), tp: 32 (over y, x, core).
Axes of the slice: x: 4, y: 4, z: 16, core: 2. Of those that a mesh axis runs over, the one named last changes fastest.
Arguments:
- latent: bfloat16 [8192, 4096], P(('sp', 'tp')), may hold values from -6 to 6
- context: bfloat16 [512, 4096], P('sp'), may hold values from -6 to 6
- condition: float32 [4096], P('sp'), may hold values from -6 to 6
- context_cond: float32 [4096], P('sp'), may hold values from -6 to 6
- mod_weight: bfloat16 [4096, 12288], P('sp', 'tp'), may hold values from -0.09375 to 0.09375
- norm_gain: float32 [4096], replicated, may hold values from 0.1 to 1.9
- query_weight: bfloat16 [4096, 4096], P(None, 'tp'), may hold values from -0.09375 to 0.09375
- key_weight: bfloat16 [4096, 2048], P(None, 'tp'), may hold values from -0.09375 to 0.09375
- value_weight: bfloat16 [4096, 2048], P(None, 'tp'), may hold values from -0.09375 to 0.09375
- out_weight: bfloat16 [4096, 4096], P(None, 'tp'), may hold values from -0.375 to 0.375
- query_gain: float32 [64], replicated, may hold values from 1.2 to 6
- key_gain: float32 [64], replicated, may hold values from 1.2 to 6
- context_lift: float32 [64], P('tp'), may hold values from 0.5 to 2
Outputs:
- updated: bfloat16 [8192, 4096], P(('sp', 'tp'))
All inputs are finite; a program needn't handle non-finite values.
Results may differ from a plain program's by a relative error of at most 0.0085.
The roundings to bfloat16 on the way count: a program that leaves them out, or rounds other values in their place, can miss the bound.
Values may be sent and summed in bfloat16 or wider, within the bound.
No kernel may reach another device: no remote copies, remote signals or barrier semaphores. Data moves between devices by JAX's collectives and lax.ppermute only.
A program may use at most 64 MiB of HBM per device.

v0:
```python
import jax
import jax.numpy as jnp
from jax import lax
from jax.sharding import PartitionSpec as P

GRID_W = 64


EPS = 1e-06


def copy_for_each(shard, axis):
    copies = jnp.broadcast_to(shard, (lax.axis_size(axis), *shard.shape))
    return lax.all_to_all(copies, axis, split_axis=0, concat_axis=0, tiled=True)


def taken_together(shard, axis):
    everything = copy_for_each(shard, axis)
    return jnp.sum(everything, axis=0)


def laid_out(pieces, dim):
    pieces = jnp.moveaxis(pieces, 0, dim)
    lengths = pieces.shape
    return pieces.reshape(*lengths[:dim], lengths[dim] * lengths[dim + 1], *lengths[dim + 2 :])


def collect(shard, axis, dim):
    pieces = copy_for_each(shard, axis)
    return laid_out(pieces, dim)


def sent_together(arrays, axis, dim, along):
    widths = [a.shape[along] for a in arrays]
    both = jnp.concatenate(arrays, axis=along)
    out = lax.all_gather(both, axis, axis=dim, tiled=True)
    return tuple(jnp.split(out, [sum(widths[:k]) for k in range(1, len(widths))], axis=along))


def modulate(row_block, gain_vec, mod_row, model_width):
    row_values = row_block.astype(jnp.float32)
    normal = row_values * lax.rsqrt(jnp.mean(row_values * row_values, axis=-1, keepdims=True) + EPS)
    shift_part = mod_row[:model_width]
    scale_part = mod_row[model_width : 2 * model_width]
    return (normal * gain_vec * (1.0 + scale_part) + shift_part).astype(jnp.bfloat16)


def head_norm(values, gain_vec):
    return values * lax.rsqrt(jnp.mean(values * values, axis=-1, keepdims=True) + EPS) * gain_vec


def rope_tables(positions, head_size):
    freq_count = head_size // 4
    inverse = 10000.0 ** (-jnp.arange(freq_count, dtype=jnp.float32) / freq_count)
    grid_row = (positions // GRID_W).astype(jnp.float32)
    grid_col = (positions % GRID_W).astype(jnp.float32)
    angles = jnp.concatenate([grid_row[:, None] * inverse, grid_col[:, None] * inverse], axis=-1)
    return (jnp.cos(angles), jnp.sin(angles))


def rotate(values, cos_table, sin_table):
    paired = values.reshape(values.shape[:-1] + (values.shape[-1] // 2, 2))
    even_part = paired[..., 0]
    odd_part = paired[..., 1]
    cos_wide = cos_table[:, None, :]
    sin_wide = sin_table[:, None, :]
    turned = jnp.stack(
        [even_part * cos_wide - odd_part * sin_wide, even_part * sin_wide + odd_part * cos_wide],
        axis=-1,
    )
    return turned.reshape(values.shape)


def local(
    latent,
    context,
    condition,
    context_cond,
    mod_weight,
    norm_gain,
    query_weight,
    key_weight,
    value_weight,
    out_weight,
    query_gain,
    key_gain,
    context_lift,
):
    model_width = latent.shape[1]
    head_size = query_gain.shape[0]
    query_count = query_weight.shape[1] // head_size
    kv_count = key_weight.shape[1] // head_size
    group_size = query_count // kv_count
    score_scale = head_size ** (-0.5)
    cond_pair = jax.nn.silu(jnp.stack([condition, context_cond])).astype(jnp.bfloat16)
    partial_mod = jnp.dot(cond_pair, mod_weight, preferred_element_type=jnp.float32)
    summed_mod = taken_together(partial_mod, "sp")
    modulation = collect(summed_mod, "tp", 1)
    normed = modulate(latent, norm_gain, modulation[0], model_width)
    block_first = lax.axis_index("sp") * (latent.shape[0] * lax.axis_size("tp"))
    gathered = lax.all_gather(normed, "tp", axis=0, tiled=True)
    row_count = gathered.shape[0]
    query_raw = jnp.dot(gathered, query_weight, preferred_element_type=jnp.float32)
    key_raw = jnp.dot(gathered, key_weight, preferred_element_type=jnp.float32)
    value_raw = jnp.dot(gathered, value_weight, preferred_element_type=jnp.float32)
    positions = block_first + jnp.arange(row_count, dtype=jnp.int32)
    cos_table, sin_table = rope_tables(positions, head_size)
    query_rot = rotate(
        head_norm(query_raw.reshape(row_count, query_count, head_size), query_gain),
        cos_table,
        sin_table,
    )
    key_rot = rotate(
        head_norm(key_raw.reshape(row_count, kv_count, head_size), key_gain), cos_table, sin_table
    )
    joined = jnp.concatenate(
        [
            query_rot.reshape(row_count, -1).astype(jnp.bfloat16),
            key_rot.reshape(row_count, -1).astype(jnp.bfloat16),
            value_raw.astype(jnp.bfloat16),
        ],
        axis=1,
    )
    query_cols = query_count * head_size
    kv_cols = kv_count * head_size
    queries = joined[:, :query_cols]
    keys_here = joined[:, query_cols : query_cols + kv_cols]
    values_here = joined[:, query_cols + kv_cols :]
    normed_ctx = modulate(context, norm_gain, modulation[1], model_width)
    key_raw = jnp.dot(normed_ctx, key_weight, preferred_element_type=jnp.float32)
    ctx_key = head_norm(key_raw.reshape(context.shape[0], kv_count, head_size), key_gain)
    ctx_value = jnp.dot(normed_ctx, value_weight, preferred_element_type=jnp.float32)
    own_keys = ctx_key.reshape(context.shape[0], -1).astype(jnp.bfloat16)
    own_values = ctx_value.astype(jnp.bfloat16)
    ctx_keys, ctx_values = sent_together((own_keys, own_values), "sp", 0, 1)
    query_rows = queries.shape[0]
    grouped = queries.reshape(query_rows, kv_count, group_size, head_size)
    lift_rows = context_lift.reshape(kv_count, group_size)
    zero_lift = jnp.zeros_like(lift_rows)

    def absorb(carry_state, key_block, value_block, offset):
        running_max, denom, numer = carry_state
        key_heads = key_block.reshape(-1, kv_count, head_size)
        value_heads = value_block.reshape(-1, kv_count, head_size)
        scores = jnp.einsum(
            "qhgd,khd->hgqk", grouped, key_heads, preferred_element_type=jnp.float32
        )
        scores = scores * score_scale + offset[:, :, None, None]
        new_max = jnp.maximum(running_max, jnp.max(scores, axis=-1))
        expo = jnp.exp(scores - new_max[..., None])
        rescale = jnp.exp(running_max - new_max)
        denom = denom * rescale + jnp.sum(expo, axis=-1)
        numer = numer * rescale[..., None] + jnp.einsum(
            "hgqk,khd->hgqd",
            expo.astype(jnp.bfloat16),
            value_heads,
            preferred_element_type=jnp.float32,
        )
        return (new_max, denom, numer)

    def sweep(carry_state, key_rows, value_rows, offset):
        row_count = key_rows.shape[0]
        block_size = 512
        if block_size == row_count:
            return absorb(carry_state, key_rows, value_rows, offset)
        key_blocks = key_rows.reshape(row_count // block_size, block_size, -1)
        value_blocks = value_rows.reshape(row_count // block_size, block_size, -1)

        def absorb_block(state_now, key_value):
            return (absorb(state_now, key_value[0], key_value[1], offset), None)

        final_state, unused = lax.scan(absorb_block, carry_state, (key_blocks, value_blocks))
        return final_state

    initial = (
        jnp.full((kv_count, group_size, query_rows), -jnp.inf, jnp.float32),
        jnp.zeros((kv_count, group_size, query_rows), jnp.float32),
        jnp.zeros((kv_count, group_size, query_rows, head_size), jnp.float32),
    )
    after_context = sweep(initial, ctx_keys, ctx_values, lift_rows)
    gathered = sent_together((keys_here, values_here), "sp", 0, 1)
    running_max, denom, numer = sweep(after_context, gathered[0], gathered[1], zero_lift)
    attended = (numer / denom[..., None]).astype(jnp.bfloat16)
    attended = attended.transpose(2, 0, 1, 3).reshape(query_rows, query_cols)
    mixed_cols = jnp.dot(
        lax.all_gather(attended, "tp", axis=1, tiled=True),
        out_weight,
        preferred_element_type=jnp.float32,
    )
    mixed_rows = lax.all_to_all(
        mixed_cols.astype(jnp.bfloat16), "tp", split_axis=0, concat_axis=1, tiled=True
    )
    gate_lat = modulation[0, 2 * model_width :]
    return (latent.astype(jnp.float32) + gate_lat * mixed_rows.astype(jnp.float32)).astype(
        jnp.bfloat16
    )


def solution(mesh):
    return jax.shard_map(
        local,
        mesh=mesh,
        in_specs=(
            P(("sp", "tp"), None),
            P("sp", None),
            P("sp"),
            P("sp"),
            P("sp", "tp"),
            P(),
            P(None, "tp"),
            P(None, "tp"),
            P(None, "tp"),
            P(None, "tp"),
            P(),
            P(),
            P("tp"),
        ),
        out_specs=P(("sp", "tp"), None),
        check_vma=False,
    )
```

profile of v0, /device:TPU:1, one launch (start us, length us, event | category | flops | bytes accessed | tf_op | source)
XLA Modules:
  0.0 295.1 jit_solution(6820324707556283022)
XLA Ops:
  6.5 1.2 fusion.51
  7.8 0.6 broadcast_in_dim.12
  8.4 15.7 %all-to-all-start = ((f32[16,2,384]{2,1,0:T(2,128)}), f32[16,2,384]{2,1,0:T(2,128)S(1)}, u32[]{:S(2)}, u32[]{:S(2)}) async-start(f32[16,2,384]{2,1,0:T(2,128)} %broadcast_in_dim.12), calls=%async_computation | async-start | bytes 98304 | tf_op jit(solution)/shard_map/all_to_all | solution.py:14
  24.2 1.1 fusion.32
  25.2 10.5 %all-to-all-done = f32[16,2,384]{2,1,0:T(2,128)S(1)} async-done(((f32[16,2,384]{2,1,0:T(2,128)}), f32[16,2,384]{2,1,0:T(2,128)S(1)}, u32[]{:S(2)}, u32[]{:S(2)}) %all-to-all-start) | async-done | bytes 49184 | tf_op jit(solution)/shard_map/all_to_all | solution.py:14
  35.7 0.7 broadcast_in_dim.13
  36.4 9.1 %all-to-all-start.1 = ((f32[32,2,384]{2,1,0:T(2,128)}), f32[32,2,384]{2,1,0:T(2,128)S(1)}, u32[]{:S(2)}, u32[]{:S(2)}) async-start(f32[32,2,384]{2,1,0:T(2,128)} %broadcast_in_dim.13), calls=%async_computation.1 | async-start | bytes 196608 | tf_op jit(solution)/shard_map/all_to_all | solution.py:14
  45.6 7.3 %all-to-all-done.1 = f32[32,2,384]{2,1,0:T(2,128)S(1)} async-done(((f32[32,2,384]{2,1,0:T(2,128)}), f32[32,2,384]{2,1,0:T(2,128)S(1)}, u32[]{:S(2)}, u32[]{:S(2)}) %all-to-all-start.1) | async-done | bytes 98336 | tf_op jit(solution)/shard_map/all_to_all | solution.py:14
  53.0 1.7 fusion.36
  54.8 0.8 mul.307
  56.1 48.6 %all-gather.4.cloned.1.call-done = bf16[512,4096]{1,0:T(8,128)(2,1)} async-done(((bf16[16,4096]{1,0:T(8,128)(2,1)}), bf16[512,4096]{1,0:T(8,128)(2,1)}) %all-gather.4.cloned.1.call-update) | async-done | bytes 4194320 | tf_op jit(solution)/shard_map/all_gather | solution.py:101
  104.7 3.6 %multiply_reduce_fusion = (f32[512]{0:T(512)S(1)}, f32[512,64]{0,1:T(8,128)S(1)}) fusion(bf16[512,4096]{1,0:T(8,128)(2,1)} %all-gather.4.cloned.1.call-done, bf16[4096,64]{0,1:T(8,128)(2,1)S(1)} %copy-done.2), kind=kOutput, calls=%fused_computation.67 | convolution fusion | flops 268500480 | bytes 4851712 | tf_op jit(solution)/shard_map/dot_general | solution.py:104
  109.0 3.6 %convolution_convert_fusion.1 = bf16[512,64]{0,1:T(8,128)(2,1)S(1)} fusion(bf16[512,4096]{1,0:T(8,128)(2,1)} %all-gather.4.cloned.1.call-done, bf16[4096,64]{0,1:T(8,128)(2,1)S(1)} %copy-done.3), kind=kOutput, calls=%fused_computation.32 | convolution fusion | flops 268468224 | bytes 4784128 | tf_op jit(solution)/shard_map/dot_general | solution.py:105
  112.6 0.7 pad_maximum_fusion
  114.3 24.3 %all_gather.12 = bf16[512,128]{1,0:T(8,128)(2,1)S(1)} all-gather(bf16[32,128]{1,0:T(8,128)(2,1)S(1)} %pad_maximum_fusion.4), channel_id=1, replica_groups=mesh['sp'=16,'tp'=32] {'sp'}, dimensions={0}, use_global_device_ids=true | all-gather | bytes 139264 | tf_op jit(solution)/shard_map/all_gather | solution.py:36
  138.6 3.7 %bitcast_reduce_fusion.2 = (f32[512,2]{0,1:T(2,128)S(1)}, f32[512,128]{0,1:T(8,128)S(1)}) fusion(bf16[512,4096]{1,0:T(8,128)(2,1)} %all-gather.4.cloned.1.call-done, bf16[4096,128]{1,0:T(8,128)(2,1)S(1)} %copy-done), kind=kOutput, calls=%fused_computation.58 | convolution fusion | flops 537000960 | bytes 5509120 | tf_op jit(solution)/shard_map/dot_general | solution.py:103
  144.0 0.5 fusion.20
  144.5 0.6 fusion.21
  145.1 30.8 %all-gather.6.cloned.1.call-done = bf16[8192,128]{0,1:T(8,128)(2,1)} async-done(((bf16[512,128]{0,1:T(8,128)(2,1)}), bf16[8192,128]{0,1:T(8,128)(2,1)}) %all-gather.6.cloned.1.call-update) | async-done | bytes 2097168 | tf_op jit(solution)/shard_map/all_gather | solution.py:36
  175.9 1.7 fusion.60
  177.8 23.2 %while.14 = (s32[]{:T(128)}, f32[1,2,512]{2,1,0:T(2,128)S(1)}, f32[1,2,512]{2,1,0:T(2,128)S(1)}, f32[1,2,512,64]{2,3,1,0:T(8,128)S(1)}, bf16[16,512,64]{1,2,0:T(...) while((s32[]{:T(128)}, f32[1,2,512]{2,1,0:T(2,128)S(1)}, ...), condition=%wide.region_11.12_spmd, body=%wide.region_8.11_spmd.sunk | while | flops 138546176 | bytes 7143525 | solution.py:172
  177.8 0.5 bitcast_reduce_fusion.4
  178.7 0.5 fusion.84
  179.3 0.5 bitcast_reduce_fusion.4
  180.1 0.5 fusion.84
  180.7 0.5 bitcast_reduce_fusion.4
  181.6 0.5 fusion.84
  182.2 0.5 bitcast_reduce_fusion.4
  183.0 0.5 fusion.84
  184.5 0.5 fusion.84
  185.9 0.5 fusion.84
  187.4 0.5 fusion.84
  188.8 0.5 fusion.84
  190.3 0.5 fusion.84
  191.7 0.5 fusion.84
  193.2 0.5 fusion.84
  194.6 0.5 fusion.84
  196.0 0.5 fusion.84
  197.5 0.5 fusion.84
  198.9 0.5 fusion.84
  200.4 0.5 fusion.84
  201.0 0.7 divide_convert_fusion
  201.7 68.8 %all-gather.8.cloned.1.call-done = bf16[512,4096]{0,1:T(8,128)(2,1)} async-done(((bf16[512,128]{0,1:T(8,128)(2,1)}), bf16[512,4096]{0,1:T(8,128)(2,1)}) %all-gather.8.cloned.1.call-update) | async-done | bytes 4194320 | tf_op jit(solution)/shard_map/all_gather | solution.py:186
  270.5 4.4 %convolution_convert_fusion = bf16[512,128]{1,0:T(8,128)(2,1)} fusion(bf16[512,4096]{0,1:T(8,128)(2,1)} %all-gather.8.cloned.1.call-done, bf16[4096,128]{1,0:T(8,128)(2,1)} %param.24), kind=kOutput, calls=%fused_computation.31 | convolution fusion | flops 536936448 | bytes 5373952 | tf_op jit(solution)/shard_map/dot_general | solution.py:185
  274.9 5.3 %all-to-all-start.2 = ((bf16[32,16,128]{2,1,0:T(8,128)(2,1)}), bf16[32,16,128]{2,1,0:T(8,128)(2,1)S(1)}, u32[]{:S(2)}, u32[]{:S(2)}) async-start(bf16[32,16,128]{2,1,0:T(8,128)(2,1)} %bitcast.35), calls=%async_computation.2 | async-start | bytes 262144 | tf_op jit(solution)/shard_map/all_to_all | solution.py:190
  280.2 0.8 slice.46
  281.0 6.8 %all-to-all-done.2 = bf16[32,16,128]{2,1,0:T(8,128)(2,1)S(1)} async-done(((bf16[32,16,128]{2,1,0:T(8,128)(2,1)}), bf16[32,16,128]{2,1,0:T(8,128)(2,1)S(1)}, u32[]{:S(2)}, u32[]{:S(2)}) %all-to-all-start.2) | async-done | bytes 131104 | tf_op jit(solution)/shard_map/all_to_all | solution.py:190
  287.9 0.7 fusion.37
  (136 shorter events, 16.2 us)
Async XLA Ops:
  6.5 132.1 %copy-start = (bf16[4096,128]{1,0:T(8,128)(2,1)S(1)}, bf16[4096,128]{1,0:T(8,128)(2,1)}, u32[]{:S(2)}) copy-start(bf16[4096,128]{1,0:T(8,128)(2,1)} %param.21) | copy-start | bytes 3145732
  6.5 49.4 %copy-start.5 = (bf16[32,4096]{1,0:T(8,128)(2,1)S(1)}, bf16[32,4096]{1,0:T(8,128)(2,1)}, u32[]{:S(2)}) copy-start(bf16[32,4096]{1,0:T(8,128)(2,1)} %param.16) | copy-start | bytes 786436
  6.5 98.1 %copy-start.2 = (bf16[4096,64]{0,1:T(8,128)(2,1)S(1)}, bf16[4096,64]{0,1:T(8,128)(2,1)}, u32[]{:S(2)}) copy-start(bf16[4096,64]{0,1:T(8,128)(2,1)} %param.22) | copy-start | bytes 1572868
  8.4 27.3 %all-to-all-start = ((f32[16,2,384]{2,1,0:T(2,128)}), f32[16,2,384]{2,1,0:T(2,128)S(1)}, u32[]{:S(2)}, u32[]{:S(2)}) async-start(f32[16,2,384]{2,1,0:T(2,128)} %broadcast_in_dim.12), calls=%async_computation | async-start | bytes 98304 | tf_op jit(solution)/shard_map/all_to_all | solution.py:14
  36.4 16.5 %all-to-all-start.1 = ((f32[32,2,384]{2,1,0:T(2,128)}), f32[32,2,384]{2,1,0:T(2,128)S(1)}, u32[]{:S(2)}, u32[]{:S(2)}) async-start(f32[32,2,384]{2,1,0:T(2,128)} %broadcast_in_dim.13), calls=%async_computation.1 | async-start | bytes 196608 | tf_op jit(solution)/shard_map/all_to_all | solution.py:14
  45.6 59.1 %all-gather.4.cloned.1.call-start = ((), (), s32[]{:S(2)}) async-start(), calls=%async_computation.3 | async-start | bytes 4325376 | tf_op jit(solution)/shard_map/all_gather | solution.py:101
  52.9 3.0 %copy-start.4 = (f32[32,2,384]{2,1,0:T(2,128)}, f32[32,2,384]{2,1,0:T(2,128)S(1)}, u32[]{:S(2)}) copy-start(f32[32,2,384]{2,1,0:T(2,128)S(1)} %all-to-all-done.1) | copy-start | bytes 294916
  54.7 121.1 %all-gather.6.cloned.1.call-start = ((), (), s32[]{:S(2)}) async-start(), calls=%async_computation.4 | async-start | bytes 2228224 | tf_op jit(solution)/shard_map/all_gather | solution.py:36
  56.1 52.2 %copy-start.7 = (f32[64]{0:T(128)S(1)}, f32[64]{0:T(128)}, u32[]{:S(2)}) copy-start(f32[64]{0:T(128)} %param.26) | copy-start | bytes 772
  56.1 52.9 %copy-start.3 = (bf16[4096,64]{0,1:T(8,128)(2,1)S(1)}, bf16[4096,64]{0,1:T(8,128)(2,1)}, u32[]{:S(2)}) copy-start(bf16[4096,64]{0,1:T(8,128)(2,1)} %param.23) | copy-start | bytes 1572868
  109.0 4.4 %copy-start.6 = (f32[4096]{0:T(1024)S(1)}, f32[4096]{0:T(1024)}, u32[]{:S(2)}) copy-start(f32[4096]{0:T(1024)} %param.20) | copy-start | bytes 49156
  113.3 157.2 %all-gather.8.cloned.1.call-start = ((), (), s32[]{:S(2)}) async-start(), calls=%async_computation.5 | async-start | bytes 4325376 | tf_op jit(solution)/shard_map/all_gather | solution.py:186
  142.3 1.2 copy-start.8
  201.7 86.2 %copy-start.1 = (bf16[16,4096]{1,0:T(8,128)(2,1)S(1)}, bf16[16,4096]{1,0:T(8,128)(2,1)}, u32[]{:S(2)}) copy-start(bf16[16,4096]{1,0:T(8,128)(2,1)} %param.15) | copy-start | bytes 393220
  274.9 12.9 %all-to-all-start.2 = ((bf16[32,16,128]{2,1,0:T(8,128)(2,1)}), bf16[32,16,128]{2,1,0:T(8,128)(2,1)S(1)}, u32[]{:S(2)}, u32[]{:S(2)}) async-start(bf16[32,16,128]{2,1,0:T(8,128)(2,1)} %bitcast.35), calls=%async_computation.2 | async-start | bytes 262144 | tf_op jit(solution)/shard_map/all_to_all | solution.py:190
Sparse Core Ops, SparseCore 0:
  54.9 49.7 all-gather.3
  113.4 62.4 all-gather.5
  201.8 68.6 all-gather.7
where the time goes:
time: 296 us; the launch traced here: 295 us
  waiting for transfers between devices  173 us (58%)
  matrix products  34.5 us (12%)
  starting transfers between devices  30.3 us (10%)
  blocking collectives  24.3 us (8%)
  other arithmetic  13.5 us (5%)
  between operations  13.5 us (5%)
  local copies, waits for them, and re-layouts  5.43 us (2%)
    all_gather x1, waiting for transfers between devices, local(): lax.all_gather(attended, 'tp', axis=1, tiled=True)  68.8 us
    all_gather x1, waiting for transfers between devices, local(): gathered = lax.all_gather(normed, 'tp', axis=0, tiled=True)  48.6 us
    all_gather x1, waiting for transfers between devices, sent_together(): out = lax.all_gather(both, axis, axis=dim, tiled=True)  30.8 us
    all_to_all x2, starting transfers between devices, copy_for_each(): return lax.all_to_all(copies, axis, split_axis=0, concat_axis=0, tiled=True)  24.9 us
    all_gather x1, blocking collectives, sent_together(): out = lax.all_gather(both, axis, axis=dim, tiled=True)  24.3 us
    all_to_all x2, waiting for transfers between devices, copy_for_each(): return lax.all_to_all(copies, axis, split_axis=0, concat_axis=0, tiled=True)  17.8 us
    dot_general x17, matrix products, absorb(): jnp.einsum('hgqk,khd->hgqd', expo.astype(jnp.bfloat16), value_heads, pref...  9.15 us
    dot_general x17, matrix products, absorb(): jnp.einsum('qhgd,khd->hgqk', grouped, key_heads, preferred_element_type=j...  8.01 us
  transfers between devices with their start and end apart: 6, of which 6 were waited for; matrix products, arithmetic and copies ran while one was open for 4% of the time, Pallas kernels for 0%

commit v1 on v0

v1 whole, which is shorter than its diff:
```python
import functools
import math
import jax
import jax.numpy as jnp
from jax import lax
from jax.experimental import pallas as pl
from jax.experimental.pallas import tpu as pltpu
from jax.sharding import PartitionSpec as P

GRID_W = 64
EPS = 1e-06
LOG2E = math.log2(math.e)
NY = 4
NX = 4
NXC = 8


def copy_for_each(shard, axis):
    copies = jnp.broadcast_to(shard, (lax.axis_size(axis), *shard.shape))
    return lax.all_to_all(copies, axis, split_axis=0, concat_axis=0, tiled=True)


def modulated(x, gain, shift):
    x = x.astype(jnp.float32)
    ms = jnp.mean(x * x, axis=-1, keepdims=True)
    return (x * lax.rsqrt(ms + EPS) * gain + shift).astype(jnp.bfloat16)


def qkv_body(hs, lat_ref, ctx_ref, gain_ref, shift_ref, w_ref, w2_ref, qg_ref, kg_ref, cos_ref, sin_ref, own_ref, other_ref, ctx_kv_ref):
    def unit(v):
        return v * lax.rsqrt(jnp.mean(v * v, axis=-1, keepdims=True) + EPS)

    def turn(v, cos, sin):
        lane = lax.broadcasted_iota(jnp.int32, v.shape, 1)
        left = pltpu.roll(v, v.shape[1] - 1, 1)
        right = pltpu.roll(v, 1, 1)
        return v * cos + jnp.where(lane % 2 == 0, left, right) * sin

    x = modulated(lat_ref[...], gain_ref[0:1], shift_ref[0:1])
    cos = cos_ref[...]
    sin = sin_ref[...]
    for w, o_ref in ((w_ref, own_ref), (w2_ref, other_ref)):
        y = jnp.dot(x, w[...], preferred_element_type=jnp.float32)
        q = jnp.concatenate([unit(y[:, :hs]), unit(y[:, hs : 2 * hs])], axis=1) * qg_ref[...]
        q = turn(q, cos, sin).astype(jnp.bfloat16)
        o_ref[:, : 2 * hs] = q * jnp.bfloat16(hs ** -0.5)
        kv = y[:, 2 * hs :]
        k = unit(kv[:, :hs]) * kg_ref[...]
        k2 = turn(jnp.concatenate([k, k], axis=1), cos, sin)
        lane = lax.broadcasted_iota(jnp.int32, k2.shape, 1)
        o_ref[:, 2 * hs :] = jnp.where(lane < hs, k2, kv).astype(jnp.bfloat16)

    @pl.when(pl.program_id(0) == 0)
    def _():
        c = modulated(ctx_ref[...], gain_ref[1:2], shift_ref[1:2])
        ckv = jnp.dot(c, w_ref[:, 2 * hs :], preferred_element_type=jnp.float32)
        ck = unit(ckv[:, :hs]) * kg_ref[...]
        ctx_kv_ref[...] = jnp.concatenate([ck, ckv[:, hs:]], axis=1).astype(jnp.bfloat16)


def qkv(lat, context, gain, shift, w, w2, qg, kg, cos, sin):
    rows, width = lat.shape
    n_ctx = context.shape[0]
    hs = kg.shape[1]
    step = rows // 2
    whole = lambda a: pl.BlockSpec(a.shape, lambda i: (0,) * a.ndim)
    return pl.pallas_call(
        functools.partial(qkv_body, hs),
        grid=(rows // step,),
        in_specs=[
            pl.BlockSpec((step, width), lambda i: (i, 0)),
            whole(context), whole(gain), whole(shift), whole(w), whole(w2), whole(qg), whole(kg),
            pl.BlockSpec((step, 2 * hs), lambda i: (i, 0)),
            pl.BlockSpec((step, 2 * hs), lambda i: (i, 0)),
        ],
        out_specs=[
            pl.BlockSpec((step, 4 * hs), lambda i: (i, 0)),
            pl.BlockSpec((step, 4 * hs), lambda i: (i, 0)),
            pl.BlockSpec((n_ctx, 2 * hs), lambda i: (0, 0)),
        ],
        out_shape=[
            jax.ShapeDtypeStruct((rows, 4 * hs), jnp.bfloat16),
            jax.ShapeDtypeStruct((rows, 4 * hs), jnp.bfloat16),
            jax.ShapeDtypeStruct((n_ctx, 2 * hs), jnp.bfloat16),
        ],
        cost_estimate=pl.CostEstimate(flops=4 * rows * width * 4 * hs, bytes_accessed=6 << 20, transcendentals=0),
        name="qkv",
    )(lat, context, gain, shift, w, w2, qg, kg, cos, sin)


def assemble_body(core_ref, own_ref, got_ref, ctx_ref, qt_ref, kv_ref):
    rows = own_ref.shape[0]
    hs = qt_ref.shape[1]

    def put(ref, start):
        t = ref[:, : 2 * hs].astype(jnp.float32).T.astype(jnp.bfloat16)
        qt_ref[0, :, start : start + rows] = t[:hs]
        qt_ref[1, :, start : start + rows] = t[hs:]

    @pl.when(core_ref[0] == 0)
    def _():
        put(own_ref, 0)
        put(got_ref, rows)

    @pl.when(core_ref[0] != 0)
    def _():
        put(got_ref, 0)
        put(own_ref, rows)

    kv_ref[0:rows] = own_ref[:, 2 * hs :]
    kv_ref[rows : 2 * rows] = got_ref[:, 2 * hs :]
    kv_ref[2 * rows :] = ctx_ref[...]


VMEM = pl.BlockSpec(memory_space=pltpu.VMEM)


def assemble(core, own, got, ctx_kv):
    rows, cols = own.shape
    hs = cols // 4
    return pl.pallas_call(
        assemble_body,
        in_specs=[pl.BlockSpec(memory_space=pltpu.SMEM), VMEM, VMEM, VMEM],
        out_specs=[VMEM, VMEM],
        out_shape=[
            pltpu.VMEM((2, hs, 2 * rows), jnp.bfloat16),
            pltpu.VMEM((2 * rows + ctx_kv.shape[0], 2 * hs), jnp.bfloat16),
        ],
        name="assemble",
    )(core, own, got, ctx_kv)


def flash_body(n_blocks, first, last, lat_rows, hs, *refs):
    qt_ref, lift_ref = refs[:2]
    blocks = refs[2 : 2 + n_blocks]
    rest = refs[2 + n_blocks :]
    if not first:
        m_ref, l_ref, acc_ref = rest[:3]
        rest = rest[3:]
    heads, _, qn = qt_ref.shape
    lift = lift_ref[...]
    for h in range(heads):
        parts = []
        top = None
        for b in blocks:
            s = jnp.dot(b[:, :hs], qt_ref[h], preferred_element_type=jnp.float32) * LOG2E
            c = s[lat_rows:] + lift[h : h + 1] * LOG2E
            s = s[:lat_rows]
            t = jnp.maximum(jnp.max(s, axis=0, keepdims=True), jnp.max(c, axis=0, keepdims=True))
            top = t if top is None else jnp.maximum(top, t)
            parts.append((b, s, c))
        if first:
            l = jnp.zeros_like(top)
            acc = jnp.zeros((hs, qn), jnp.float32)
        else:
            m = m_ref[h : h + 1]
            top = jnp.maximum(top, m)
            alpha = jnp.exp2(m - top)
            l = l_ref[h : h + 1] * alpha
            acc = acc_ref[h] * alpha
        for b, s, c in parts:
            e = jnp.exp2(s - top)
            f = jnp.exp2(c - top)
            l = l + (jnp.sum(e, axis=0, keepdims=True) + jnp.sum(f, axis=0, keepdims=True))
            p = jnp.concatenate([e.astype(jnp.bfloat16), f.astype(jnp.bfloat16)], axis=0)
            acc = acc + lax.dot_general(
                b[:, hs:], p, (((0,), (0,)), ((), ())), preferred_element_type=jnp.float32
            )
        if last:
            o = (acc / l).T.astype(jnp.bfloat16)
            n = lat_rows // (2 * NY)
            for c2 in range(2):
                for y in range(NY):
                    j = (c2 * NY + y) * n
                    rest[0][y, c2 * n : (c2 + 1) * n, h * hs : (h + 1) * hs] = o[j : j + n]
        else:
            rest[0][h : h + 1] = top
            rest[1][h : h + 1] = l
            rest[2][h] = acc


def flash(qt, lift, blocks, state, lat_rows, last):
    heads, hs, qn = qt.shape
    first = state is None
    args = [qt, lift, *blocks] + ([] if first else list(state))
    args = [pltpu.with_memory_space_constraint(a, pltpu.VMEM) for a in args]
    if last:
        outs = [pltpu.VMEM((NY, qn // NY, heads * hs), jnp.bfloat16)]
    else:
        outs = [
            pltpu.VMEM((heads, qn), jnp.float32),
            pltpu.VMEM((heads, qn), jnp.float32),
            pltpu.VMEM((heads, hs, qn), jnp.float32),
        ]
    res = pl.pallas_call(
        functools.partial(flash_body, len(blocks), first, last, lat_rows, hs),
        in_specs=[VMEM] * len(args),
        out_specs=[VMEM] * len(outs),
        out_shape=outs,
        cost_estimate=pl.CostEstimate(
            flops=4 * heads * hs * qn * blocks[0].shape[0] * len(blocks), bytes_accessed=1 << 20, transcendentals=0
        ),
        name="flash",
    )(*args)
    return res[0] if last else res


def project_body(a_ref, w_ref, o_ref):
    ny = a_ref.shape[0]
    a = jnp.concatenate([a_ref[y] for y in range(ny)], axis=1)
    n = w_ref.shape[4]

    def column(j):
        return jnp.concatenate([w_ref[0, j, y] for y in range(ny)], axis=0)

    for j in range(0, w_ref.shape[1], 2):
        w = jnp.concatenate([column(j), column(j + 1)], axis=1)
        o_ref[:, j * n : (j + 2) * n] = jnp.dot(a, w, preferred_element_type=jnp.float32).astype(jnp.bfloat16)


def out_partial(a, w):
    ny, nxc, ny2, kk, n = w.shape
    rows = a.shape[1]
    return pl.pallas_call(
        project_body,
        grid=(ny,),
        in_specs=[
            pl.BlockSpec(a.shape, lambda i: (0, 0, 0)),
            pl.BlockSpec((1, nxc, ny2, kk, n), lambda i: (i, 0, 0, 0, 0)),
        ],
        out_specs=pl.BlockSpec((rows, nxc * n), lambda i: (0, i)),
        out_shape=jax.ShapeDtypeStruct((rows, ny * nxc * n), jnp.bfloat16),
        cost_estimate=pl.CostEstimate(flops=2 * rows * w.size, bytes_accessed=2 * w.size, transcendentals=0),
        name="out_partial",
    )(a, w)


def local(
    latent,
    context,
    condition,
    context_cond,
    mod_weight,
    norm_gain,
    query_weight,
    key_weight,
    value_weight,
    out_weight,
    query_gain,
    key_gain,
    context_lift,
):
    own_rows, width = latent.shape
    hs = query_gain.shape[0]
    n_sp = lax.axis_size("sp")
    n_tp = lax.axis_size("tp")
    group_y = [[y * NXC + c for y in range(NY)] for c in range(NXC)]
    group_cx = [[y * NXC + 2 * x + c for c in range(2) for x in range(NX)] for y in range(NY)]
    group_core = [[2 * i + c for i in range(n_tp // 2)] for c in range(2)]
    swap = [(t, t ^ 1) for t in range(n_tp)]
    tp = lax.axis_index("tp")
    core = tp % 2
    block_rows = own_rows * n_tp

    lat_copies = jnp.broadcast_to(latent, (n_tp // 2, own_rows, width))
    lat_half = lax.all_to_all(lat_copies, "tp", 0, 0, axis_index_groups=group_core, tiled=True)
    lat_half = lat_half.reshape(block_rows // 2, width)

    half = jnp.arange(block_rows // 2, dtype=jnp.int32)
    inside = (half // own_rows) * (2 * own_rows) + core * own_rows + half % own_rows
    positions = lax.axis_index("sp") * block_rows + inside
    freq_count = hs // 4
    inverse = 10000.0 ** (-jnp.arange(freq_count, dtype=jnp.float32) / freq_count)
    grid_row = (positions // GRID_W).astype(jnp.float32)
    grid_col = (positions % GRID_W).astype(jnp.float32)
    angles = jnp.concatenate([grid_row[:, None] * inverse, grid_col[:, None] * inverse], axis=-1)
    cos = jnp.tile(jnp.repeat(jnp.cos(angles), 2, axis=1), (1, 2))
    sign = jnp.tile(jnp.array([-1.0, 1.0], jnp.float32), hs)
    sin = jnp.tile(jnp.repeat(jnp.sin(angles), 2, axis=1), (1, 2)) * sign
    w_own = jnp.concatenate([query_weight, key_weight, value_weight], axis=1)
    w_other = lax.ppermute(w_own, "tp", swap)
    per_head = out_weight.shape[0] // n_tp
    w_split = out_weight.reshape(NY, NXC, per_head, out_weight.shape[1]).transpose(1, 0, 2, 3)
    w_split = jnp.broadcast_to(w_split, (NY, *w_split.shape)).reshape(n_tp, *w_split.shape[1:])
    lift = jnp.broadcast_to(context_lift[:, None], (context_lift.shape[0], block_rows))
    q_gain = jnp.tile(query_gain, 2)[None]
    k_gain = key_gain[None]

    cond_pair = jax.nn.silu(jnp.stack([condition, context_cond])).astype(jnp.bfloat16)
    partial_mod = jnp.dot(cond_pair, mod_weight, preferred_element_type=jnp.float32)
    summed_mod = lax.psum(partial_mod, "sp")
    summed_mod, lat_half, w_own, cos, sin, w_split, lift, q_gain, k_gain = lax.optimization_barrier(
        (summed_mod, lat_half, w_own, cos, sin, w_split, lift, q_gain, k_gain)
    )
    mod = copy_for_each(summed_mod, "tp")
    mod = jnp.moveaxis(mod, 0, 1).reshape(2, 3 * width)
    shift = mod[:, :width]
    gain = norm_gain * (1.0 + mod[:, width : 2 * width])

    own, other, ctx_kv = qkv(lat_half, context, gain, shift, w_own, w_other, q_gain, k_gain, cos, sin)
    got = lax.ppermute(other, "tp", swap)
    qt, kv = assemble(core.reshape(1).astype(jnp.int32), own, got, ctx_kv)
    kv, w_split = lax.optimization_barrier((kv, w_split))
    w_rows = lax.all_to_all(w_split, "tp", 0, 0, tiled=True)

    up = [(i, (i + 1) % n_sp) for i in range(n_sp)]
    down = [(d, s) for s, d in up]
    fwd = bwd = kv
    blocks = [kv]
    state = None
    for step in range(1, n_sp // 2 + 1):
        nxt_f = lax.ppermute(fwd, "sp", up)
        nxt_b = lax.ppermute(bwd, "sp", down) if step < n_sp // 2 else None
        state = flash(qt, lift, blocks, state, block_rows, False)
        if step == 5:
            nxt_f, nxt_b, state, w_rows = lax.optimization_barrier((nxt_f, nxt_b, state, w_rows))
        else:
            nxt_f, nxt_b, state = lax.optimization_barrier((nxt_f, nxt_b, state))
        fwd, bwd = nxt_f, nxt_b
        blocks = [fwd] if bwd is None else [fwd, bwd]
    attended = flash(qt, lift, blocks, state, block_rows, True)
    w_rows = w_rows.reshape(NY, NXC, *w_rows.shape[1:])

    heads_y = lax.all_to_all(attended, "tp", 0, 0, axis_index_groups=group_y, tiled=True)
    part = out_partial(heads_y, w_rows)
    part = part.reshape(NXC, own_rows, width)
    parts = lax.all_to_all(part, "tp", 0, 0, axis_index_groups=group_cx, tiled=True)
    mixed = jnp.sum(parts.astype(jnp.float32), axis=0).astype(jnp.bfloat16)
    gate = mod[0, 2 * width :]
    return (latent.astype(jnp.float32) + gate * mixed.astype(jnp.float32)).astype(jnp.bfloat16)


def solution(mesh):
    return jax.shard_map(
        local,
        mesh=mesh,
        in_specs=(
            P(("sp", "tp"), None),
            P("sp", None),
            P("sp"),
            P("sp"),
            P("sp", "tp"),
            P(),
            P(None, "tp"),
            P(None, "tp"),
            P(None, "tp"),
            P(None, "tp"),
            P(),
            P(),
            P("tp"),
        ),
        out_specs=P(("sp", "tp"), None),
        check_vma=False,
    )
```

time: 296 us -> 216 us (0.73)
  waiting for transfers between devices: 173 us -> 31.4 us
  starting transfers between devices: 30.3 us -> 94.7 us
  matrix products: 34.5 us -> 0.14 us
  Pallas kernels: 0 us -> 30.4 us
  between operations: 13.5 us -> 0.49 us
  blocking collectives: 24.3 us -> 36.9 us
  local copies, waits for them, and re-layouts: 5.43 us -> 14.7 us
  other arithmetic: 13.5 us -> 5.96 us
    all_gather x3 -> x0, waiting for transfers between devices: 148 us -> none  [the longest x1 68.8 us: local(): lax.all_gather(attended, 'tp', axis=1, tiled=True)]
    ppermute x0 -> x17, starting transfers between devices: none -> 57.6 us  [the longest x7 35 us: local(): nxt_b = lax.ppermute(bwd, 'sp', down) if step < n_sp // 2 else None]
    dot_general x40 -> x0, matrix products: 33.3 us -> none  [the longest x17 9.15 us: absorb(): jnp.einsum('hgqk,khd->hgqd', expo.astype(jnp.bfloat16), value_heads, pref...]
    pallas_call x0 -> x12, Pallas kernels: none -> 30.4 us  [the longest x9 17.6 us: flash(): pl.pallas_call(functools.partial(flash_body, len(blocks), first, last, la...]
    psum x0 -> x1, blocking collectives: none -> 28.1 us  [local(): summed_mod = lax.psum(partial_mod, 'sp')]
    all_gather x1 -> x0, blocking collectives: 24.3 us -> none  [sent_together(): out = lax.all_gather(both, axis, axis=dim, tiled=True)]
    all_to_all x1 -> x3, starting transfers between devices: 5.3 us -> 23.4 us  [the longest x1 11 us: local(): lax.all_to_all(part, 'tp', 0, 0, axis_index_groups=group_cx, tiled=True)]
    all_to_all x1 -> x3, waiting for transfers between devices: 6.83 us -> 19.3 us  [the longest x1 14.9 us: local(): lax.all_to_all(part, 'tp', 0, 0, axis_index_groups=group_cx, tiled=True)]
  transfers between devices with their start and end apart: 6 -> 21, of which waited for: 6 -> 7; matrix products, arithmetic and copies ran while one was open for 4% -> 8% of each run, Pallas kernels for 0% -> 8%
where the time goes in v1:
time: 216 us; the launch traced here: 215 us
  starting transfers between devices  94.7 us (44%)
  blocking collectives  36.9 us (17%)
  waiting for transfers between devices  31.4 us (15%)
  Pallas kernels  30.4 us (14%)
  local copies, waits for them, and re-layouts  14.7 us (7%)
  other arithmetic  5.96 us (3%)
    ppermute x7, starting transfers between devices, local(): nxt_b = lax.ppermute(bwd, 'sp', down) if step < n_sp // 2 else None  35 us
    psum x1, blocking collectives, local(): summed_mod = lax.psum(partial_mod, 'sp')  28.1 us
    pallas_call x9, Pallas kernels, flash(): pl.pallas_call(functools.partial(flash_body, len(blocks), first, last, la...  17.6 us
    ppermute x8, starting transfers between devices, local(): nxt_f = lax.ppermute(fwd, 'sp', up)  15.3 us
    all_to_all x1, waiting for transfers between devices, local(): lax.all_to_all(part, 'tp', 0, 0, axis_index_groups=group_cx, tiled=True)  14.9 us
    all_to_all x1, starting transfers between devices, copy_for_each(): return lax.all_to_all(copies, axis, split_axis=0, concat_axis=0, tiled=True)  13.6 us
    all_to_all x1, starting transfers between devices, local(): lax.all_to_all(part, 'tp', 0, 0, axis_index_groups=group_cx, tiled=True)  11 us
    all_to_all x1, blocking collectives, local(): lax.all_to_all(attended, 'tp', 0, 0, axis_index_groups=group_y, tiled=True)  8.8 us
  transfers between devices with their start and end apart: 21, of which 7 were waited for; matrix products, arithmetic and copies ran while one was open for 8% of the time, Pallas kernels for 8%

profile of v1, /device:TPU:1, one launch (start us, length us, event | category | flops | bytes accessed | tf_op | source)
XLA Modules:
  0.0 214.7 jit_solution(18212184605912051505)
XLA Ops:
  0.0 2.5 %broadcast_in_dim.14 = bf16[16,16,4096]{2,1,0:T(8,128)(2,1)} broadcast(bf16[16,4096]{1,0:T(8,128)(2,1)} %param.14), dimensions={1,2} | broadcast | bytes 2228224 | tf_op jit(solution)/shard_map/broadcast_in_dim | solution.py:265
  2.5 7.6 %all-to-all-start = ((bf16[16,16,4096]{2,1,0:T(8,128)(2,1)}), bf16[16,16,4096]{2,1,0:T(8,128)(2,1)S(1)}, u32[]{:S(2)}, u32[]{:S(2)}) async-start(bf16[16,16,4096]{2,1,0:T(8,128)(2,1)} %broadcast_in_dim.14), calls=%async_computation | async-start | bytes 4194304 | tf_op jit(solution)/shard_map/all_to_all | solution.py:266
  10.1 1.5 copy.23
  11.7 2.4 %copy.24 = bf16[4096,64]{1,0:T(8,128)(2,1)} copy(bf16[4096,64]{0,1:T(8,128)(2,1)} %param.22) | data formatting | bytes 1048576 | tf_op args[8]
  14.0 3.6 %pad_maximum_fusion.w_ref = bf16[4096,256]{1,0:T(8,128)(2,1)} fusion(bf16[4096,64]{1,0:T(8,128)(2,1)} %copy.24, bf16[4096,64]{1,0:T(8,128)(2,1)S(1)} %copy.23, bf16[4096,128]{1,0:T(8,128)(2,1)} %param.20), kind=kLoop, calls=%fused_computation | loop fusion | flops 6291456 | bytes 4194304 | tf_op jit(solution)/shard_map/concatenate | solution.py:280
  17.6 5.0 %collective-permute-start = (bf16[4096,256]{1,0:T(8,128)(2,1)}, bf16[4096,256]{1,0:T(8,128)(2,1)}, u32[]{:S(2)}, u32[]{:S(2)}) collective-permute-start(bf16[4096,256]{1,0:T(8,128)(2,1)} %pad_maximum_fusion.w_ref), channel_id=1, source_target_pairs={{0,1},{1,0},{2,3},{3,2},{4,5},{5,4},{6,7},{7,6},{8,9},{9,8},{10,11... | collective-permute-start | bytes 6291464 | tf_op jit(solution)/shard_map/ppermute | solution.py:281
  23.4 1.3 copy.26
  26.1 28.1 %psum.7 = f32[2,384]{1,0:T(2,128)S(1)} all-reduce(f32[2,384]{1,0:T(2,128)S(1)} %fusion.6), channel_id=1, replica_groups=mesh['sp'=16,'tp'=32] {'sp'}, use_global_device_ids=true, to_apply=%region_0.1 | all-reduce | flops 768 | bytes 6144 | tf_op jit(solution)/shard_map/psum | solution.py:291
  55.0 3.0 %broadcast_in_dim.32 = bf16[4,8,4,128,128]{4,3,2,1,0:T(8,128)(2,1)} broadcast(bf16[8,4,128,128]{3,2,1,0:T(8,128)(2,1)S(1)} %copy.26), dimensions={1,2,3,4} | broadcast | bytes 5242880 | tf_op jit(solution)/shard_map/broadcast_in_dim | solution.py:284
  58.7 13.6 %all-to-all-start.1 = ((f32[32,2,384]{2,1,0:T(2,128)}), f32[32,2,384]{2,1,0:T(2,128)S(1)}, u32[]{:S(2)}, u32[]{:S(2)}) async-start(f32[32,2,384]{2,1,0:T(2,128)} %broadcast_in_dim.35), calls=%async_computation.1 | async-start | bytes 196608 | tf_op jit(solution)/shard_map/all_to_all | solution.py:20
  72.4 0.8 copy.27.cos_ref
  73.1 6.6 %all-to-all-done.1 = f32[32,2,384]{2,1,0:T(2,128)S(1)} async-done(((f32[32,2,384]{2,1,0:T(2,128)}), f32[32,2,384]{2,1,0:T(2,128)S(1)}, u32[]{:S(2)}, u32[]{:S(2)}) %all-to-all-start.1) | async-done | bytes 98336 | tf_op jit(solution)/shard_map/all_to_all | solution.py:20
  80.4 7.1 %qkv.1 = (bf16[256,256]{1,0:T(8,128)(2,1)}, bf16[256,256]{1,0:T(8,128)(2,1)}, bf16[32,128]{1,0:T(8,128)(2,1)}) custom-call(bf16[256,4096]{1,0:T(8,128)(2,1)} %bitcast.23, bf16[32,4096]{1,0:T(8,128)(2,1)} %ctx_ref.1, f32[2,4096]{1,0:T(2,128)} %get-tuple-element.166.gain_ref, f32[2,4096]{1,0:T(2,128)} %get-tuple-element.165.shift_ref, ...), custom_call_target="tpu_custom_call" | custom-call | flops 1073741824 | bytes 6291456 | tf_op jit(solution)/shard_map/qkv/pallas_call | solution.py:67
  87.5 2.3 %collective-permute-start.1 = (bf16[256,256]{1,0:T(8,128)(2,1)}, bf16[256,256]{1,0:T(8,128)(2,1)S(1)}, u32[]{:S(2)}, u32[]{:S(2)}) collective-permute-start(bf16[256,256]{1,0:T(8,128)(2,1)} %get-tuple-element.93), channel_id=1, source_target_pairs={{0,1},{1,0},{2,3},{3,2},{4,5},{5,4},{6,7},{7,6},{8,9},{9,8},{10,11... | collective-permute-start | bytes 393224 | tf_op jit(solution)/shard_map/ppermute | solution.py:301
  89.8 1.2 collective-permute-done.1.got_ref
  91.6 1.1 assemble.1
  92.7 4.8 %all-to-all-start.2 = ((bf16[32,4,128,128]{3,2,1,0:T(8,128)(2,1)}), bf16[32,4,128,128]{3,2,1,0:T(8,128)(2,1)}, u32[]{:S(2)}, u32[]{:S(2)}) async-start(bf16[32,4,128,128]{3,2,1,0:T(8,128)(2,1)} %bitcast.22), calls=%async_computation.2 | async-start | bytes 8388608 | tf_op jit(solution)/shard_map/all_to_all | solution.py:304
  97.5 1.9 collective-permute-start.2
  99.5 4.6 %collective-permute-start.3 = (bf16[544,128]{1,0:T(8,128)(2,1)S(1)}, bf16[544,128]{1,0:T(8,128)(2,1)S(1)}, u32[]{:S(2)}, u32[]{:S(2)}) collective-permute-start(bf16[544,128]{1,0:T(8,128)(2,1)S(1)} %get-tuple-element.99.refs_2_), channel_id=1, source_target_pairs={{32,0},{64,32},{96,64},{128,96},{160,128},{192,160},{224,192},{256... | collective-permute-start | bytes 417800 | tf_op jit(solution)/shard_map/ppermute | solution.py:313
  104.0 1.2 flash.9
  105.6 0.8 collective-permute-done.3.refs_3_
  106.4 1.9 collective-permute-start.4
  108.3 5.4 %collective-permute-start.5 = (bf16[544,128]{1,0:T(8,128)(2,1)S(1)}, bf16[544,128]{1,0:T(8,128)(2,1)S(1)}, u32[]{:S(2)}, u32[]{:S(2)}) collective-permute-start(bf16[544,128]{1,0:T(8,128)(2,1)S(1)} %collective-permute-done.3.refs_3_), channel_id=1, source_target_pairs={{32,0},{64,32},{96,64},{128,96},{160,128},{192,160},{224,192},{256... | collective-permute-start | bytes 417800 | tf_op jit(solution)/shard_map/ppermute | solution.py:313
  113.7 2.2 %flash.10 = (f32[2,512]{1,0:T(2,128)S(1)}, f32[2,512]{1,0:T(2,128)S(1)}, f32[2,64,512]{2,1,0:T(8,128)S(1)}) custom-call(bf16[2,64,512]{2,1,0:T(8,128)(2,1)S(1)} %get-tuple-element.95.refs_0_, f32[2,512]{1,0:T(2,128)S(1)} %broadcast_in_dim.33.refs_1_, bf16[544,128]{1,0:T(8,128)(2,1)S(1)} %collective-permute-done.2.refs_2_, ...), custom_call_target="tpu_custom_call" | custom-call | flops 285212672 | bytes 1048576 | tf_op jit(solution)/shard_map/flash/pallas_call | solution.py:195
  115.9 1.9 collective-permute-start.6
  117.8 5.2 %collective-permute-start.7 = (bf16[544,128]{1,0:T(8,128)(2,1)S(1)}, bf16[544,128]{1,0:T(8,128)(2,1)S(1)}, u32[]{:S(2)}, u32[]{:S(2)}) collective-permute-start(bf16[544,128]{1,0:T(8,128)(2,1)S(1)} %collective-permute-done.5.refs_3_), channel_id=1, source_target_pairs={{32,0},{64,32},{96,64},{128,96},{160,128},{192,160},{224,192},{256... | collective-permute-start | bytes 417800 | tf_op jit(solution)/shard_map/ppermute | solution.py:313
  123.0 2.2 %flash.11 = (f32[2,512]{1,0:T(2,128)S(1)}, f32[2,512]{1,0:T(2,128)S(1)}, f32[2,64,512]{2,1,0:T(8,128)S(1)}) custom-call(bf16[2,64,512]{2,1,0:T(8,128)(2,1)S(1)} %get-tuple-element.95.refs_0_, f32[2,512]{1,0:T(2,128)S(1)} %broadcast_in_dim.33.refs_1_, bf16[544,128]{1,0:T(8,128)(2,1)S(1)} %collective-permute-done.4.refs_2_, ...), custom_call_target="tpu_custom_call" | custom-call | flops 285212672 | bytes 1048576 | tf_op jit(solution)/shard_map/flash/pallas_call | solution.py:195
  125.2 1.9 collective-permute-start.8
  127.1 5.4 %collective-permute-start.9 = (bf16[544,128]{1,0:T(8,128)(2,1)S(1)}, bf16[544,128]{1,0:T(8,128)(2,1)S(1)}, u32[]{:S(2)}, u32[]{:S(2)}) collective-permute-start(bf16[544,128]{1,0:T(8,128)(2,1)S(1)} %collective-permute-done.7.refs_3_), channel_id=1, source_target_pairs={{32,0},{64,32},{96,64},{128,96},{160,128},{192,160},{224,192},{256... | collective-permute-start | bytes 417800 | tf_op jit(solution)/shard_map/ppermute | solution.py:313
  132.5 2.2 %flash.12 = (f32[2,512]{1,0:T(2,128)S(1)}, f32[2,512]{1,0:T(2,128)S(1)}, f32[2,64,512]{2,1,0:T(8,128)S(1)}) custom-call(bf16[2,64,512]{2,1,0:T(8,128)(2,1)S(1)} %get-tuple-element.95.refs_0_, f32[2,512]{1,0:T(2,128)S(1)} %broadcast_in_dim.33.refs_1_, bf16[544,128]{1,0:T(8,128)(2,1)S(1)} %collective-permute-done.6.refs_2_, ...), custom_call_target="tpu_custom_call" | custom-call | flops 285212672 | bytes 1048576 | tf_op jit(solution)/shard_map/flash/pallas_call | solution.py:195
  134.7 1.9 collective-permute-start.10
  136.7 5.0 %collective-permute-start.11 = (bf16[544,128]{1,0:T(8,128)(2,1)S(1)}, bf16[544,128]{1,0:T(8,128)(2,1)S(1)}, u32[]{:S(2)}, u32[]{:S(2)}) collective-permute-start(bf16[544,128]{1,0:T(8,128)(2,1)S(1)} %collective-permute-done.9.refs_3_), channel_id=1, source_target_pairs={{32,0},{64,32},{96,64},{128,96},{160,128},{192,160},{224,192},{256... | collective-permute-start | bytes 417800 | tf_op jit(solution)/shard_map/ppermute | solution.py:313
  141.7 2.2 %flash.13 = (f32[2,512]{1,0:T(2,128)S(1)}, f32[2,512]{1,0:T(2,128)S(1)}, f32[2,64,512]{2,1,0:T(8,128)S(1)}) custom-call(bf16[2,64,512]{2,1,0:T(8,128)(2,1)S(1)} %get-tuple-element.95.refs_0_, f32[2,512]{1,0:T(2,128)S(1)} %broadcast_in_dim.33.refs_1_, bf16[544,128]{1,0:T(8,128)(2,1)S(1)} %collective-permute-done.8.refs_2_, ...), custom_call_target="tpu_custom_call" | custom-call | flops 285212672 | bytes 1048576 | tf_op jit(solution)/shard_map/flash/pallas_call | solution.py:195
  143.9 4.4 %all-to-all-done.2 = bf16[32,4,128,128]{3,2,1,0:T(8,128)(2,1)} async-done(((bf16[32,4,128,128]{3,2,1,0:T(8,128)(2,1)}), bf16[32,4,128,128]{3,2,1,0:T(8,128)(2,1)}, u32[]{:S(2)}, u32[]{:S(2)}) %all-to-all-start.2) | async-done | bytes 4194336 | tf_op jit(solution)/shard_map/all_to_all | solution.py:304
  148.2 1.9 collective-permute-start.12
  150.2 4.6 %collective-permute-start.13 = (bf16[544,128]{1,0:T(8,128)(2,1)S(1)}, bf16[544,128]{1,0:T(8,128)(2,1)S(1)}, u32[]{:S(2)}, u32[]{:S(2)}) collective-permute-start(bf16[544,128]{1,0:T(8,128)(2,1)S(1)} %collective-permute-done.11.refs_3_), channel_id=1, source_target_pairs={{32,0},{64,32},{96,64},{128,96},{160,128},{192,160},{224,192},{256... | collective-permute-start | bytes 417800 | tf_op jit(solution)/shard_map/ppermute | solution.py:313
  154.7 2.1 %flash.14 = (f32[2,512]{1,0:T(2,128)S(1)}, f32[2,512]{1,0:T(2,128)S(1)}, f32[2,64,512]{2,1,0:T(8,128)S(1)}) custom-call(bf16[2,64,512]{2,1,0:T(8,128)(2,1)S(1)} %get-tuple-element.95.refs_0_, f32[2,512]{1,0:T(2,128)S(1)} %broadcast_in_dim.33.refs_1_, bf16[544,128]{1,0:T(8,128)(2,1)S(1)} %collective-permute-done.10.refs_2_, ...), custom_call_target="tpu_custom_call" | custom-call | flops 285212672 | bytes 1048576 | tf_op jit(solution)/shard_map/flash/pallas_call | solution.py:195
  156.9 1.9 collective-permute-start.14
  158.8 4.8 %collective-permute-start.15 = (bf16[544,128]{1,0:T(8,128)(2,1)S(1)}, bf16[544,128]{1,0:T(8,128)(2,1)S(1)}, u32[]{:S(2)}, u32[]{:S(2)}) collective-permute-start(bf16[544,128]{1,0:T(8,128)(2,1)S(1)} %collective-permute-done.13.refs_3_), channel_id=1, source_target_pairs={{32,0},{64,32},{96,64},{128,96},{160,128},{192,160},{224,192},{256... | collective-permute-start | bytes 417800 | tf_op jit(solution)/shard_map/ppermute | solution.py:313
  163.7 2.1 flash.15
  165.8 1.9 collective-permute-start.16
  167.8 2.2 %flash.16 = (f32[2,512]{1,0:T(2,128)S(1)}, f32[2,512]{1,0:T(2,128)S(1)}, f32[2,64,512]{2,1,0:T(8,128)S(1)}) custom-call(bf16[2,64,512]{2,1,0:T(8,128)(2,1)S(1)} %get-tuple-element.95.refs_0_, f32[2,512]{1,0:T(2,128)S(1)} %broadcast_in_dim.33.refs_1_, bf16[544,128]{1,0:T(8,128)(2,1)S(1)} %collective-permute-done.14.refs_2_, ...), custom_call_target="tpu_custom_call" | custom-call | flops 285212672 | bytes 1048576 | tf_op jit(solution)/shard_map/flash/pallas_call | solution.py:195
  169.9 3.2 %collective-permute-done.16.refs_2_ = bf16[544,128]{1,0:T(8,128)(2,1)S(1)} collective-permute-done((bf16[544,128]{1,0:T(8,128)(2,1)S(1)}, bf16[544,128]{1,0:T(8,128)(2,1)S(1)}, u32[]{:S(2)}, u32[]{:S(2)}) %collective-permute-start.16) | collective-permute-done | bytes 139296 | tf_op jit(solution)/shard_map/ppermute | solution.py:312
  173.1 1.4 flash.17
  174.5 8.8 %all_to_all.25.a_ref = bf16[4,128,128]{2,1,0:T(8,128)(2,1)} all-to-all(bf16[4,128,128]{2,1,0:T(8,128)(2,1)S(1)} %flash.17), channel_id=1, replica_groups={{0,8,16,24},{1,9,17,25},{2,10,18,26},{3,11,19,27},{4,12,20,28},{5,13,21..., dimensions={0} | all-to-all | bytes 262144 | tf_op jit(solution)/shard_map/all_to_all | solution.py:324
  183.3 4.6 %out_partial.1 = bf16[128,4096]{1,0:T(8,128)(2,1)} custom-call(bf16[4,128,128]{2,1,0:T(8,128)(2,1)} %all_to_all.25.a_ref, bf16[4,8,4,128,128]{4,3,2,1,0:T(8,128)(2,1)} %bitcast.14.w_ref), custom_call_target="tpu_custom_call" | custom-call | flops 536870912 | bytes 4194304 | tf_op jit(solution)/shard_map/out_partial/pallas_call | solution.py:224
  187.9 11.0 %all-to-all-start.4 = ((bf16[8,16,4096]{2,1,0:T(8,128)(2,1)}), bf16[8,16,4096]{2,1,0:T(8,128)(2,1)S(1)}, u32[]{:S(2)}, u32[]{:S(2)}) async-start(bf16[8,16,4096]{2,1,0:T(8,128)(2,1)} %bitcast.24), calls=%async_computation.4 | async-start | bytes 2097152 | tf_op jit(solution)/shard_map/all_to_all | solution.py:327
  198.9 14.9 %all-to-all-done.4 = bf16[8,16,4096]{2,1,0:T(8,128)(2,1)S(1)} async-done(((bf16[8,16,4096]{2,1,0:T(8,128)(2,1)}), bf16[8,16,4096]{2,1,0:T(8,128)(2,1)S(1)}, u32[]{:S(2)}, u32[]{:S(2)}) %all-to-all-start.4) | async-done | bytes 1048608 | tf_op jit(solution)/shard_map/all_to_all | solution.py:327
  (56 shorter events, 6.0 us)
Async XLA Ops:
  0.0 26.0 %copy-start = (bf16[256,384]{1,0:T(8,128)(2,1)S(1)}, bf16[256,384]{1,0:T(8,128)(2,1)}, u32[]{:S(2)}) copy-start(bf16[256,384]{1,0:T(8,128)(2,1)} %param.18) | copy-start | bytes 589828
  2.5 52.4 %all-to-all-start = ((bf16[16,16,4096]{2,1,0:T(8,128)(2,1)}), bf16[16,16,4096]{2,1,0:T(8,128)(2,1)S(1)}, u32[]{:S(2)}, u32[]{:S(2)}) async-start(bf16[16,16,4096]{2,1,0:T(8,128)(2,1)} %broadcast_in_dim.14), calls=%async_computation | async-start | bytes 4194304 | tf_op jit(solution)/shard_map/all_to_all | solution.py:266
  14.0 9.1 %copy-start.7 = (f32[2]{0:T(128)S(1)}, f32[2]{0:T(128)}, u32[]{:S(2)}) copy-start(f32[2]{0:T(128)} %constant.91.clone) | copy-start | bytes 28
  17.6 8.4 %copy-start.5 = (f32[256]{0:T(256)S(1)}, f32[256]{0:T(256)}, u32[]{:S(2)}) copy-start(f32[256]{0:T(256)} %param.17) | copy-start | bytes 3076
  17.6 8.4 %copy-start.6 = (f32[256]{0:T(256)S(1)}, f32[256]{0:T(256)}, u32[]{:S(2)}) copy-start(f32[256]{0:T(256)} %param.16) | copy-start | bytes 3076
  17.6 62.8 %collective-permute-start = (bf16[4096,256]{1,0:T(8,128)(2,1)}, bf16[4096,256]{1,0:T(8,128)(2,1)}, u32[]{:S(2)}, u32[]{:S(2)}) collective-permute-start(bf16[4096,256]{1,0:T(8,128)(2,1)} %pad_maximum_fusion.w_ref), channel_id=1, source_target_pairs={{0,1},{1,0},{2,3},{3,2},{4,5},{5,4},{6,7},{7,6},{8,9},{9,8},{10,11... | collective-permute-start | bytes 6291464 | tf_op jit(solution)/shard_map/ppermute | solution.py:281
  54.9 3.1 %copy-start.1 = (bf16[16,16,4096]{2,1,0:T(8,128)(2,1)}, bf16[16,16,4096]{2,1,0:T(8,128)(2,1)S(1)}, u32[]{:S(2)}) copy-start(bf16[16,16,4096]{2,1,0:T(8,128)(2,1)S(1)} %all-to-all-done) | copy-start | bytes 6291460
  54.9 3.1 %copy-start.8 = (f32[2]{0:T(128)S(1)}, f32[2]{0:T(128)}, u32[]{:S(2)}) copy-start(f32[2]{0:T(128)} %param.26) | copy-start | bytes 28
  54.9 24.8 %copy-start.4 = (f32[4096]{0:T(1024)S(1)}, f32[4096]{0:T(1024)}, u32[]{:S(2)}) copy-start(f32[4096]{0:T(1024)} %param.19) | copy-start | bytes 49156
  58.7 21.0 %all-to-all-start.1 = ((f32[32,2,384]{2,1,0:T(2,128)}), f32[32,2,384]{2,1,0:T(2,128)S(1)}, u32[]{:S(2)}, u32[]{:S(2)}) async-start(f32[32,2,384]{2,1,0:T(2,128)} %broadcast_in_dim.35), calls=%async_computation.1 | async-start | bytes 196608 | tf_op jit(solution)/shard_map/all_to_all | solution.py:20
  87.5 3.5 %collective-permute-start.1 = (bf16[256,256]{1,0:T(8,128)(2,1)}, bf16[256,256]{1,0:T(8,128)(2,1)S(1)}, u32[]{:S(2)}, u32[]{:S(2)}) collective-permute-start(bf16[256,256]{1,0:T(8,128)(2,1)} %get-tuple-element.93), channel_id=1, source_target_pairs={{0,1},{1,0},{2,3},{3,2},{4,5},{5,4},{6,7},{7,6},{8,9},{9,8},{10,11... | collective-permute-start | bytes 393224 | tf_op jit(solution)/shard_map/ppermute | solution.py:301
  91.0 0.7 copy-start.3
  92.7 55.5 %all-to-all-start.2 = ((bf16[32,4,128,128]{3,2,1,0:T(8,128)(2,1)}), bf16[32,4,128,128]{3,2,1,0:T(8,128)(2,1)}, u32[]{:S(2)}, u32[]{:S(2)}) async-start(bf16[32,4,128,128]{3,2,1,0:T(8,128)(2,1)} %bitcast.22), calls=%async_computation.2 | async-start | bytes 8388608 | tf_op jit(solution)/shard_map/all_to_all | solution.py:304
  97.5 8.0 %collective-permute-start.2 = (bf16[544,128]{1,0:T(8,128)(2,1)S(1)}, bf16[544,128]{1,0:T(8,128)(2,1)S(1)}, u32[]{:S(2)}, u32[]{:S(2)}) collective-permute-start(bf16[544,128]{1,0:T(8,128)(2,1)S(1)} %get-tuple-element.99.refs_2_), channel_id=1, source_target_pairs={{0,32},{32,64},{64,96},{96,128},{128,160},{160,192},{192,224},{224... | collective-permute-start | bytes 417800 | tf_op jit(solution)/shard_map/ppermute | solution.py:312
  99.5 6.9 %collective-permute-start.3 = (bf16[544,128]{1,0:T(8,128)(2,1)S(1)}, bf16[544,128]{1,0:T(8,128)(2,1)S(1)}, u32[]{:S(2)}, u32[]{:S(2)}) collective-permute-start(bf16[544,128]{1,0:T(8,128)(2,1)S(1)} %get-tuple-element.99.refs_2_), channel_id=1, source_target_pairs={{32,0},{64,32},{96,64},{128,96},{160,128},{192,160},{224,192},{256... | collective-permute-start | bytes 417800 | tf_op jit(solution)/shard_map/ppermute | solution.py:313
  106.4 9.5 %collective-permute-start.4 = (bf16[544,128]{1,0:T(8,128)(2,1)S(1)}, bf16[544,128]{1,0:T(8,128)(2,1)S(1)}, u32[]{:S(2)}, u32[]{:S(2)}) collective-permute-start(bf16[544,128]{1,0:T(8,128)(2,1)S(1)} %collective-permute-done.2.refs_2_), channel_id=1, source_target_pairs={{0,32},{32,64},{64,96},{96,128},{128,160},{160,192},{192,224},{224... | collective-permute-start | bytes 417800 | tf_op jit(solution)/shard_map/ppermute | solution.py:312
  108.3 7.6 %collective-permute-start.5 = (bf16[544,128]{1,0:T(8,128)(2,1)S(1)}, bf16[544,128]{1,0:T(8,128)(2,1)S(1)}, u32[]{:S(2)}, u32[]{:S(2)}) collective-permute-start(bf16[544,128]{1,0:T(8,128)(2,1)S(1)} %collective-permute-done.3.refs_3_), channel_id=1, source_target_pairs={{32,0},{64,32},{96,64},{128,96},{160,128},{192,160},{224,192},{256... | collective-permute-start | bytes 417800 | tf_op jit(solution)/shard_map/ppermute | solution.py:313
  115.9 9.3 %collective-permute-start.6 = (bf16[544,128]{1,0:T(8,128)(2,1)S(1)}, bf16[544,128]{1,0:T(8,128)(2,1)S(1)}, u32[]{:S(2)}, u32[]{:S(2)}) collective-permute-start(bf16[544,128]{1,0:T(8,128)(2,1)S(1)} %collective-permute-done.4.refs_2_), channel_id=1, source_target_pairs={{0,32},{32,64},{64,96},{96,128},{128,160},{160,192},{192,224},{224... | collective-permute-start | bytes 417800 | tf_op jit(solution)/shard_map/ppermute | solution.py:312
  117.8 7.4 %collective-permute-start.7 = (bf16[544,128]{1,0:T(8,128)(2,1)S(1)}, bf16[544,128]{1,0:T(8,128)(2,1)S(1)}, u32[]{:S(2)}, u32[]{:S(2)}) collective-permute-start(bf16[544,128]{1,0:T(8,128)(2,1)S(1)} %collective-permute-done.5.refs_3_), channel_id=1, source_target_pairs={{32,0},{64,32},{96,64},{128,96},{160,128},{192,160},{224,192},{256... | collective-permute-start | bytes 417800 | tf_op jit(solution)/shard_map/ppermute | solution.py:313
  125.2 9.5 %collective-permute-start.8 = (bf16[544,128]{1,0:T(8,128)(2,1)S(1)}, bf16[544,128]{1,0:T(8,128)(2,1)S(1)}, u32[]{:S(2)}, u32[]{:S(2)}) collective-permute-start(bf16[544,128]{1,0:T(8,128)(2,1)S(1)} %collective-permute-done.6.refs_2_), channel_id=1, source_target_pairs={{0,32},{32,64},{64,96},{96,128},{128,160},{160,192},{192,224},{224... | collective-permute-start | bytes 417800 | tf_op jit(solution)/shard_map/ppermute | solution.py:312
  127.1 7.6 %collective-permute-start.9 = (bf16[544,128]{1,0:T(8,128)(2,1)S(1)}, bf16[544,128]{1,0:T(8,128)(2,1)S(1)}, u32[]{:S(2)}, u32[]{:S(2)}) collective-permute-start(bf16[544,128]{1,0:T(8,128)(2,1)S(1)} %collective-permute-done.7.refs_3_), channel_id=1, source_target_pairs={{32,0},{64,32},{96,64},{128,96},{160,128},{192,160},{224,192},{256... | collective-permute-start | bytes 417800 | tf_op jit(solution)/shard_map/ppermute | solution.py:313
  134.7 9.1 %collective-permute-start.10 = (bf16[544,128]{1,0:T(8,128)(2,1)S(1)}, bf16[544,128]{1,0:T(8,128)(2,1)S(1)}, u32[]{:S(2)}, u32[]{:S(2)}) collective-permute-start(bf16[544,128]{1,0:T(8,128)(2,1)S(1)} %collective-permute-done.8.refs_2_), channel_id=1, source_target_pairs={{0,32},{32,64},{64,96},{96,128},{128,160},{160,192},{192,224},{224... | collective-permute-start | bytes 417800 | tf_op jit(solution)/shard_map/ppermute | solution.py:312
  136.7 7.2 %collective-permute-start.11 = (bf16[544,128]{1,0:T(8,128)(2,1)S(1)}, bf16[544,128]{1,0:T(8,128)(2,1)S(1)}, u32[]{:S(2)}, u32[]{:S(2)}) collective-permute-start(bf16[544,128]{1,0:T(8,128)(2,1)S(1)} %collective-permute-done.9.refs_3_), channel_id=1, source_target_pairs={{32,0},{64,32},{96,64},{128,96},{160,128},{192,160},{224,192},{256... | collective-permute-start | bytes 417800 | tf_op jit(solution)/shard_map/ppermute | solution.py:313
  148.2 8.7 %collective-permute-start.12 = (bf16[544,128]{1,0:T(8,128)(2,1)S(1)}, bf16[544,128]{1,0:T(8,128)(2,1)S(1)}, u32[]{:S(2)}, u32[]{:S(2)}) collective-permute-start(bf16[544,128]{1,0:T(8,128)(2,1)S(1)} %collective-permute-done.10.refs_2_), channel_id=1, source_target_pairs={{0,32},{32,64},{64,96},{96,128},{128,160},{160,192},{192,224},{224... | collective-permute-start | bytes 417800 | tf_op jit(solution)/shard_map/ppermute | solution.py:312
  150.2 6.8 %collective-permute-start.13 = (bf16[544,128]{1,0:T(8,128)(2,1)S(1)}, bf16[544,128]{1,0:T(8,128)(2,1)S(1)}, u32[]{:S(2)}, u32[]{:S(2)}) collective-permute-start(bf16[544,128]{1,0:T(8,128)(2,1)S(1)} %collective-permute-done.11.refs_3_), channel_id=1, source_target_pairs={{32,0},{64,32},{96,64},{128,96},{160,128},{192,160},{224,192},{256... | collective-permute-start | bytes 417800 | tf_op jit(solution)/shard_map/ppermute | solution.py:313
  156.9 8.9 %collective-permute-start.14 = (bf16[544,128]{1,0:T(8,128)(2,1)S(1)}, bf16[544,128]{1,0:T(8,128)(2,1)S(1)}, u32[]{:S(2)}, u32[]{:S(2)}) collective-permute-start(bf16[544,128]{1,0:T(8,128)(2,1)S(1)} %collective-permute-done.12.refs_2_), channel_id=1, source_target_pairs={{0,32},{32,64},{64,96},{96,128},{128,160},{160,192},{192,224},{224... | collective-permute-start | bytes 417800 | tf_op jit(solution)/shard_map/ppermute | solution.py:312
  158.8 7.0 %collective-permute-start.15 = (bf16[544,128]{1,0:T(8,128)(2,1)S(1)}, bf16[544,128]{1,0:T(8,128)(2,1)S(1)}, u32[]{:S(2)}, u32[]{:S(2)}) collective-permute-start(bf16[544,128]{1,0:T(8,128)(2,1)S(1)} %collective-permute-done.13.refs_3_), channel_id=1, source_target_pairs={{32,0},{64,32},{96,64},{128,96},{160,128},{192,160},{224,192},{256... | collective-permute-start | bytes 417800 | tf_op jit(solution)/shard_map/ppermute | solution.py:313
  165.8 7.3 %collective-permute-start.16 = (bf16[544,128]{1,0:T(8,128)(2,1)S(1)}, bf16[544,128]{1,0:T(8,128)(2,1)S(1)}, u32[]{:S(2)}, u32[]{:S(2)}) collective-permute-start(bf16[544,128]{1,0:T(8,128)(2,1)S(1)} %collective-permute-done.14.refs_2_), channel_id=1, source_target_pairs={{0,32},{32,64},{64,96},{96,128},{128,160},{160,192},{192,224},{224... | collective-permute-start | bytes 417800 | tf_op jit(solution)/shard_map/ppermute | solution.py:312
  187.9 26.1 %copy-start.2 = (bf16[16,4096]{1,0:T(8,128)(2,1)S(1)}, bf16[16,4096]{1,0:T(8,128)(2,1)}, u32[]{:S(2)}) copy-start(bf16[16,4096]{1,0:T(8,128)(2,1)} %param.14) | copy-start | bytes 393220
  187.9 26.0 %all-to-all-start.4 = ((bf16[8,16,4096]{2,1,0:T(8,128)(2,1)}), bf16[8,16,4096]{2,1,0:T(8,128)(2,1)S(1)}, u32[]{:S(2)}, u32[]{:S(2)}) async-start(bf16[8,16,4096]{2,1,0:T(8,128)(2,1)} %bitcast.24), calls=%async_computation.4 | async-start | bytes 2097152 | tf_op jit(solution)/shard_map/all_to_all | solution.py:327

commit v2 on v1

--- a/solution.py
+++ b/solution.py
@@ -7,6 +7,7 @@
 from jax.experimental.pallas import tpu as pltpu
 from jax.sharding import PartitionSpec as P
 
+
 GRID_W = 64
 EPS = 1e-06
 LOG2E = math.log2(math.e)
@@ -15,18 +16,45 @@
 NXC = 8
 
 
-def copy_for_each(shard, axis):
-    copies = jnp.broadcast_to(shard, (lax.axis_size(axis), *shard.shape))
-    return lax.all_to_all(copies, axis, split_axis=0, concat_axis=0, tiled=True)
-
-
 def modulated(x, gain, shift):
     x = x.astype(jnp.float32)
     ms = jnp.mean(x * x, axis=-1, keepdims=True)
     return (x * lax.rsqrt(ms + EPS) * gain + shift).astype(jnp.bfloat16)
 
 
-def qkv_body(hs, lat_ref, ctx_ref, gain_ref, shift_ref, w_ref, w2_ref, qg_ref, kg_ref, cos_ref, sin_ref, own_ref, other_ref, ctx_kv_ref):
+VMEM = pl.BlockSpec(memory_space=pltpu.VMEM)
+SMEM = pl.BlockSpec(memory_space=pltpu.SMEM)
+
+
+def near(*arrays):
+    return [pltpu.with_memory_space_constraint(a, pltpu.VMEM) for a in arrays]
+
+
+def spread_body(w_ref, o_ref, sems):
+    copies = []
+    for y in range(o_ref.shape[0]):
+        for k in range(w_ref.shape[0]):
+            copies.append(pltpu.make_async_copy(w_ref.at[k], o_ref.at[y, :, k], sems.at[y, k]))
+    for copy in copies:
+        copy.start()
+    for copy in copies:
+        copy.wait()
+
+
+def spread(w):
+    ny, nxc, kk, n = w.shape
+    return pl.pallas_call(
+        spread_body,
+        in_specs=[VMEM],
+        out_specs=pl.BlockSpec(memory_space=pl.ANY),
+        out_shape=jax.ShapeDtypeStruct((ny, nxc, ny, kk, n), w.dtype),
+        scratch_shapes=[pltpu.SemaphoreType.DMA((ny, ny))],
+        cost_estimate=pl.CostEstimate(flops=0, bytes_accessed=10 * w.size, transcendentals=0),
+        name="spread",
+    )(w)
+
+
+def qkv_body(hs, lat_ref, ctx_ref, gain_ref, shift_ref, wq_ref, wkv_ref, wq2_ref, wkv2_ref, qg_ref, kg_ref, cos_ref, sin_ref, own_ref, other_ref, ctx_kv_ref):
     def unit(v):
         return v * lax.rsqrt(jnp.mean(v * v, axis=-1, keepdims=True) + EPS)
 
@@ -36,56 +64,48 @@
         right = pltpu.roll(v, 1, 1)
         return v * cos + jnp.where(lane % 2 == 0, left, right) * sin
 
+    def against(a, w):
+        return lax.dot_general(a, w[...], (((1,), (1,)), ((), ())), preferred_element_type=jnp.float32)
+
     x = modulated(lat_ref[...], gain_ref[0:1], shift_ref[0:1])
     cos = cos_ref[...]
     sin = sin_ref[...]
-    for w, o_ref in ((w_ref, own_ref), (w2_ref, other_ref)):
-        y = jnp.dot(x, w[...], preferred_element_type=jnp.float32)
-        q = jnp.concatenate([unit(y[:, :hs]), unit(y[:, hs : 2 * hs])], axis=1) * qg_ref[...]
+    for wq, wkv, o_ref in ((wq_ref, wkv_ref, own_ref), (wq2_ref, wkv2_ref, other_ref)):
+        y = jnp.dot(x, wq[...], preferred_element_type=jnp.float32)
+        q = jnp.concatenate([unit(y[:, :hs]), unit(y[:, hs:])], axis=1) * qg_ref[...]
         q = turn(q, cos, sin).astype(jnp.bfloat16)
         o_ref[:, : 2 * hs] = q * jnp.bfloat16(hs ** -0.5)
-        kv = y[:, 2 * hs :]
+        kv = against(x, wkv)
         k = unit(kv[:, :hs]) * kg_ref[...]
         k2 = turn(jnp.concatenate([k, k], axis=1), cos, sin)
         lane = lax.broadcasted_iota(jnp.int32, k2.shape, 1)
         o_ref[:, 2 * hs :] = jnp.where(lane < hs, k2, kv).astype(jnp.bfloat16)
 
-    @pl.when(pl.program_id(0) == 0)
-    def _():
-        c = modulated(ctx_ref[...], gain_ref[1:2], shift_ref[1:2])
-        ckv = jnp.dot(c, w_ref[:, 2 * hs :], preferred_element_type=jnp.float32)
-        ck = unit(ckv[:, :hs]) * kg_ref[...]
-        ctx_kv_ref[...] = jnp.concatenate([ck, ckv[:, hs:]], axis=1).astype(jnp.bfloat16)
-
-
-def qkv(lat, context, gain, shift, w, w2, qg, kg, cos, sin):
-    rows, width = lat.shape
-    n_ctx = context.shape[0]
-    hs = kg.shape[1]
-    step = rows // 2
-    whole = lambda a: pl.BlockSpec(a.shape, lambda i: (0,) * a.ndim)
+    c = modulated(ctx_ref[...], gain_ref[1:2], shift_ref[1:2])
+    ckv = against(c, wkv_ref)
+    ck = unit(ckv[:, :hs]) * kg_ref[...]
+    ctx_kv_ref[...] = jnp.concatenate([ck, ckv[:, hs:]], axis=1).astype(jnp.bfloat16)
+
+
+def qkv(*args):
+    rows = args[0].shape[0]
+    n_ctx = args[1].shape[0]
+    hs = args[9].shape[1]
     return pl.pallas_call(
         functools.partial(qkv_body, hs),
-        grid=(rows // step,),
-        in_specs=[
-            pl.BlockSpec((step, width), lambda i: (i, 0)),
-            whole(context), whole(gain), whole(shift), whole(w), whole(w2), whole(qg), whole(kg),
-            pl.BlockSpec((step, 2 * hs), lambda i: (i, 0)),
-            pl.BlockSpec((step, 2 * hs), lambda i: (i, 0)),
-        ],
-        out_specs=[
-            pl.BlockSpec((step, 4 * hs), lambda i: (i, 0)),
-            pl.BlockSpec((step, 4 * hs), lambda i: (i, 0)),
-            pl.BlockSpec((n_ctx, 2 * hs), lambda i: (0, 0)),
-        ],
+        in_specs=[VMEM] * len(args),
+        out_specs=[VMEM] * 3,
         out_shape=[
             jax.ShapeDtypeStruct((rows, 4 * hs), jnp.bfloat16),
             jax.ShapeDtypeStruct((rows, 4 * hs), jnp.bfloat16),
             jax.ShapeDtypeStruct((n_ctx, 2 * hs), jnp.bfloat16),
         ],
-        cost_estimate=pl.CostEstimate(flops=4 * rows * width * 4 * hs, bytes_accessed=6 << 20, transcendentals=0),
+        cost_estimate=pl.CostEstimate(
+            flops=16 * rows * args[0].shape[1] * hs, bytes_accessed=6 << 20, transcendentals=0
+        ),
+        compiler_params=pltpu.CompilerParams(vmem_limit_bytes=24 << 20),
         name="qkv",
-    )(lat, context, gain, shift, w, w2, qg, kg, cos, sin)
+    )(*near(*args))
 
 
 def assemble_body(core_ref, own_ref, got_ref, ctx_ref, qt_ref, kv_ref):
@@ -110,9 +130,6 @@
     kv_ref[0:rows] = own_ref[:, 2 * hs :]
     kv_ref[rows : 2 * rows] = got_ref[:, 2 * hs :]
     kv_ref[2 * rows :] = ctx_ref[...]
-
-
-VMEM = pl.BlockSpec(memory_space=pltpu.VMEM)
 
 
 def assemble(core, own, got, ctx_kv):
@@ -120,14 +137,14 @@
     hs = cols // 4
     return pl.pallas_call(
         assemble_body,
-        in_specs=[pl.BlockSpec(memory_space=pltpu.SMEM), VMEM, VMEM, VMEM],
+        in_specs=[SMEM, VMEM, VMEM, VMEM],
         out_specs=[VMEM, VMEM],
         out_shape=[
             pltpu.VMEM((2, hs, 2 * rows), jnp.bfloat16),
             pltpu.VMEM((2 * rows + ctx_kv.shape[0], 2 * hs), jnp.bfloat16),
         ],
         name="assemble",
-    )(core, own, got, ctx_kv)
+    )(core, *near(own, got, ctx_kv))
 
 
 def flash_body(n_blocks, first, last, lat_rows, hs, *refs):
@@ -183,7 +200,7 @@
     heads, hs, qn = qt.shape
     first = state is None
     args = [qt, lift, *blocks] + ([] if first else list(state))
-    args = [pltpu.with_memory_space_constraint(a, pltpu.VMEM) for a in args]
+    args = near(*args)
     if last:
         outs = [pltpu.VMEM((NY, qn // NY, heads * hs), jnp.bfloat16)]
     else:
@@ -205,34 +222,41 @@
     return res[0] if last else res
 
 
-def project_body(a_ref, w_ref, o_ref):
+def project_body(core_ref, a_ref, w_ref, keep_ref, send_ref):
     ny = a_ref.shape[0]
-    a = jnp.concatenate([a_ref[y] for y in range(ny)], axis=1)
+    half = a_ref.shape[1] // 2
+    core = core_ref[0]
+
+    def rows_of(c):
+        start = pl.multiple_of(c * half, half)
+        return jnp.concatenate([a_ref[y, pl.ds(start, half), :] for y in range(ny)], axis=1)
+
+    a = jnp.concatenate([rows_of(core), rows_of(1 - core)], axis=0)
     n = w_ref.shape[4]
-
-    def column(j):
-        return jnp.concatenate([w_ref[0, j, y] for y in range(ny)], axis=0)
-
-    for j in range(0, w_ref.shape[1], 2):
-        w = jnp.concatenate([column(j), column(j + 1)], axis=1)
-        o_ref[:, j * n : (j + 2) * n] = jnp.dot(a, w, preferred_element_type=jnp.float32).astype(jnp.bfloat16)
-
-
-def out_partial(a, w):
-    ny, nxc, ny2, kk, n = w.shape
-    rows = a.shape[1]
+    cols = [(i, j) for i in range(w_ref.shape[0]) for j in range(w_ref.shape[1])]
+
+    def column(i, j):
+        return jnp.concatenate([w_ref[i, j, y] for y in range(ny)], axis=0)
+
+    for k in range(0, len(cols), 2):
+        w = jnp.concatenate([column(*cols[k]), column(*cols[k + 1])], axis=1)
+        r = jnp.dot(a, w, preferred_element_type=jnp.float32).astype(jnp.bfloat16)
+        keep_ref[:, k * n : (k + 2) * n] = r[:half]
+        send_ref[:, k * n : (k + 2) * n] = r[half:]
+
+
+def out_partial(core, a, w):
+    half = a.shape[1] // 2
+    width = w.shape[0] * w.shape[1] * w.shape[4]
     return pl.pallas_call(
         project_body,
-        grid=(ny,),
-        in_specs=[
-            pl.BlockSpec(a.shape, lambda i: (0, 0, 0)),
-            pl.BlockSpec((1, nxc, ny2, kk, n), lambda i: (i, 0, 0, 0, 0)),
-        ],
-        out_specs=pl.BlockSpec((rows, nxc * n), lambda i: (0, i)),
-        out_shape=jax.ShapeDtypeStruct((rows, ny * nxc * n), jnp.bfloat16),
-        cost_estimate=pl.CostEstimate(flops=2 * rows * w.size, bytes_accessed=2 * w.size, transcendentals=0),
+        in_specs=[SMEM, VMEM, VMEM],
+        out_specs=[VMEM, VMEM],
+        out_shape=[pltpu.VMEM((half, width), jnp.bfloat16), pltpu.VMEM((half, width), jnp.bfloat16)],
+        cost_estimate=pl.CostEstimate(flops=4 * half * w.size, bytes_accessed=2 * w.size, transcendentals=0),
+        compiler_params=pltpu.CompilerParams(vmem_limit_bytes=24 << 20),
         name="out_partial",
-    )(a, w)
+    )(core, *near(a, w))
 
 
 def local(
@@ -255,7 +279,7 @@
     n_sp = lax.axis_size("sp")
     n_tp = lax.axis_size("tp")
     group_y = [[y * NXC + c for y in range(NY)] for c in range(NXC)]
-    group_cx = [[y * NXC + 2 * x + c for c in range(2) for x in range(NX)] for y in range(NY)]
+    group_x = [[y * NXC + 2 * x + c for x in range(NX)] for y in range(NY) for c in range(2)]
     group_core = [[2 * i + c for i in range(n_tp // 2)] for c in range(2)]
     swap = [(t, t ^ 1) for t in range(n_tp)]
     tp = lax.axis_index("tp")
@@ -277,27 +301,36 @@
     cos = jnp.tile(jnp.repeat(jnp.cos(angles), 2, axis=1), (1, 2))
     sign = jnp.tile(jnp.array([-1.0, 1.0], jnp.float32), hs)
     sin = jnp.tile(jnp.repeat(jnp.sin(angles), 2, axis=1), (1, 2)) * sign
-    w_own = jnp.concatenate([query_weight, key_weight, value_weight], axis=1)
-    w_other = lax.ppermute(w_own, "tp", swap)
-    per_head = out_weight.shape[0] // n_tp
-    w_split = out_weight.reshape(NY, NXC, per_head, out_weight.shape[1]).transpose(1, 0, 2, 3)
-    w_split = jnp.broadcast_to(w_split, (NY, *w_split.shape)).reshape(n_tp, *w_split.shape[1:])
     lift = jnp.broadcast_to(context_lift[:, None], (context_lift.shape[0], block_rows))
     q_gain = jnp.tile(query_gain, 2)[None]
     k_gain = key_gain[None]
 
     cond_pair = jax.nn.silu(jnp.stack([condition, context_cond])).astype(jnp.bfloat16)
     partial_mod = jnp.dot(cond_pair, mod_weight, preferred_element_type=jnp.float32)
-    summed_mod = lax.psum(partial_mod, "sp")
-    summed_mod, lat_half, w_own, cos, sin, w_split, lift, q_gain, k_gain = lax.optimization_barrier(
-        (summed_mod, lat_half, w_own, cos, sin, w_split, lift, q_gain, k_gain)
+    run = math.gcd(n_sp, 4)
+    near_z = [[g * run + i for i in range(run)] for g in range(n_sp // run)]
+    far_z = [[g + run * i for i in range(n_sp // run)] for g in range(run)]
+    summed_mod = lax.psum(lax.psum(partial_mod, "sp", axis_index_groups=near_z), "sp", axis_index_groups=far_z)
+    summed_mod, lat_half, cos, sin, lift, q_gain, k_gain = lax.optimization_barrier(
+        (summed_mod, lat_half, cos, sin, lift, q_gain, k_gain)
     )
-    mod = copy_for_each(summed_mod, "tp")
+    summed_mod, query_weight, key_weight, value_weight, out_weight = lax.optimization_barrier(
+        (summed_mod, query_weight, key_weight, value_weight, out_weight)
+    )
+    wq = query_weight
+    wkv = jnp.concatenate([key_weight.T, value_weight.T], axis=0)
+    wq2 = lax.ppermute(wq, "tp", swap)
+    wkv2 = lax.ppermute(wkv, "tp", swap)
+    per_head = out_weight.shape[0] // n_tp
+    w_split = spread(out_weight.reshape(NY, NXC, per_head, out_weight.shape[1]))
+    w_split = w_split.reshape(n_tp, NY, per_head, out_weight.shape[1])
+    mod_copies = jnp.broadcast_to(summed_mod, (n_tp, *summed_mod.shape))
+    mod = lax.all_to_all(mod_copies, "tp", 0, 0, tiled=True)
     mod = jnp.moveaxis(mod, 0, 1).reshape(2, 3 * width)
     shift = mod[:, :width]
     gain = norm_gain * (1.0 + mod[:, width : 2 * width])
 
-    own, other, ctx_kv = qkv(lat_half, context, gain, shift, w_own, w_other, q_gain, k_gain, cos, sin)
+    own, other, ctx_kv = qkv(lat_half, context, gain, shift, wq, wkv, wq2, wkv2, q_gain, k_gain, cos, sin)
     got = lax.ppermute(other, "tp", swap)
     qt, kv = assemble(core.reshape(1).astype(jnp.int32), own, got, ctx_kv)
     kv, w_split = lax.optimization_barrier((kv, w_split))
@@ -312,7 +345,7 @@
         nxt_f = lax.ppermute(fwd, "sp", up)
         nxt_b = lax.ppermute(bwd, "sp", down) if step < n_sp // 2 else None
         state = flash(qt, lift, blocks, state, block_rows, False)
-        if step == 5:
+        if step == 7:
             nxt_f, nxt_b, state, w_rows = lax.optimization_barrier((nxt_f, nxt_b, state, w_rows))
         else:
             nxt_f, nxt_b, state = lax.optimization_barrier((nxt_f, nxt_b, state))
@@ -322,9 +355,10 @@
     w_rows = w_rows.reshape(NY, NXC, *w_rows.shape[1:])
 
     heads_y = lax.all_to_all(attended, "tp", 0, 0, axis_index_groups=group_y, tiled=True)
-    part = out_partial(heads_y, w_rows)
-    part = part.reshape(NXC, own_rows, width)
-    parts = lax.all_to_all(part, "tp", 0, 0, axis_index_groups=group_cx, tiled=True)
+    keep, send = out_partial(core.reshape(1).astype(jnp.int32), heads_y, w_rows)
+    part = keep.astype(jnp.float32) + lax.ppermute(send, "tp", swap).astype(jnp.float32)
+    part = part.astype(jnp.bfloat16).reshape(NX, own_rows, width)
+    parts = lax.all_to_all(part, "tp", 0, 0, axis_index_groups=group_x, tiled=True)
     mixed = jnp.sum(parts.astype(jnp.float32), axis=0).astype(jnp.bfloat16)
     gate = mod[0, 2 * width :]
     return (latent.astype(jnp.float32) + gate * mixed.astype(jnp.float32)).astype(jnp.bfloat16)

time: 216 us -> 207 us (0.958)
  waiting for transfers between devices: 31.4 us -> 21.9 us
  local copies, waits for them, and re-layouts: 14.7 us -> 12 us
    ppermute x1 -> x3, starting transfers between devices: 5.01 us -> 19.6 us  [the longest x1 11.6 us: local(): lax.ppermute(send, 'tp', swap).astype(jnp.float32)]
    all_to_all x2, starting transfers between devices: 24.7 us -> 11.8 us  [the longest x1 7.81 us: local(): mod = lax.all_to_all(mod_copies, 'tp', 0, 0, tiled=True)]
    all_to_all x2, waiting for transfers between devices: 21.6 us -> 13.9 us  [the longest x1 8.15 us: local(): lax.all_to_all(part, 'tp', 0, 0, axis_index_groups=group_x, tiled=True)]
    ppermute x7, starting transfers between devices: 35 us -> 28.3 us  [local(): nxt_b = lax.ppermute(bwd, 'sp', down) if step < n_sp // 2 else None]
    ppermute x8, starting transfers between devices: 15.3 us -> 21.5 us  [local(): nxt_f = lax.ppermute(fwd, 'sp', up)]
    all_to_all x1, waiting for transfers between devices: 4.37 us -> 0.01 us  [local(): w_rows = lax.all_to_all(w_split, 'tp', 0, 0, tiled=True)]
    broadcast_in_dim x2 -> x1, local copies, waits for them, and re-layouts: 3.69 us -> 0.67 us  [local(): mod_copies = jnp.broadcast_to(summed_mod, (n_tp, *summed_mod.shape))]
    ppermute x8, waiting for transfers between devices: 3.5 us -> 5.94 us  [local(): nxt_f = lax.ppermute(fwd, 'sp', up)]
  transfers between devices with their start and end apart: 21 -> 23, of which waited for: 7 -> 6; matrix products, arithmetic and copies ran while one was open for 8% -> 4% of each run, Pallas kernels for 8% -> 10%
where the time goes in v2:
time: 207 us; the launch traced here: 205 us
  starting transfers between devices  95.8 us (46%)
  blocking collectives  37.4 us (18%)
  Pallas kernels  30 us (14%)
  waiting for transfers between devices  21.9 us (11%)
  local copies, waits for them, and re-layouts  12 us (6%)
  other arithmetic  6.55 us (3%)
    ppermute x7, starting transfers between devices, local(): nxt_b = lax.ppermute(bwd, 'sp', down) if step < n_sp // 2 else None  28.3 us
    ppermute x8, starting transfers between devices, local(): nxt_f = lax.ppermute(fwd, 'sp', up)  21.5 us
    pallas_call x9, Pallas kernels, flash(): pl.pallas_call(functools.partial(flash_body, len(blocks), first, last, la...  17.6 us
    psum x1, blocking collectives, local(): lax.psum(lax.psum(partial_mod, 'sp', axis_index_groups=near_z), 'sp', axi...  16.8 us
    ppermute x1, starting transfers between devices, local(): lax.ppermute(send, 'tp', swap).astype(jnp.float32)  11.6 us
    psum x1, blocking collectives, local(): lax.psum(partial_mod, 'sp', axis_index_groups=near_z)  11.5 us
    all_to_all x1, blocking collectives, local(): lax.all_to_all(attended, 'tp', 0, 0, axis_index_groups=group_y, tiled=True)  9.09 us
    all_to_all x1, waiting for transfers between devices, local(): lax.all_to_all(part, 'tp', 0, 0, axis_index_groups=group_x, tiled=True)  8.15 us
  transfers between devices with their start and end apart: 23, of which 6 were waited for; matrix products, arithmetic and copies ran while one was open for 4% of the time, Pallas kernels for 10%

profile of v2, /device:TPU:1, one launch (start us, length us, event | category | flops | bytes accessed | tf_op | source)
XLA Modules:
  0.0 205.2 jit_solution(8469302510339256744)
XLA Ops:
  0.0 2.5 %broadcast_in_dim.12 = bf16[16,16,4096]{2,1,0:T(8,128)(2,1)} broadcast(bf16[16,4096]{1,0:T(8,128)(2,1)} %param.14), dimensions={1,2} | broadcast | bytes 2228224 | tf_op jit(solution)/shard_map/broadcast_in_dim | solution.py:289
  2.5 7.7 %all-to-all-start = ((bf16[16,16,4096]{2,1,0:T(8,128)(2,1)}), bf16[16,16,4096]{2,1,0:T(8,128)(2,1)S(1)}, u32[]{:S(2)}, u32[]{:S(2)}) async-start(bf16[16,16,4096]{2,1,0:T(8,128)(2,1)} %broadcast_in_dim.12), calls=%async_computation | async-start | bytes 4194304 | tf_op jit(solution)/shard_map/all_to_all | solution.py:290
  14.5 11.5 %psum.14 = f32[2,384]{1,0:T(2,128)S(1)} all-reduce(f32[2,384]{1,0:T(2,128)S(1)} %fusion.6), channel_id=1, replica_groups={{0,32,64,96},{128,160,192,224},{256,288,320,352},{384,416,448,480},{1,3..., use_global_device_ids=true, to_apply=%region_0.1 | all-reduce | flops 768 | bytes 6144 | tf_op jit(solution)/shard_map/psum | solution.py:313
  26.0 16.8 %psum.15 = f32[2,384]{1,0:T(2,128)S(1)} all-reduce(f32[2,384]{1,0:T(2,128)S(1)} %psum.14), channel_id=1, replica_groups={{0,128,256,384},{32,160,288,416},{64,192,320,448},{96,224,352,480},{1,1..., use_global_device_ids=true, to_apply=%region_1.2 | all-reduce | flops 768 | bytes 6144 | tf_op jit(solution)/shard_map/psum | solution.py:313
  42.8 0.9 broadcast_multiply_fusion.sin_ref
  45.2 2.3 %pad_maximum_fusion.wkv_ref = bf16[128,4096]{1,0:T(8,128)(2,1)} fusion(bf16[64,4096]{1,0:T(8,128)(2,1)} %bitcast.28, bf16[64,4096]{1,0:T(8,128)(2,1)} %bitcast.29), kind=kLoop, calls=%fused_computation | loop fusion | flops 2097152 | bytes 2097152 | tf_op jit(solution)/shard_map/concatenate | solution.py:321
  47.5 6.0 %collective-permute-start.1 = (bf16[128,4096]{1,0:T(8,128)(2,1)}, bf16[128,4096]{1,0:T(8,128)(2,1)}, u32[]{:S(2)}, u32[]{:S(2)}) collective-permute-start(bf16[128,4096]{1,0:T(8,128)(2,1)} %pad_maximum_fusion.wkv_ref), channel_id=1, source_target_pairs={{0,1},{1,0},{2,3},{3,2},{4,5},{5,4},{6,7},{7,6},{8,9},{9,8},{10,11... | collective-permute-start | bytes 3145736 | tf_op jit(solution)/shard_map/ppermute | solution.py:323
  53.5 1.9 collective-permute-start
  56.1 7.8 %all-to-all-start.1 = ((f32[32,2,384]{2,1,0:T(2,128)}), f32[32,2,384]{2,1,0:T(2,128)}, u32[]{:S(2)}, u32[]{:S(2)}) async-start(f32[32,2,384]{2,1,0:T(2,128)} %broadcast_in_dim.31), calls=%async_computation.1 | async-start | bytes 196608 | tf_op jit(solution)/shard_map/all_to_all | solution.py:328
  63.9 1.6 copy.18.cos_ref
  65.6 5.8 %all-to-all-done.1 = f32[32,2,384]{2,1,0:T(2,128)} async-done(((f32[32,2,384]{2,1,0:T(2,128)}), f32[32,2,384]{2,1,0:T(2,128)}, u32[]{:S(2)}, u32[]{:S(2)}) %all-to-all-start.1) | async-done | bytes 98336 | tf_op jit(solution)/shard_map/all_to_all | solution.py:328
  73.1 0.9 copy-done.3
  74.1 5.9 %qkv.1 = (bf16[256,256]{1,0:T(8,128)(2,1)S(1)}, bf16[256,256]{1,0:T(8,128)(2,1)}, bf16[32,128]{1,0:T(8,128)(2,1)S(1)}) custom-call(bf16[256,4096]{1,0:T(8,128)(2,1)S(1)} %bitcast.22, bf16[32,4096]{1,0:T(8,128)(2,1)S(1)} %copy-done.3, f32[2,4096]{1,0:T(2,128)S(1)} %get-tuple-element.176.gain_ref, f32[2,4096]{1,0:T(2,128)S(1)} %get-tuple-element.175.shift_ref, ...), custom_call_target="tpu_custom_call" | custom-call | flops 1073741824 | bytes 6291456 | tf_op jit(solution)/shard_map/qkv/pallas_call | solution.py:94
  80.6 2.3 %collective-permute-start.2 = (bf16[256,256]{1,0:T(8,128)(2,1)}, bf16[256,256]{1,0:T(8,128)(2,1)S(1)}, u32[]{:S(2)}, u32[]{:S(2)}) collective-permute-start(bf16[256,256]{1,0:T(8,128)(2,1)} %get-tuple-element.101), channel_id=1, source_target_pairs={{0,1},{1,0},{2,3},{3,2},{4,5},{5,4},{6,7},{7,6},{8,9},{9,8},{10,11... | collective-permute-start | bytes 393224 | tf_op jit(solution)/shard_map/ppermute | solution.py:334
  82.9 3.4 %spread.1 = bf16[4,8,4,128,128]{4,3,2,1,0:T(8,128)(2,1)} custom-call(bf16[4,8,128,128]{3,2,1,0:T(8,128)(2,1)} %bitcast.25), custom_call_target="tpu_custom_call" | custom-call | bytes 5242880 | tf_op jit(solution)/shard_map/spread/pallas_call | solution.py:46
  86.5 4.7 %all-to-all-start.2 = ((bf16[32,4,128,128]{3,2,1,0:T(8,128)(2,1)}), bf16[32,4,128,128]{3,2,1,0:T(8,128)(2,1)}, u32[]{:S(2)}, u32[]{:S(2)}) async-start(bf16[32,4,128,128]{3,2,1,0:T(8,128)(2,1)} %bitcast.24), calls=%async_computation.2 | async-start | bytes 8388608 | tf_op jit(solution)/shard_map/all_to_all | solution.py:337
  91.2 3.2 %collective-permute-start.4 = (bf16[544,128]{1,0:T(8,128)(2,1)S(1)}, bf16[544,128]{1,0:T(8,128)(2,1)S(1)}, u32[]{:S(2)}, u32[]{:S(2)}) collective-permute-start(bf16[544,128]{1,0:T(8,128)(2,1)S(1)} %get-tuple-element.107.refs_2_), channel_id=1, source_target_pairs={{32,0},{64,32},{96,64},{128,96},{160,128},{192,160},{224,192},{256... | collective-permute-start | bytes 417800 | tf_op jit(solution)/shard_map/ppermute | solution.py:346
  94.3 2.1 %collective-permute-start.3 = (bf16[544,128]{1,0:T(8,128)(2,1)S(1)}, bf16[544,128]{1,0:T(8,128)(2,1)S(1)}, u32[]{:S(2)}, u32[]{:S(2)}) collective-permute-start(bf16[544,128]{1,0:T(8,128)(2,1)S(1)} %get-tuple-element.107.refs_2_), channel_id=1, source_target_pairs={{0,32},{32,64},{64,96},{96,128},{128,160},{160,192},{192,224},{224... | collective-permute-start | bytes 417800 | tf_op jit(solution)/shard_map/ppermute | solution.py:345
  96.5 1.2 flash.9
  98.1 4.1 %collective-permute-done.3.refs_2_ = bf16[544,128]{1,0:T(8,128)(2,1)S(1)} collective-permute-done((bf16[544,128]{1,0:T(8,128)(2,1)S(1)}, bf16[544,128]{1,0:T(8,128)(2,1)S(1)}, u32[]{:S(2)}, u32[]{:S(2)}) %collective-permute-start.3) | collective-permute-done | bytes 139296 | tf_op jit(solution)/shard_map/ppermute | solution.py:345
  102.2 1.9 collective-permute-start.5
  104.1 4.6 %collective-permute-start.6 = (bf16[544,128]{1,0:T(8,128)(2,1)S(1)}, bf16[544,128]{1,0:T(8,128)(2,1)S(1)}, u32[]{:S(2)}, u32[]{:S(2)}) collective-permute-start(bf16[544,128]{1,0:T(8,128)(2,1)S(1)} %collective-permute-done.4.refs_3_), channel_id=1, source_target_pairs={{32,0},{64,32},{96,64},{128,96},{160,128},{192,160},{224,192},{256... | collective-permute-start | bytes 417800 | tf_op jit(solution)/shard_map/ppermute | solution.py:346
  108.7 2.2 %flash.10 = (f32[2,512]{1,0:T(2,128)S(1)}, f32[2,512]{1,0:T(2,128)S(1)}, f32[2,64,512]{2,1,0:T(8,128)S(1)}) custom-call(bf16[2,64,512]{2,1,0:T(8,128)(2,1)S(1)} %get-tuple-element.103.refs_0_, f32[2,512]{1,0:T(2,128)S(1)} %broadcast_in_dim.29.refs_1_, bf16[544,128]{1,0:T(8,128)(2,1)S(1)} %collective-permute-done.3.refs_2_, ...), custom_call_target="tpu_custom_call" | custom-call | flops 285212672 | bytes 1048576 | tf_op jit(solution)/shard_map/flash/pallas_call | solution.py:212
  110.9 1.9 collective-permute-start.7
  112.8 5.2 %collective-permute-start.8 = (bf16[544,128]{1,0:T(8,128)(2,1)S(1)}, bf16[544,128]{1,0:T(8,128)(2,1)S(1)}, u32[]{:S(2)}, u32[]{:S(2)}) collective-permute-start(bf16[544,128]{1,0:T(8,128)(2,1)S(1)} %collective-permute-done.6.refs_3_), channel_id=1, source_target_pairs={{32,0},{64,32},{96,64},{128,96},{160,128},{192,160},{224,192},{256... | collective-permute-start | bytes 417800 | tf_op jit(solution)/shard_map/ppermute | solution.py:346
  118.0 2.2 %flash.11 = (f32[2,512]{1,0:T(2,128)S(1)}, f32[2,512]{1,0:T(2,128)S(1)}, f32[2,64,512]{2,1,0:T(8,128)S(1)}) custom-call(bf16[2,64,512]{2,1,0:T(8,128)(2,1)S(1)} %get-tuple-element.103.refs_0_, f32[2,512]{1,0:T(2,128)S(1)} %broadcast_in_dim.29.refs_1_, bf16[544,128]{1,0:T(8,128)(2,1)S(1)} %collective-permute-done.5.refs_2_, ...), custom_call_target="tpu_custom_call" | custom-call | flops 285212672 | bytes 1048576 | tf_op jit(solution)/shard_map/flash/pallas_call | solution.py:212
  120.2 3.0 %collective-permute-start.9 = (bf16[544,128]{1,0:T(8,128)(2,1)S(1)}, bf16[544,128]{1,0:T(8,128)(2,1)S(1)}, u32[]{:S(2)}, u32[]{:S(2)}) collective-permute-start(bf16[544,128]{1,0:T(8,128)(2,1)S(1)} %collective-permute-done.7.refs_2_), channel_id=1, source_target_pairs={{0,32},{32,64},{64,96},{96,128},{128,160},{160,192},{192,224},{224... | collective-permute-start | bytes 417800 | tf_op jit(solution)/shard_map/ppermute | solution.py:345
  123.2 4.3 %collective-permute-start.10 = (bf16[544,128]{1,0:T(8,128)(2,1)S(1)}, bf16[544,128]{1,0:T(8,128)(2,1)S(1)}, u32[]{:S(2)}, u32[]{:S(2)}) collective-permute-start(bf16[544,128]{1,0:T(8,128)(2,1)S(1)} %collective-permute-done.8.refs_3_), channel_id=1, source_target_pairs={{32,0},{64,32},{96,64},{128,96},{160,128},{192,160},{224,192},{256... | collective-permute-start | bytes 417800 | tf_op jit(solution)/shard_map/ppermute | solution.py:346
  127.5 2.1 %flash.12 = (f32[2,512]{1,0:T(2,128)S(1)}, f32[2,512]{1,0:T(2,128)S(1)}, f32[2,64,512]{2,1,0:T(8,128)S(1)}) custom-call(bf16[2,64,512]{2,1,0:T(8,128)(2,1)S(1)} %get-tuple-element.103.refs_0_, f32[2,512]{1,0:T(2,128)S(1)} %broadcast_in_dim.29.refs_1_, bf16[544,128]{1,0:T(8,128)(2,1)S(1)} %collective-permute-done.7.refs_2_, ...), custom_call_target="tpu_custom_call" | custom-call | flops 285212672 | bytes 1048576 | tf_op jit(solution)/shard_map/flash/pallas_call | solution.py:212
  129.7 3.1 %collective-permute-start.11 = (bf16[544,128]{1,0:T(8,128)(2,1)S(1)}, bf16[544,128]{1,0:T(8,128)(2,1)S(1)}, u32[]{:S(2)}, u32[]{:S(2)}) collective-permute-start(bf16[544,128]{1,0:T(8,128)(2,1)S(1)} %collective-permute-done.9.refs_2_), channel_id=1, source_target_pairs={{0,32},{32,64},{64,96},{96,128},{128,160},{160,192},{192,224},{224... | collective-permute-start | bytes 417800 | tf_op jit(solution)/shard_map/ppermute | solution.py:345
  132.8 3.9 %collective-permute-start.12 = (bf16[544,128]{1,0:T(8,128)(2,1)S(1)}, bf16[544,128]{1,0:T(8,128)(2,1)S(1)}, u32[]{:S(2)}, u32[]{:S(2)}) collective-permute-start(bf16[544,128]{1,0:T(8,128)(2,1)S(1)} %collective-permute-done.10.refs_3_), channel_id=1, source_target_pairs={{32,0},{64,32},{96,64},{128,96},{160,128},{192,160},{224,192},{256... | collective-permute-start | bytes 417800 | tf_op jit(solution)/shard_map/ppermute | solution.py:346
  136.7 2.2 %flash.13 = (f32[2,512]{1,0:T(2,128)S(1)}, f32[2,512]{1,0:T(2,128)S(1)}, f32[2,64,512]{2,1,0:T(8,128)S(1)}) custom-call(bf16[2,64,512]{2,1,0:T(8,128)(2,1)S(1)} %get-tuple-element.103.refs_0_, f32[2,512]{1,0:T(2,128)S(1)} %broadcast_in_dim.29.refs_1_, bf16[544,128]{1,0:T(8,128)(2,1)S(1)} %collective-permute-done.9.refs_2_, ...), custom_call_target="tpu_custom_call" | custom-call | flops 285212672 | bytes 1048576 | tf_op jit(solution)/shard_map/flash/pallas_call | solution.py:212
  138.9 3.1 %collective-permute-start.13 = (bf16[544,128]{1,0:T(8,128)(2,1)S(1)}, bf16[544,128]{1,0:T(8,128)(2,1)S(1)}, u32[]{:S(2)}, u32[]{:S(2)}) collective-permute-start(bf16[544,128]{1,0:T(8,128)(2,1)S(1)} %collective-permute-done.11.refs_2_), channel_id=1, source_target_pairs={{0,32},{32,64},{64,96},{96,128},{128,160},{160,192},{192,224},{224... | collective-permute-start | bytes 417800 | tf_op jit(solution)/shard_map/ppermute | solution.py:345
  142.0 3.6 %collective-permute-start.14 = (bf16[544,128]{1,0:T(8,128)(2,1)S(1)}, bf16[544,128]{1,0:T(8,128)(2,1)S(1)}, u32[]{:S(2)}, u32[]{:S(2)}) collective-permute-start(bf16[544,128]{1,0:T(8,128)(2,1)S(1)} %collective-permute-done.12.refs_3_), channel_id=1, source_target_pairs={{32,0},{64,32},{96,64},{128,96},{160,128},{192,160},{224,192},{256... | collective-permute-start | bytes 417800 | tf_op jit(solution)/shard_map/ppermute | solution.py:346
  145.6 2.2 %flash.14 = (f32[2,512]{1,0:T(2,128)S(1)}, f32[2,512]{1,0:T(2,128)S(1)}, f32[2,64,512]{2,1,0:T(8,128)S(1)}) custom-call(bf16[2,64,512]{2,1,0:T(8,128)(2,1)S(1)} %get-tuple-element.103.refs_0_, f32[2,512]{1,0:T(2,128)S(1)} %broadcast_in_dim.29.refs_1_, bf16[544,128]{1,0:T(8,128)(2,1)S(1)} %collective-permute-done.11.refs_2_, ...), custom_call_target="tpu_custom_call" | custom-call | flops 285212672 | bytes 1048576 | tf_op jit(solution)/shard_map/flash/pallas_call | solution.py:212
  147.8 3.1 %collective-permute-start.15 = (bf16[544,128]{1,0:T(8,128)(2,1)S(1)}, bf16[544,128]{1,0:T(8,128)(2,1)S(1)}, u32[]{:S(2)}, u32[]{:S(2)}) collective-permute-start(bf16[544,128]{1,0:T(8,128)(2,1)S(1)} %collective-permute-done.13.refs_2_), channel_id=1, source_target_pairs={{0,32},{32,64},{64,96},{96,128},{128,160},{160,192},{192,224},{224... | collective-permute-start | bytes 417800 | tf_op jit(solution)/shard_map/ppermute | solution.py:345
  150.9 3.6 %collective-permute-start.16 = (bf16[544,128]{1,0:T(8,128)(2,1)S(1)}, bf16[544,128]{1,0:T(8,128)(2,1)S(1)}, u32[]{:S(2)}, u32[]{:S(2)}) collective-permute-start(bf16[544,128]{1,0:T(8,128)(2,1)S(1)} %collective-permute-done.14.refs_3_), channel_id=1, source_target_pairs={{32,0},{64,32},{96,64},{128,96},{160,128},{192,160},{224,192},{256... | collective-permute-start | bytes 417800 | tf_op jit(solution)/shard_map/ppermute | solution.py:346
  154.5 2.2 %flash.15 = (f32[2,512]{1,0:T(2,128)S(1)}, f32[2,512]{1,0:T(2,128)S(1)}, f32[2,64,512]{2,1,0:T(8,128)S(1)}) custom-call(bf16[2,64,512]{2,1,0:T(8,128)(2,1)S(1)} %get-tuple-element.103.refs_0_, f32[2,512]{1,0:T(2,128)S(1)} %broadcast_in_dim.29.refs_1_, bf16[544,128]{1,0:T(8,128)(2,1)S(1)} %collective-permute-done.13.refs_2_, ...), custom_call_target="tpu_custom_call" | custom-call | flops 285212672 | bytes 1048576 | tf_op jit(solution)/shard_map/flash/pallas_call | solution.py:212
  156.7 3.2 %collective-permute-start.17 = (bf16[544,128]{1,0:T(8,128)(2,1)S(1)}, bf16[544,128]{1,0:T(8,128)(2,1)S(1)}, u32[]{:S(2)}, u32[]{:S(2)}) collective-permute-start(bf16[544,128]{1,0:T(8,128)(2,1)S(1)} %collective-permute-done.15.refs_2_), channel_id=1, source_target_pairs={{0,32},{32,64},{64,96},{96,128},{128,160},{160,192},{192,224},{224... | collective-permute-start | bytes 417800 | tf_op jit(solution)/shard_map/ppermute | solution.py:345
  160.0 2.2 %flash.16 = (f32[2,512]{1,0:T(2,128)S(1)}, f32[2,512]{1,0:T(2,128)S(1)}, f32[2,64,512]{2,1,0:T(8,128)S(1)}) custom-call(bf16[2,64,512]{2,1,0:T(8,128)(2,1)S(1)} %get-tuple-element.103.refs_0_, f32[2,512]{1,0:T(2,128)S(1)} %broadcast_in_dim.29.refs_1_, bf16[544,128]{1,0:T(8,128)(2,1)S(1)} %collective-permute-done.15.refs_2_, ...), custom_call_target="tpu_custom_call" | custom-call | flops 285212672 | bytes 1048576 | tf_op jit(solution)/shard_map/flash/pallas_call | solution.py:212
  162.1 1.8 collective-permute-done.17.refs_2_
  164.0 1.4 flash.17
  165.3 9.1 %all_to_all.25.a_ref = bf16[4,128,128]{2,1,0:T(8,128)(2,1)S(1)} all-to-all(bf16[4,128,128]{2,1,0:T(8,128)(2,1)S(1)} %flash.17), channel_id=1, replica_groups={{0,8,16,24},{1,9,17,25},{2,10,18,26},{3,11,19,27},{4,12,20,28},{5,13,21..., dimensions={0} | all-to-all | bytes 262144 | tf_op jit(solution)/shard_map/all_to_all | solution.py:357
  174.4 2.9 %out_partial.1 = (bf16[64,4096]{1,0:T(8,128)(2,1)S(1)}, bf16[64,4096]{1,0:T(8,128)(2,1)S(1)}) custom-call(s32[1]{0:T(128)} %bitcast.9.core_ref, bf16[4,128,128]{2,1,0:T(8,128)(2,1)S(1)} %all_to_all.25.a_ref, bf16[4,8,4,128,128]{4,3,2,1,0:T(8,128)(2,1)} %bitcast.15.w_ref), custom_call_target="tpu_custom_call" | custom-call | flops 536870912 | bytes 4194304 | tf_op jit(solution)/shard_map/out_partial/pallas_call | solution.py:251
  177.4 11.6 %collective-permute-start.18 = (bf16[64,4096]{1,0:T(8,128)(2,1)S(1)}, bf16[64,4096]{1,0:T(8,128)(2,1)S(1)}, u32[]{:S(2)}, u32[]{:S(2)}) collective-permute-start(bf16[64,4096]{1,0:T(8,128)(2,1)S(1)} %get-tuple-element.174), channel_id=1, source_target_pairs={{0,1},{1,0},{2,3},{3,2},{4,5},{5,4},{6,7},{7,6},{8,9},{9,8},{10,11... | collective-permute-start | bytes 1572872 | tf_op jit(solution)/shard_map/ppermute | solution.py:359
  189.0 1.5 collective-permute-done.18
  191.5 4.0 %all-to-all-start.4 = ((bf16[4,16,4096]{2,1,0:T(8,128)(2,1)}), bf16[4,16,4096]{2,1,0:T(8,128)(2,1)S(1)}, u32[]{:S(2)}, u32[]{:S(2)}) async-start(bf16[4,16,4096]{2,1,0:T(8,128)(2,1)} %bitcast.16), calls=%async_computation.4 | async-start | bytes 1048576 | tf_op jit(solution)/shard_map/all_to_all | solution.py:361
  196.2 8.1 %all-to-all-done.4 = bf16[4,16,4096]{2,1,0:T(8,128)(2,1)S(1)} async-done(((bf16[4,16,4096]{2,1,0:T(8,128)(2,1)}), bf16[4,16,4096]{2,1,0:T(8,128)(2,1)S(1)}, u32[]{:S(2)}, u32[]{:S(2)}) %all-to-all-start.4) | async-done | bytes 524320 | tf_op jit(solution)/shard_map/all_to_all | solution.py:361
  (65 shorter events, 11.7 us)
Async XLA Ops:
  0.0 13.7 %copy-start = (bf16[256,384]{1,0:T(8,128)(2,1)S(1)}, bf16[256,384]{1,0:T(8,128)(2,1)}, u32[]{:S(2)}) copy-start(bf16[256,384]{1,0:T(8,128)(2,1)} %param.18) | copy-start | bytes 589828
  2.5 7.7 %copy-start.11 = (f32[64]{0:T(128)S(1)}, f32[64]{0:T(128)}, u32[]{:S(2)}) copy-start(f32[64]{0:T(128)} %param.24) | copy-start | bytes 772
  2.5 7.8 %copy-start.10 = (f32[2]{0:T(128)S(1)}, f32[2]{0:T(128)}, u32[]{:S(2)}) copy-start(f32[2]{0:T(128)} %constant.91.clone) | copy-start | bytes 28
  2.5 11.1 %copy-start.9 = (f32[256]{0:T(256)S(1)}, f32[256]{0:T(256)}, u32[]{:S(2)}) copy-start(f32[256]{0:T(256)} %param.17) | copy-start | bytes 3076
  2.5 41.2 %all-to-all-start = ((bf16[16,16,4096]{2,1,0:T(8,128)(2,1)}), bf16[16,16,4096]{2,1,0:T(8,128)(2,1)S(1)}, u32[]{:S(2)}, u32[]{:S(2)}) async-start(bf16[16,16,4096]{2,1,0:T(8,128)(2,1)} %broadcast_in_dim.12), calls=%async_computation | async-start | bytes 4194304 | tf_op jit(solution)/shard_map/all_to_all | solution.py:290
  10.3 43.2 %copy-start.1 = (bf16[4096,128]{1,0:T(8,128)(2,1)S(1)}, bf16[4096,128]{1,0:T(8,128)(2,1)}, u32[]{:S(2)}) copy-start(bf16[4096,128]{1,0:T(8,128)(2,1)} %wq_ref) | copy-start | bytes 3145732
  12.0 60.2 %copy-start.6 = (f32[64]{0:T(128)S(1)}, f32[64]{0:T(128)}, u32[]{:S(2)}) copy-start(f32[64]{0:T(128)} %param.25) | copy-start | bytes 772
  45.2 26.2 %copy-start.8 = (f32[4096]{0:T(1024)S(1)}, f32[4096]{0:T(1024)}, u32[]{:S(2)}) copy-start(f32[4096]{0:T(1024)} %param.19) | copy-start | bytes 49156
  47.5 24.7 %collective-permute-start.1 = (bf16[128,4096]{1,0:T(8,128)(2,1)}, bf16[128,4096]{1,0:T(8,128)(2,1)}, u32[]{:S(2)}, u32[]{:S(2)}) collective-permute-start(bf16[128,4096]{1,0:T(8,128)(2,1)} %pad_maximum_fusion.wkv_ref), channel_id=1, source_target_pairs={{0,1},{1,0},{2,3},{3,2},{4,5},{5,4},{6,7},{7,6},{8,9},{9,8},{10,11... | collective-permute-start | bytes 3145736 | tf_op jit(solution)/shard_map/ppermute | solution.py:323
  53.5 18.7 %collective-permute-start = (bf16[4096,128]{1,0:T(8,128)(2,1)S(1)}, bf16[4096,128]{1,0:T(8,128)(2,1)}, u32[]{:S(2)}, u32[]{:S(2)}) collective-permute-start(bf16[4096,128]{1,0:T(8,128)(2,1)S(1)} %copy-done.1), channel_id=1, source_target_pairs={{0,1},{1,0},{2,3},{3,2},{4,5},{5,4},{6,7},{7,6},{8,9},{9,8},{10,11... | collective-permute-start | bytes 3145736 | tf_op jit(solution)/shard_map/ppermute | solution.py:322
  56.1 15.3 %all-to-all-start.1 = ((f32[32,2,384]{2,1,0:T(2,128)}), f32[32,2,384]{2,1,0:T(2,128)}, u32[]{:S(2)}, u32[]{:S(2)}) async-start(f32[32,2,384]{2,1,0:T(2,128)} %broadcast_in_dim.31), calls=%async_computation.1 | async-start | bytes 196608 | tf_op jit(solution)/shard_map/all_to_all | solution.py:328
  72.2 0.9 copy-start.2
  73.1 0.9 copy-start.3
  80.0 0.6 copy-start.4
  80.6 5.7 %collective-permute-start.2 = (bf16[256,256]{1,0:T(8,128)(2,1)}, bf16[256,256]{1,0:T(8,128)(2,1)S(1)}, u32[]{:S(2)}, u32[]{:S(2)}) collective-permute-start(bf16[256,256]{1,0:T(8,128)(2,1)} %get-tuple-element.101), channel_id=1, source_target_pairs={{0,1},{1,0},{2,3},{3,2},{4,5},{5,4},{6,7},{7,6},{8,9},{9,8},{10,11... | collective-permute-start | bytes 393224 | tf_op jit(solution)/shard_map/ppermute | solution.py:334
  82.9 3.4 %copy-start.5 = (bf16[256,256]{1,0:T(8,128)(2,1)S(1)}, bf16[256,256]{1,0:T(8,128)(2,1)}, u32[]{:S(2)}) copy-start(bf16[256,256]{1,0:T(8,128)(2,1)} %copy-done.4) | copy-start | bytes 393220
  86.5 70.2 %all-to-all-start.2 = ((bf16[32,4,128,128]{3,2,1,0:T(8,128)(2,1)}), bf16[32,4,128,128]{3,2,1,0:T(8,128)(2,1)}, u32[]{:S(2)}, u32[]{:S(2)}) async-start(bf16[32,4,128,128]{3,2,1,0:T(8,128)(2,1)} %bitcast.24), calls=%async_computation.2 | async-start | bytes 8388608 | tf_op jit(solution)/shard_map/all_to_all | solution.py:337
  91.2 6.9 %collective-permute-start.4 = (bf16[544,128]{1,0:T(8,128)(2,1)S(1)}, bf16[544,128]{1,0:T(8,128)(2,1)S(1)}, u32[]{:S(2)}, u32[]{:S(2)}) collective-permute-start(bf16[544,128]{1,0:T(8,128)(2,1)S(1)} %get-tuple-element.107.refs_2_), channel_id=1, source_target_pairs={{32,0},{64,32},{96,64},{128,96},{160,128},{192,160},{224,192},{256... | collective-permute-start | bytes 417800 | tf_op jit(solution)/shard_map/ppermute | solution.py:346
  94.3 7.8 %collective-permute-start.3 = (bf16[544,128]{1,0:T(8,128)(2,1)S(1)}, bf16[544,128]{1,0:T(8,128)(2,1)S(1)}, u32[]{:S(2)}, u32[]{:S(2)}) collective-permute-start(bf16[544,128]{1,0:T(8,128)(2,1)S(1)} %get-tuple-element.107.refs_2_), channel_id=1, source_target_pairs={{0,32},{32,64},{64,96},{96,128},{128,160},{160,192},{192,224},{224... | collective-permute-start | bytes 417800 | tf_op jit(solution)/shard_map/ppermute | solution.py:345
  102.2 8.7 %collective-permute-start.5 = (bf16[544,128]{1,0:T(8,128)(2,1)S(1)}, bf16[544,128]{1,0:T(8,128)(2,1)S(1)}, u32[]{:S(2)}, u32[]{:S(2)}) collective-permute-start(bf16[544,128]{1,0:T(8,128)(2,1)S(1)} %collective-permute-done.3.refs_2_), channel_id=1, source_target_pairs={{0,32},{32,64},{64,96},{96,128},{128,160},{160,192},{192,224},{224... | collective-permute-start | bytes 417800 | tf_op jit(solution)/shard_map/ppermute | solution.py:345
  104.1 6.8 %collective-permute-start.6 = (bf16[544,128]{1,0:T(8,128)(2,1)S(1)}, bf16[544,128]{1,0:T(8,128)(2,1)S(1)}, u32[]{:S(2)}, u32[]{:S(2)}) collective-permute-start(bf16[544,128]{1,0:T(8,128)(2,1)S(1)} %collective-permute-done.4.refs_3_), channel_id=1, source_target_pairs={{32,0},{64,32},{96,64},{128,96},{160,128},{192,160},{224,192},{256... | collective-permute-start | bytes 417800 | tf_op jit(solution)/shard_map/ppermute | solution.py:346
  110.9 9.3 %collective-permute-start.7 = (bf16[544,128]{1,0:T(8,128)(2,1)S(1)}, bf16[544,128]{1,0:T(8,128)(2,1)S(1)}, u32[]{:S(2)}, u32[]{:S(2)}) collective-permute-start(bf16[544,128]{1,0:T(8,128)(2,1)S(1)} %collective-permute-done.5.refs_2_), channel_id=1, source_target_pairs={{0,32},{32,64},{64,96},{96,128},{128,160},{160,192},{192,224},{224... | collective-permute-start | bytes 417800 | tf_op jit(solution)/shard_map/ppermute | solution.py:345
  112.8 7.4 %collective-permute-start.8 = (bf16[544,128]{1,0:T(8,128)(2,1)S(1)}, bf16[544,128]{1,0:T(8,128)(2,1)S(1)}, u32[]{:S(2)}, u32[]{:S(2)}) collective-permute-start(bf16[544,128]{1,0:T(8,128)(2,1)S(1)} %collective-permute-done.6.refs_3_), channel_id=1, source_target_pairs={{32,0},{64,32},{96,64},{128,96},{160,128},{192,160},{224,192},{256... | collective-permute-start | bytes 417800 | tf_op jit(solution)/shard_map/ppermute | solution.py:346
  120.2 9.5 %collective-permute-start.9 = (bf16[544,128]{1,0:T(8,128)(2,1)S(1)}, bf16[544,128]{1,0:T(8,128)(2,1)S(1)}, u32[]{:S(2)}, u32[]{:S(2)}) collective-permute-start(bf16[544,128]{1,0:T(8,128)(2,1)S(1)} %collective-permute-done.7.refs_2_), channel_id=1, source_target_pairs={{0,32},{32,64},{64,96},{96,128},{128,160},{160,192},{192,224},{224... | collective-permute-start | bytes 417800 | tf_op jit(solution)/shard_map/ppermute | solution.py:345
  123.2 6.5 %collective-permute-start.10 = (bf16[544,128]{1,0:T(8,128)(2,1)S(1)}, bf16[544,128]{1,0:T(8,128)(2,1)S(1)}, u32[]{:S(2)}, u32[]{:S(2)}) collective-permute-start(bf16[544,128]{1,0:T(8,128)(2,1)S(1)} %collective-permute-done.8.refs_3_), channel_id=1, source_target_pairs={{32,0},{64,32},{96,64},{128,96},{160,128},{192,160},{224,192},{256... | collective-permute-start | bytes 417800 | tf_op jit(solution)/shard_map/ppermute | solution.py:346
  129.7 9.2 %collective-permute-start.11 = (bf16[544,128]{1,0:T(8,128)(2,1)S(1)}, bf16[544,128]{1,0:T(8,128)(2,1)S(1)}, u32[]{:S(2)}, u32[]{:S(2)}) collective-permute-start(bf16[544,128]{1,0:T(8,128)(2,1)S(1)} %collective-permute-done.9.refs_2_), channel_id=1, source_target_pairs={{0,32},{32,64},{64,96},{96,128},{128,160},{160,192},{192,224},{224... | collective-permute-start | bytes 417800 | tf_op jit(solution)/shard_map/ppermute | solution.py:345
  132.8 6.1 %collective-permute-start.12 = (bf16[544,128]{1,0:T(8,128)(2,1)S(1)}, bf16[544,128]{1,0:T(8,128)(2,1)S(1)}, u32[]{:S(2)}, u32[]{:S(2)}) collective-permute-start(bf16[544,128]{1,0:T(8,128)(2,1)S(1)} %collective-permute-done.10.refs_3_), channel_id=1, source_target_pairs={{32,0},{64,32},{96,64},{128,96},{160,128},{192,160},{224,192},{256... | collective-permute-start | bytes 417800 | tf_op jit(solution)/shard_map/ppermute | solution.py:346
  138.9 8.9 %collective-permute-start.13 = (bf16[544,128]{1,0:T(8,128)(2,1)S(1)}, bf16[544,128]{1,0:T(8,128)(2,1)S(1)}, u32[]{:S(2)}, u32[]{:S(2)}) collective-permute-start(bf16[544,128]{1,0:T(8,128)(2,1)S(1)} %collective-permute-done.11.refs_2_), channel_id=1, source_target_pairs={{0,32},{32,64},{64,96},{96,128},{128,160},{160,192},{192,224},{224... | collective-permute-start | bytes 417800 | tf_op jit(solution)/shard_map/ppermute | solution.py:345
  142.0 5.8 %collective-permute-start.14 = (bf16[544,128]{1,0:T(8,128)(2,1)S(1)}, bf16[544,128]{1,0:T(8,128)(2,1)S(1)}, u32[]{:S(2)}, u32[]{:S(2)}) collective-permute-start(bf16[544,128]{1,0:T(8,128)(2,1)S(1)} %collective-permute-done.12.refs_3_), channel_id=1, source_target_pairs={{32,0},{64,32},{96,64},{128,96},{160,128},{192,160},{224,192},{256... | collective-permute-start | bytes 417800 | tf_op jit(solution)/shard_map/ppermute | solution.py:346
  147.8 8.9 %collective-permute-start.15 = (bf16[544,128]{1,0:T(8,128)(2,1)S(1)}, bf16[544,128]{1,0:T(8,128)(2,1)S(1)}, u32[]{:S(2)}, u32[]{:S(2)}) collective-permute-start(bf16[544,128]{1,0:T(8,128)(2,1)S(1)} %collective-permute-done.13.refs_2_), channel_id=1, source_target_pairs={{0,32},{32,64},{64,96},{96,128},{128,160},{160,192},{192,224},{224... | collective-permute-start | bytes 417800 | tf_op jit(solution)/shard_map/ppermute | solution.py:345
  150.9 5.8 %collective-permute-start.16 = (bf16[544,128]{1,0:T(8,128)(2,1)S(1)}, bf16[544,128]{1,0:T(8,128)(2,1)S(1)}, u32[]{:S(2)}, u32[]{:S(2)}) collective-permute-start(bf16[544,128]{1,0:T(8,128)(2,1)S(1)} %collective-permute-done.14.refs_3_), channel_id=1, source_target_pairs={{32,0},{64,32},{96,64},{128,96},{160,128},{192,160},{224,192},{256... | collective-permute-start | bytes 417800 | tf_op jit(solution)/shard_map/ppermute | solution.py:346
  156.7 7.2 %collective-permute-start.17 = (bf16[544,128]{1,0:T(8,128)(2,1)S(1)}, bf16[544,128]{1,0:T(8,128)(2,1)S(1)}, u32[]{:S(2)}, u32[]{:S(2)}) collective-permute-start(bf16[544,128]{1,0:T(8,128)(2,1)S(1)} %collective-permute-done.15.refs_2_), channel_id=1, source_target_pairs={{0,32},{32,64},{64,96},{96,128},{128,160},{160,192},{192,224},{224... | collective-permute-start | bytes 417800 | tf_op jit(solution)/shard_map/ppermute | solution.py:345
  177.4 27.1 %copy-start.7 = (bf16[16,4096]{1,0:T(8,128)(2,1)S(1)}, bf16[16,4096]{1,0:T(8,128)(2,1)}, u32[]{:S(2)}) copy-start(bf16[16,4096]{1,0:T(8,128)(2,1)} %param.14) | copy-start | bytes 393220
  177.4 13.2 %collective-permute-start.18 = (bf16[64,4096]{1,0:T(8,128)(2,1)S(1)}, bf16[64,4096]{1,0:T(8,128)(2,1)S(1)}, u32[]{:S(2)}, u32[]{:S(2)}) collective-permute-start(bf16[64,4096]{1,0:T(8,128)(2,1)S(1)} %get-tuple-element.174), channel_id=1, source_target_pairs={{0,1},{1,0},{2,3},{3,2},{4,5},{5,4},{6,7},{7,6},{8,9},{9,8},{10,11... | collective-permute-start | bytes 1572872 | tf_op jit(solution)/shard_map/ppermute | solution.py:359
  191.5 12.9 %all-to-all-start.4 = ((bf16[4,16,4096]{2,1,0:T(8,128)(2,1)}), bf16[4,16,4096]{2,1,0:T(8,128)(2,1)S(1)}, u32[]{:S(2)}, u32[]{:S(2)}) async-start(bf16[4,16,4096]{2,1,0:T(8,128)(2,1)} %bitcast.16), calls=%async_computation.4 | async-start | bytes 1048576 | tf_op jit(solution)/shard_map/all_to_all | solution.py:361

commit v3 on v2

--- a/solution.py
+++ b/solution.py
@@ -52,6 +52,26 @@
         cost_estimate=pl.CostEstimate(flops=0, bytes_accessed=10 * w.size, transcendentals=0),
         name="spread",
     )(w)
+
+
+def repeat_body(x_ref, o_ref, sems):
+    copies = [pltpu.make_async_copy(x_ref, o_ref.at[i], sems.at[i]) for i in range(o_ref.shape[0])]
+    for copy in copies:
+        copy.start()
+    for copy in copies:
+        copy.wait()
+
+
+def repeated(x, count):
+    return pl.pallas_call(
+        repeat_body,
+        in_specs=[VMEM],
+        out_specs=pl.BlockSpec(memory_space=pl.ANY),
+        out_shape=jax.ShapeDtypeStruct((count, *x.shape), x.dtype),
+        scratch_shapes=[pltpu.SemaphoreType.DMA((count,))],
+        cost_estimate=pl.CostEstimate(flops=0, bytes_accessed=2 * (count + 1) * x.size, transcendentals=0),
+        name="repeated",
+    )(x)
 
 
 def qkv_body(hs, lat_ref, ctx_ref, gain_ref, shift_ref, wq_ref, wkv_ref, wq2_ref, wkv2_ref, qg_ref, kg_ref, cos_ref, sin_ref, own_ref, other_ref, ctx_kv_ref):
@@ -105,7 +125,7 @@
         ),
         compiler_params=pltpu.CompilerParams(vmem_limit_bytes=24 << 20),
         name="qkv",
-    )(*near(*args))
+    )(*[near(a)[0] if a.size >= 1 << 19 else a for a in args])
 
 
 def assemble_body(core_ref, own_ref, got_ref, ctx_ref, qt_ref, kv_ref):
@@ -286,7 +306,7 @@
     core = tp % 2
     block_rows = own_rows * n_tp
 
-    lat_copies = jnp.broadcast_to(latent, (n_tp // 2, own_rows, width))
+    lat_copies = repeated(latent, n_tp // 2)
     lat_half = lax.all_to_all(lat_copies, "tp", 0, 0, axis_index_groups=group_core, tiled=True)
     lat_half = lat_half.reshape(block_rows // 2, width)
 
@@ -333,8 +353,6 @@
     own, other, ctx_kv = qkv(lat_half, context, gain, shift, wq, wkv, wq2, wkv2, q_gain, k_gain, cos, sin)
     got = lax.ppermute(other, "tp", swap)
     qt, kv = assemble(core.reshape(1).astype(jnp.int32), own, got, ctx_kv)
-    kv, w_split = lax.optimization_barrier((kv, w_split))
-    w_rows = lax.all_to_all(w_split, "tp", 0, 0, tiled=True)
 
     up = [(i, (i + 1) % n_sp) for i in range(n_sp)]
     down = [(d, s) for s, d in up]
@@ -345,6 +363,9 @@
         nxt_f = lax.ppermute(fwd, "sp", up)
         nxt_b = lax.ppermute(bwd, "sp", down) if step < n_sp // 2 else None
         state = flash(qt, lift, blocks, state, block_rows, False)
+        if step == 1:
+            state, w_split = lax.optimization_barrier((state, w_split))
+            w_rows = lax.all_to_all(w_split, "tp", 0, 0, tiled=True)
         if step == 7:
             nxt_f, nxt_b, state, w_rows = lax.optimization_barrier((nxt_f, nxt_b, state, w_rows))
         else:

time: 207 us -> 208 us (level)
  local copies, waits for them, and re-layouts: 12 us -> 9.48 us
  Pallas kernels: 30 us -> 32.5 us
    broadcast_in_dim x1 -> x0, local copies, waits for them, and re-layouts: 2.53 us -> none  [local(): lat_copies = jnp.broadcast_to(latent, (n_tp // 2, own_rows, width))]
    pallas_call x0 -> x1, Pallas kernels: none -> 2.44 us  [repeated(): pl.pallas_call(repeat_body, in_specs=[VMEM], out_specs=pl.BlockSpec(memor...]
  transfers between devices with their start and end apart: 23 -> 23, of which waited for: 6 -> 6; matrix products, arithmetic and copies ran while one was open for 4% -> 4% of each run, Pallas kernels for 10% -> 9%
where the time goes in v3:
time: 208 us; the launch traced here: 206 us
  starting transfers between devices  95.9 us (46%)
  blocking collectives  37.4 us (18%)
  Pallas kernels  32.5 us (16%)
  waiting for transfers between devices  23.1 us (11%)
  local copies, waits for them, and re-layouts  9.48 us (5%)
  other arithmetic  6.55 us (3%)
    ppermute x7, starting transfers between devices, local(): nxt_b = lax.ppermute(bwd, 'sp', down) if step < n_sp // 2 else None  28.3 us
    ppermute x8, starting transfers between devices, local(): nxt_f = lax.ppermute(fwd, 'sp', up)  21.5 us
    pallas_call x9, Pallas kernels, flash(): pl.pallas_call(functools.partial(flash_body, len(blocks), first, last, la...  17.6 us
    psum x1, blocking collectives, local(): lax.psum(lax.psum(partial_mod, 'sp', axis_index_groups=near_z), 'sp', axi...  16.8 us
    ppermute x1, starting transfers between devices, local(): lax.ppermute(send, 'tp', swap).astype(jnp.float32)  11.7 us
    psum x1, blocking collectives, local(): lax.psum(partial_mod, 'sp', axis_index_groups=near_z)  11.5 us
    all_to_all x1, blocking collectives, local(): lax.all_to_all(attended, 'tp', 0, 0, axis_index_groups=group_y, tiled=True)  9.08 us
    all_to_all x1, waiting for transfers between devices, local(): lax.all_to_all(part, 'tp', 0, 0, axis_index_groups=group_x, tiled=True)  8.15 us
  transfers between devices with their start and end apart: 23, of which 6 were waited for; matrix products, arithmetic and copies ran while one was open for 4% of the time, Pallas kernels for 9%

profile of v3, /device:TPU:1, one launch (start us, length us, event | category | flops | bytes accessed | tf_op | source)
XLA Modules:
  0.0 206.3 jit_solution(18078481901626258517)
XLA Ops:
  0.0 2.4 %repeated.1 = bf16[16,16,4096]{2,1,0:T(8,128)(2,1)} custom-call(bf16[16,4096]{1,0:T(8,128)(2,1)} %x_ref.1), custom_call_target="tpu_custom_call" | custom-call | bytes 2228224 | tf_op jit(solution)/shard_map/repeated/pallas_call | solution.py:66
  2.5 7.7 %all-to-all-start = ((bf16[16,16,4096]{2,1,0:T(8,128)(2,1)}), bf16[16,16,4096]{2,1,0:T(8,128)(2,1)S(1)}, u32[]{:S(2)}, u32[]{:S(2)}) async-start(bf16[16,16,4096]{2,1,0:T(8,128)(2,1)} %repeated.1), calls=%async_computation | async-start | bytes 4194304 | tf_op jit(solution)/shard_map/all_to_all | solution.py:310
  14.5 11.5 %psum.14 = f32[2,384]{1,0:T(2,128)S(1)} all-reduce(f32[2,384]{1,0:T(2,128)S(1)} %fusion.6), channel_id=1, replica_groups={{0,32,64,96},{128,160,192,224},{256,288,320,352},{384,416,448,480},{1,3..., use_global_device_ids=true, to_apply=%region_0.1 | all-reduce | flops 768 | bytes 6144 | tf_op jit(solution)/shard_map/psum | solution.py:333
  26.0 16.8 %psum.15 = f32[2,384]{1,0:T(2,128)S(1)} all-reduce(f32[2,384]{1,0:T(2,128)S(1)} %psum.14), channel_id=1, replica_groups={{0,128,256,384},{32,160,288,416},{64,192,320,448},{96,224,352,480},{1,1..., use_global_device_ids=true, to_apply=%region_1.2 | all-reduce | flops 768 | bytes 6144 | tf_op jit(solution)/shard_map/psum | solution.py:333
  45.1 2.3 %pad_maximum_fusion.wkv_ref = bf16[128,4096]{1,0:T(8,128)(2,1)} fusion(bf16[64,4096]{1,0:T(8,128)(2,1)} %bitcast.28, bf16[64,4096]{1,0:T(8,128)(2,1)} %bitcast.29), kind=kLoop, calls=%fused_computation | loop fusion | flops 2097152 | bytes 2097152 | tf_op jit(solution)/shard_map/concatenate | solution.py:341
  47.4 6.0 %collective-permute-start.1 = (bf16[128,4096]{1,0:T(8,128)(2,1)}, bf16[128,4096]{1,0:T(8,128)(2,1)}, u32[]{:S(2)}, u32[]{:S(2)}) collective-permute-start(bf16[128,4096]{1,0:T(8,128)(2,1)} %pad_maximum_fusion.wkv_ref), channel_id=1, source_target_pairs={{0,1},{1,0},{2,3},{3,2},{4,5},{5,4},{6,7},{7,6},{8,9},{9,8},{10,11... | collective-permute-start | bytes 3145736 | tf_op jit(solution)/shard_map/ppermute | solution.py:343
  53.5 1.9 collective-permute-start
  56.1 7.8 %all-to-all-start.1 = ((f32[32,2,384]{2,1,0:T(2,128)}), f32[32,2,384]{2,1,0:T(2,128)}, u32[]{:S(2)}, u32[]{:S(2)}) async-start(f32[32,2,384]{2,1,0:T(2,128)} %broadcast_in_dim.27), calls=%async_computation.1 | async-start | bytes 196608 | tf_op jit(solution)/shard_map/all_to_all | solution.py:348
  63.9 1.6 copy.18.cos_ref
  65.5 5.8 %all-to-all-done.1 = f32[32,2,384]{2,1,0:T(2,128)} async-done(((f32[32,2,384]{2,1,0:T(2,128)}), f32[32,2,384]{2,1,0:T(2,128)}, u32[]{:S(2)}, u32[]{:S(2)}) %all-to-all-start.1) | async-done | bytes 98336 | tf_op jit(solution)/shard_map/all_to_all | solution.py:348
  73.1 0.9 copy-done.3
  74.0 5.9 %qkv.1 = (bf16[256,256]{1,0:T(8,128)(2,1)S(1)}, bf16[256,256]{1,0:T(8,128)(2,1)}, bf16[32,128]{1,0:T(8,128)(2,1)S(1)}) custom-call(bf16[256,4096]{1,0:T(8,128)(2,1)S(1)} %bitcast.22, bf16[32,4096]{1,0:T(8,128)(2,1)S(1)} %copy-done.3, f32[2,4096]{1,0:T(2,128)S(1)} %get-tuple-element.180.gain_ref, f32[2,4096]{1,0:T(2,128)S(1)} %get-tuple-element.179.shift_ref, ...), custom_call_target="tpu_custom_call" | custom-call | flops 1073741824 | bytes 6291456 | tf_op jit(solution)/shard_map/qkv/pallas_call | solution.py:114
  80.6 2.3 %collective-permute-start.2 = (bf16[256,256]{1,0:T(8,128)(2,1)}, bf16[256,256]{1,0:T(8,128)(2,1)S(1)}, u32[]{:S(2)}, u32[]{:S(2)}) collective-permute-start(bf16[256,256]{1,0:T(8,128)(2,1)} %get-tuple-element.103), channel_id=1, source_target_pairs={{0,1},{1,0},{2,3},{3,2},{4,5},{5,4},{6,7},{7,6},{8,9},{9,8},{10,11... | collective-permute-start | bytes 393224 | tf_op jit(solution)/shard_map/ppermute | solution.py:354
  82.9 3.4 %spread.1 = bf16[4,8,4,128,128]{4,3,2,1,0:T(8,128)(2,1)} custom-call(bf16[4,8,128,128]{3,2,1,0:T(8,128)(2,1)} %bitcast.25), custom_call_target="tpu_custom_call" | custom-call | bytes 5242880 | tf_op jit(solution)/shard_map/spread/pallas_call | solution.py:46
  86.4 1.2 flash.9
  87.6 4.7 %all-to-all-start.2 = ((bf16[32,4,128,128]{3,2,1,0:T(8,128)(2,1)}), bf16[32,4,128,128]{3,2,1,0:T(8,128)(2,1)}, u32[]{:S(2)}, u32[]{:S(2)}) async-start(bf16[32,4,128,128]{3,2,1,0:T(8,128)(2,1)} %bitcast.24), calls=%async_computation.2 | async-start | bytes 8388608 | tf_op jit(solution)/shard_map/all_to_all | solution.py:368
  92.3 3.2 %collective-permute-start.4 = (bf16[544,128]{1,0:T(8,128)(2,1)S(1)}, bf16[544,128]{1,0:T(8,128)(2,1)S(1)}, u32[]{:S(2)}, u32[]{:S(2)}) collective-permute-start(bf16[544,128]{1,0:T(8,128)(2,1)S(1)} %get-tuple-element.107.refs_2_), channel_id=1, source_target_pairs={{32,0},{64,32},{96,64},{128,96},{160,128},{192,160},{224,192},{256... | collective-permute-start | bytes 417800 | tf_op jit(solution)/shard_map/ppermute | solution.py:364
  95.5 2.1 %collective-permute-start.3 = (bf16[544,128]{1,0:T(8,128)(2,1)S(1)}, bf16[544,128]{1,0:T(8,128)(2,1)S(1)}, u32[]{:S(2)}, u32[]{:S(2)}) collective-permute-start(bf16[544,128]{1,0:T(8,128)(2,1)S(1)} %get-tuple-element.107.refs_2_), channel_id=1, source_target_pairs={{0,32},{32,64},{64,96},{96,128},{128,160},{160,192},{192,224},{224... | collective-permute-start | bytes 417800 | tf_op jit(solution)/shard_map/ppermute | solution.py:363
  97.6 1.6 collective-permute-done.4.refs_3_
  99.2 4.1 %collective-permute-done.3.refs_2_ = bf16[544,128]{1,0:T(8,128)(2,1)S(1)} collective-permute-done((bf16[544,128]{1,0:T(8,128)(2,1)S(1)}, bf16[544,128]{1,0:T(8,128)(2,1)S(1)}, u32[]{:S(2)}, u32[]{:S(2)}) %collective-permute-start.3) | collective-permute-done | bytes 139296 | tf_op jit(solution)/shard_map/ppermute | solution.py:363
  103.3 1.9 collective-permute-start.5
  105.2 4.6 %collective-permute-start.6 = (bf16[544,128]{1,0:T(8,128)(2,1)S(1)}, bf16[544,128]{1,0:T(8,128)(2,1)S(1)}, u32[]{:S(2)}, u32[]{:S(2)}) collective-permute-start(bf16[544,128]{1,0:T(8,128)(2,1)S(1)} %collective-permute-done.4.refs_3_), channel_id=1, source_target_pairs={{32,0},{64,32},{96,64},{128,96},{160,128},{192,160},{224,192},{256... | collective-permute-start | bytes 417800 | tf_op jit(solution)/shard_map/ppermute | solution.py:364
  109.8 2.1 %flash.10 = (f32[2,512]{1,0:T(2,128)S(1)}, f32[2,512]{1,0:T(2,128)S(1)}, f32[2,64,512]{2,1,0:T(8,128)S(1)}) custom-call(bf16[2,64,512]{2,1,0:T(8,128)(2,1)S(1)} %get-tuple-element.105.refs_0_, f32[2,512]{1,0:T(2,128)S(1)} %broadcast_in_dim.12.refs_1_, bf16[544,128]{1,0:T(8,128)(2,1)S(1)} %collective-permute-done.3.refs_2_, ...), custom_call_target="tpu_custom_call" | custom-call | flops 285212672 | bytes 1048576 | tf_op jit(solution)/shard_map/flash/pallas_call | solution.py:232
  112.0 1.9 collective-permute-start.7
  113.9 5.2 %collective-permute-start.8 = (bf16[544,128]{1,0:T(8,128)(2,1)S(1)}, bf16[544,128]{1,0:T(8,128)(2,1)S(1)}, u32[]{:S(2)}, u32[]{:S(2)}) collective-permute-start(bf16[544,128]{1,0:T(8,128)(2,1)S(1)} %collective-permute-done.6.refs_3_), channel_id=1, source_target_pairs={{32,0},{64,32},{96,64},{128,96},{160,128},{192,160},{224,192},{256... | collective-permute-start | bytes 417800 | tf_op jit(solution)/shard_map/ppermute | solution.py:364
  119.2 2.2 %flash.11 = (f32[2,512]{1,0:T(2,128)S(1)}, f32[2,512]{1,0:T(2,128)S(1)}, f32[2,64,512]{2,1,0:T(8,128)S(1)}) custom-call(bf16[2,64,512]{2,1,0:T(8,128)(2,1)S(1)} %get-tuple-element.105.refs_0_, f32[2,512]{1,0:T(2,128)S(1)} %broadcast_in_dim.12.refs_1_, bf16[544,128]{1,0:T(8,128)(2,1)S(1)} %collective-permute-done.5.refs_2_, ...), custom_call_target="tpu_custom_call" | custom-call | flops 285212672 | bytes 1048576 | tf_op jit(solution)/shard_map/flash/pallas_call | solution.py:232
  121.3 3.0 %collective-permute-start.9 = (bf16[544,128]{1,0:T(8,128)(2,1)S(1)}, bf16[544,128]{1,0:T(8,128)(2,1)S(1)}, u32[]{:S(2)}, u32[]{:S(2)}) collective-permute-start(bf16[544,128]{1,0:T(8,128)(2,1)S(1)} %collective-permute-done.7.refs_2_), channel_id=1, source_target_pairs={{0,32},{32,64},{64,96},{96,128},{128,160},{160,192},{192,224},{224... | collective-permute-start | bytes 417800 | tf_op jit(solution)/shard_map/ppermute | solution.py:363
  124.4 4.3 %collective-permute-start.10 = (bf16[544,128]{1,0:T(8,128)(2,1)S(1)}, bf16[544,128]{1,0:T(8,128)(2,1)S(1)}, u32[]{:S(2)}, u32[]{:S(2)}) collective-permute-start(bf16[544,128]{1,0:T(8,128)(2,1)S(1)} %collective-permute-done.8.refs_3_), channel_id=1, source_target_pairs={{32,0},{64,32},{96,64},{128,96},{160,128},{192,160},{224,192},{256... | collective-permute-start | bytes 417800 | tf_op jit(solution)/shard_map/ppermute | solution.py:364
  128.7 2.2 %flash.12 = (f32[2,512]{1,0:T(2,128)S(1)}, f32[2,512]{1,0:T(2,128)S(1)}, f32[2,64,512]{2,1,0:T(8,128)S(1)}) custom-call(bf16[2,64,512]{2,1,0:T(8,128)(2,1)S(1)} %get-tuple-element.105.refs_0_, f32[2,512]{1,0:T(2,128)S(1)} %broadcast_in_dim.12.refs_1_, bf16[544,128]{1,0:T(8,128)(2,1)S(1)} %collective-permute-done.7.refs_2_, ...), custom_call_target="tpu_custom_call" | custom-call | flops 285212672 | bytes 1048576 | tf_op jit(solution)/shard_map/flash/pallas_call | solution.py:232
  130.8 3.1 %collective-permute-start.11 = (bf16[544,128]{1,0:T(8,128)(2,1)S(1)}, bf16[544,128]{1,0:T(8,128)(2,1)S(1)}, u32[]{:S(2)}, u32[]{:S(2)}) collective-permute-start(bf16[544,128]{1,0:T(8,128)(2,1)S(1)} %collective-permute-done.9.refs_2_), channel_id=1, source_target_pairs={{0,32},{32,64},{64,96},{96,128},{128,160},{160,192},{192,224},{224... | collective-permute-start | bytes 417800 | tf_op jit(solution)/shard_map/ppermute | solution.py:363
  133.9 3.9 %collective-permute-start.12 = (bf16[544,128]{1,0:T(8,128)(2,1)S(1)}, bf16[544,128]{1,0:T(8,128)(2,1)S(1)}, u32[]{:S(2)}, u32[]{:S(2)}) collective-permute-start(bf16[544,128]{1,0:T(8,128)(2,1)S(1)} %collective-permute-done.10.refs_3_), channel_id=1, source_target_pairs={{32,0},{64,32},{96,64},{128,96},{160,128},{192,160},{224,192},{256... | collective-permute-start | bytes 417800 | tf_op jit(solution)/shard_map/ppermute | solution.py:364
  137.8 2.2 %flash.13 = (f32[2,512]{1,0:T(2,128)S(1)}, f32[2,512]{1,0:T(2,128)S(1)}, f32[2,64,512]{2,1,0:T(8,128)S(1)}) custom-call(bf16[2,64,512]{2,1,0:T(8,128)(2,1)S(1)} %get-tuple-element.105.refs_0_, f32[2,512]{1,0:T(2,128)S(1)} %broadcast_in_dim.12.refs_1_, bf16[544,128]{1,0:T(8,128)(2,1)S(1)} %collective-permute-done.9.refs_2_, ...), custom_call_target="tpu_custom_call" | custom-call | flops 285212672 | bytes 1048576 | tf_op jit(solution)/shard_map/flash/pallas_call | solution.py:232
  140.0 3.1 %collective-permute-start.13 = (bf16[544,128]{1,0:T(8,128)(2,1)S(1)}, bf16[544,128]{1,0:T(8,128)(2,1)S(1)}, u32[]{:S(2)}, u32[]{:S(2)}) collective-permute-start(bf16[544,128]{1,0:T(8,128)(2,1)S(1)} %collective-permute-done.11.refs_2_), channel_id=1, source_target_pairs={{0,32},{32,64},{64,96},{96,128},{128,160},{160,192},{192,224},{224... | collective-permute-start | bytes 417800 | tf_op jit(solution)/shard_map/ppermute | solution.py:363
  143.1 3.6 %collective-permute-start.14 = (bf16[544,128]{1,0:T(8,128)(2,1)S(1)}, bf16[544,128]{1,0:T(8,128)(2,1)S(1)}, u32[]{:S(2)}, u32[]{:S(2)}) collective-permute-start(bf16[544,128]{1,0:T(8,128)(2,1)S(1)} %collective-permute-done.12.refs_3_), channel_id=1, source_target_pairs={{32,0},{64,32},{96,64},{128,96},{160,128},{192,160},{224,192},{256... | collective-permute-start | bytes 417800 | tf_op jit(solution)/shard_map/ppermute | solution.py:364
  146.7 2.1 %flash.14 = (f32[2,512]{1,0:T(2,128)S(1)}, f32[2,512]{1,0:T(2,128)S(1)}, f32[2,64,512]{2,1,0:T(8,128)S(1)}) custom-call(bf16[2,64,512]{2,1,0:T(8,128)(2,1)S(1)} %get-tuple-element.105.refs_0_, f32[2,512]{1,0:T(2,128)S(1)} %broadcast_in_dim.12.refs_1_, bf16[544,128]{1,0:T(8,128)(2,1)S(1)} %collective-permute-done.11.refs_2_, ...), custom_call_target="tpu_custom_call" | custom-call | flops 285212672 | bytes 1048576 | tf_op jit(solution)/shard_map/flash/pallas_call | solution.py:232
  148.9 3.1 %collective-permute-start.15 = (bf16[544,128]{1,0:T(8,128)(2,1)S(1)}, bf16[544,128]{1,0:T(8,128)(2,1)S(1)}, u32[]{:S(2)}, u32[]{:S(2)}) collective-permute-start(bf16[544,128]{1,0:T(8,128)(2,1)S(1)} %collective-permute-done.13.refs_2_), channel_id=1, source_target_pairs={{0,32},{32,64},{64,96},{96,128},{128,160},{160,192},{192,224},{224... | collective-permute-start | bytes 417800 | tf_op jit(solution)/shard_map/ppermute | solution.py:363
  152.1 3.6 %collective-permute-start.16 = (bf16[544,128]{1,0:T(8,128)(2,1)S(1)}, bf16[544,128]{1,0:T(8,128)(2,1)S(1)}, u32[]{:S(2)}, u32[]{:S(2)}) collective-permute-start(bf16[544,128]{1,0:T(8,128)(2,1)S(1)} %collective-permute-done.14.refs_3_), channel_id=1, source_target_pairs={{32,0},{64,32},{96,64},{128,96},{160,128},{192,160},{224,192},{256... | collective-permute-start | bytes 417800 | tf_op jit(solution)/shard_map/ppermute | solution.py:364
  155.7 2.2 %flash.15 = (f32[2,512]{1,0:T(2,128)S(1)}, f32[2,512]{1,0:T(2,128)S(1)}, f32[2,64,512]{2,1,0:T(8,128)S(1)}) custom-call(bf16[2,64,512]{2,1,0:T(8,128)(2,1)S(1)} %get-tuple-element.105.refs_0_, f32[2,512]{1,0:T(2,128)S(1)} %broadcast_in_dim.12.refs_1_, bf16[544,128]{1,0:T(8,128)(2,1)S(1)} %collective-permute-done.13.refs_2_, ...), custom_call_target="tpu_custom_call" | custom-call | flops 285212672 | bytes 1048576 | tf_op jit(solution)/shard_map/flash/pallas_call | solution.py:232
  157.9 3.2 %collective-permute-start.17 = (bf16[544,128]{1,0:T(8,128)(2,1)S(1)}, bf16[544,128]{1,0:T(8,128)(2,1)S(1)}, u32[]{:S(2)}, u32[]{:S(2)}) collective-permute-start(bf16[544,128]{1,0:T(8,128)(2,1)S(1)} %collective-permute-done.15.refs_2_), channel_id=1, source_target_pairs={{0,32},{32,64},{64,96},{96,128},{128,160},{160,192},{192,224},{224... | collective-permute-start | bytes 417800 | tf_op jit(solution)/shard_map/ppermute | solution.py:363
  161.1 2.2 %flash.16 = (f32[2,512]{1,0:T(2,128)S(1)}, f32[2,512]{1,0:T(2,128)S(1)}, f32[2,64,512]{2,1,0:T(8,128)S(1)}) custom-call(bf16[2,64,512]{2,1,0:T(8,128)(2,1)S(1)} %get-tuple-element.105.refs_0_, f32[2,512]{1,0:T(2,128)S(1)} %broadcast_in_dim.12.refs_1_, bf16[544,128]{1,0:T(8,128)(2,1)S(1)} %collective-permute-done.15.refs_2_, ...), custom_call_target="tpu_custom_call" | custom-call | flops 285212672 | bytes 1048576 | tf_op jit(solution)/shard_map/flash/pallas_call | solution.py:232
  163.3 1.8 collective-permute-done.17.refs_2_
  165.1 1.4 flash.17
  166.5 9.1 %all_to_all.25.a_ref = bf16[4,128,128]{2,1,0:T(8,128)(2,1)S(1)} all-to-all(bf16[4,128,128]{2,1,0:T(8,128)(2,1)S(1)} %flash.17), channel_id=1, replica_groups={{0,8,16,24},{1,9,17,25},{2,10,18,26},{3,11,19,27},{4,12,20,28},{5,13,21..., dimensions={0} | all-to-all | bytes 262144 | tf_op jit(solution)/shard_map/all_to_all | solution.py:378
  175.6 2.9 %out_partial.1 = (bf16[64,4096]{1,0:T(8,128)(2,1)S(1)}, bf16[64,4096]{1,0:T(8,128)(2,1)S(1)}) custom-call(s32[1]{0:T(128)} %bitcast.9.core_ref, bf16[4,128,128]{2,1,0:T(8,128)(2,1)S(1)} %all_to_all.25.a_ref, bf16[4,8,4,128,128]{4,3,2,1,0:T(8,128)(2,1)} %bitcast.15.w_ref), custom_call_target="tpu_custom_call" | custom-call | flops 536870912 | bytes 4194304 | tf_op jit(solution)/shard_map/out_partial/pallas_call | solution.py:271
  178.5 11.7 %collective-permute-start.18 = (bf16[64,4096]{1,0:T(8,128)(2,1)S(1)}, bf16[64,4096]{1,0:T(8,128)(2,1)S(1)}, u32[]{:S(2)}, u32[]{:S(2)}) collective-permute-start(bf16[64,4096]{1,0:T(8,128)(2,1)S(1)} %get-tuple-element.178), channel_id=1, source_target_pairs={{0,1},{1,0},{2,3},{3,2},{4,5},{5,4},{6,7},{7,6},{8,9},{9,8},{10,11... | collective-permute-start | bytes 1572872 | tf_op jit(solution)/shard_map/ppermute | solution.py:380
  190.2 1.5 collective-permute-done.18
  192.6 4.0 %all-to-all-start.4 = ((bf16[4,16,4096]{2,1,0:T(8,128)(2,1)}), bf16[4,16,4096]{2,1,0:T(8,128)(2,1)S(1)}, u32[]{:S(2)}, u32[]{:S(2)}) async-start(bf16[4,16,4096]{2,1,0:T(8,128)(2,1)} %bitcast.16), calls=%async_computation.4 | async-start | bytes 1048576 | tf_op jit(solution)/shard_map/all_to_all | solution.py:382
  197.4 8.1 %all-to-all-done.4 = bf16[4,16,4096]{2,1,0:T(8,128)(2,1)S(1)} async-done(((bf16[4,16,4096]{2,1,0:T(8,128)(2,1)}), bf16[4,16,4096]{2,1,0:T(8,128)(2,1)S(1)}, u32[]{:S(2)}, u32[]{:S(2)}) %all-to-all-start.4) | async-done | bytes 524320 | tf_op jit(solution)/shard_map/all_to_all | solution.py:382
  (65 shorter events, 12.2 us)
Async XLA Ops:
  0.0 13.6 %copy-start = (bf16[256,384]{1,0:T(8,128)(2,1)S(1)}, bf16[256,384]{1,0:T(8,128)(2,1)}, u32[]{:S(2)}) copy-start(bf16[256,384]{1,0:T(8,128)(2,1)} %param.18) | copy-start | bytes 589828
  2.4 7.8 %copy-start.11 = (f32[64]{0:T(128)S(1)}, f32[64]{0:T(128)}, u32[]{:S(2)}) copy-start(f32[64]{0:T(128)} %param.24) | copy-start | bytes 772
  2.5 7.9 %copy-start.10 = (f32[2]{0:T(128)S(1)}, f32[2]{0:T(128)}, u32[]{:S(2)}) copy-start(f32[2]{0:T(128)} %constant.91.clone) | copy-start | bytes 28
  2.5 11.1 %copy-start.9 = (f32[256]{0:T(256)S(1)}, f32[256]{0:T(256)}, u32[]{:S(2)}) copy-start(f32[256]{0:T(256)} %param.17) | copy-start | bytes 3076
  2.5 41.2 %all-to-all-start = ((bf16[16,16,4096]{2,1,0:T(8,128)(2,1)}), bf16[16,16,4096]{2,1,0:T(8,128)(2,1)S(1)}, u32[]{:S(2)}, u32[]{:S(2)}) async-start(bf16[16,16,4096]{2,1,0:T(8,128)(2,1)} %repeated.1), calls=%async_computation | async-start | bytes 4194304 | tf_op jit(solution)/shard_map/all_to_all | solution.py:310
  10.2 43.2 %copy-start.1 = (bf16[4096,128]{1,0:T(8,128)(2,1)S(1)}, bf16[4096,128]{1,0:T(8,128)(2,1)}, u32[]{:S(2)}) copy-start(bf16[4096,128]{1,0:T(8,128)(2,1)} %wq_ref) | copy-start | bytes 3145732
  12.0 60.2 %copy-start.6 = (f32[64]{0:T(128)S(1)}, f32[64]{0:T(128)}, u32[]{:S(2)}) copy-start(f32[64]{0:T(128)} %param.25) | copy-start | bytes 772
  45.1 26.2 %copy-start.8 = (f32[4096]{0:T(1024)S(1)}, f32[4096]{0:T(1024)}, u32[]{:S(2)}) copy-start(f32[4096]{0:T(1024)} %param.19) | copy-start | bytes 49156
  47.4 24.7 %collective-permute-start.1 = (bf16[128,4096]{1,0:T(8,128)(2,1)}, bf16[128,4096]{1,0:T(8,128)(2,1)}, u32[]{:S(2)}, u32[]{:S(2)}) collective-permute-start(bf16[128,4096]{1,0:T(8,128)(2,1)} %pad_maximum_fusion.wkv_ref), channel_id=1, source_target_pairs={{0,1},{1,0},{2,3},{3,2},{4,5},{5,4},{6,7},{7,6},{8,9},{9,8},{10,11... | collective-permute-start | bytes 3145736 | tf_op jit(solution)/shard_map/ppermute | solution.py:343
  53.5 18.7 %collective-permute-start = (bf16[4096,128]{1,0:T(8,128)(2,1)S(1)}, bf16[4096,128]{1,0:T(8,128)(2,1)}, u32[]{:S(2)}, u32[]{:S(2)}) collective-permute-start(bf16[4096,128]{1,0:T(8,128)(2,1)S(1)} %copy-done.1), channel_id=1, source_target_pairs={{0,1},{1,0},{2,3},{3,2},{4,5},{5,4},{6,7},{7,6},{8,9},{9,8},{10,11... | collective-permute-start | bytes 3145736 | tf_op jit(solution)/shard_map/ppermute | solution.py:342
  56.1 15.3 %all-to-all-start.1 = ((f32[32,2,384]{2,1,0:T(2,128)}), f32[32,2,384]{2,1,0:T(2,128)}, u32[]{:S(2)}, u32[]{:S(2)}) async-start(f32[32,2,384]{2,1,0:T(2,128)} %broadcast_in_dim.27), calls=%async_computation.1 | async-start | bytes 196608 | tf_op jit(solution)/shard_map/all_to_all | solution.py:348
  72.2 0.9 copy-start.2
  73.1 0.9 copy-start.3
  79.9 0.6 copy-start.4
  80.6 5.7 %collective-permute-start.2 = (bf16[256,256]{1,0:T(8,128)(2,1)}, bf16[256,256]{1,0:T(8,128)(2,1)S(1)}, u32[]{:S(2)}, u32[]{:S(2)}) collective-permute-start(bf16[256,256]{1,0:T(8,128)(2,1)} %get-tuple-element.103), channel_id=1, source_target_pairs={{0,1},{1,0},{2,3},{3,2},{4,5},{5,4},{6,7},{7,6},{8,9},{9,8},{10,11... | collective-permute-start | bytes 393224 | tf_op jit(solution)/shard_map/ppermute | solution.py:354
  82.9 3.4 %copy-start.5 = (bf16[256,256]{1,0:T(8,128)(2,1)S(1)}, bf16[256,256]{1,0:T(8,128)(2,1)}, u32[]{:S(2)}) copy-start(bf16[256,256]{1,0:T(8,128)(2,1)} %copy-done.4) | copy-start | bytes 393220
  87.6 70.2 %all-to-all-start.2 = ((bf16[32,4,128,128]{3,2,1,0:T(8,128)(2,1)}), bf16[32,4,128,128]{3,2,1,0:T(8,128)(2,1)}, u32[]{:S(2)}, u32[]{:S(2)}) async-start(bf16[32,4,128,128]{3,2,1,0:T(8,128)(2,1)} %bitcast.24), calls=%async_computation.2 | async-start | bytes 8388608 | tf_op jit(solution)/shard_map/all_to_all | solution.py:368
  92.3 6.9 %collective-permute-start.4 = (bf16[544,128]{1,0:T(8,128)(2,1)S(1)}, bf16[544,128]{1,0:T(8,128)(2,1)S(1)}, u32[]{:S(2)}, u32[]{:S(2)}) collective-permute-start(bf16[544,128]{1,0:T(8,128)(2,1)S(1)} %get-tuple-element.107.refs_2_), channel_id=1, source_target_pairs={{32,0},{64,32},{96,64},{128,96},{160,128},{192,160},{224,192},{256... | collective-permute-start | bytes 417800 | tf_op jit(solution)/shard_map/ppermute | solution.py:364
  95.5 7.8 %collective-permute-start.3 = (bf16[544,128]{1,0:T(8,128)(2,1)S(1)}, bf16[544,128]{1,0:T(8,128)(2,1)S(1)}, u32[]{:S(2)}, u32[]{:S(2)}) collective-permute-start(bf16[544,128]{1,0:T(8,128)(2,1)S(1)} %get-tuple-element.107.refs_2_), channel_id=1, source_target_pairs={{0,32},{32,64},{64,96},{96,128},{128,160},{160,192},{192,224},{224... | collective-permute-start | bytes 417800 | tf_op jit(solution)/shard_map/ppermute | solution.py:363
  103.3 8.7 %collective-permute-start.5 = (bf16[544,128]{1,0:T(8,128)(2,1)S(1)}, bf16[544,128]{1,0:T(8,128)(2,1)S(1)}, u32[]{:S(2)}, u32[]{:S(2)}) collective-permute-start(bf16[544,128]{1,0:T(8,128)(2,1)S(1)} %collective-permute-done.3.refs_2_), channel_id=1, source_target_pairs={{0,32},{32,64},{64,96},{96,128},{128,160},{160,192},{192,224},{224... | collective-permute-start | bytes 417800 | tf_op jit(solution)/shard_map/ppermute | solution.py:363
  105.2 6.8 %collective-permute-start.6 = (bf16[544,128]{1,0:T(8,128)(2,1)S(1)}, bf16[544,128]{1,0:T(8,128)(2,1)S(1)}, u32[]{:S(2)}, u32[]{:S(2)}) collective-permute-start(bf16[544,128]{1,0:T(8,128)(2,1)S(1)} %collective-permute-done.4.refs_3_), channel_id=1, source_target_pairs={{32,0},{64,32},{96,64},{128,96},{160,128},{192,160},{224,192},{256... | collective-permute-start | bytes 417800 | tf_op jit(solution)/shard_map/ppermute | solution.py:364
  112.0 9.3 %collective-permute-start.7 = (bf16[544,128]{1,0:T(8,128)(2,1)S(1)}, bf16[544,128]{1,0:T(8,128)(2,1)S(1)}, u32[]{:S(2)}, u32[]{:S(2)}) collective-permute-start(bf16[544,128]{1,0:T(8,128)(2,1)S(1)} %collective-permute-done.5.refs_2_), channel_id=1, source_target_pairs={{0,32},{32,64},{64,96},{96,128},{128,160},{160,192},{192,224},{224... | collective-permute-start | bytes 417800 | tf_op jit(solution)/shard_map/ppermute | solution.py:363
  113.9 7.4 %collective-permute-start.8 = (bf16[544,128]{1,0:T(8,128)(2,1)S(1)}, bf16[544,128]{1,0:T(8,128)(2,1)S(1)}, u32[]{:S(2)}, u32[]{:S(2)}) collective-permute-start(bf16[544,128]{1,0:T(8,128)(2,1)S(1)} %collective-permute-done.6.refs_3_), channel_id=1, source_target_pairs={{32,0},{64,32},{96,64},{128,96},{160,128},{192,160},{224,192},{256... | collective-permute-start | bytes 417800 | tf_op jit(solution)/shard_map/ppermute | solution.py:364
  121.3 9.5 %collective-permute-start.9 = (bf16[544,128]{1,0:T(8,128)(2,1)S(1)}, bf16[544,128]{1,0:T(8,128)(2,1)S(1)}, u32[]{:S(2)}, u32[]{:S(2)}) collective-permute-start(bf16[544,128]{1,0:T(8,128)(2,1)S(1)} %collective-permute-done.7.refs_2_), channel_id=1, source_target_pairs={{0,32},{32,64},{64,96},{96,128},{128,160},{160,192},{192,224},{224... | collective-permute-start | bytes 417800 | tf_op jit(solution)/shard_map/ppermute | solution.py:363
  124.4 6.5 %collective-permute-start.10 = (bf16[544,128]{1,0:T(8,128)(2,1)S(1)}, bf16[544,128]{1,0:T(8,128)(2,1)S(1)}, u32[]{:S(2)}, u32[]{:S(2)}) collective-permute-start(bf16[544,128]{1,0:T(8,128)(2,1)S(1)} %collective-permute-done.8.refs_3_), channel_id=1, source_target_pairs={{32,0},{64,32},{96,64},{128,96},{160,128},{192,160},{224,192},{256... | collective-permute-start | bytes 417800 | tf_op jit(solution)/shard_map/ppermute | solution.py:364
  130.8 9.1 %collective-permute-start.11 = (bf16[544,128]{1,0:T(8,128)(2,1)S(1)}, bf16[544,128]{1,0:T(8,128)(2,1)S(1)}, u32[]{:S(2)}, u32[]{:S(2)}) collective-permute-start(bf16[544,128]{1,0:T(8,128)(2,1)S(1)} %collective-permute-done.9.refs_2_), channel_id=1, source_target_pairs={{0,32},{32,64},{64,96},{96,128},{128,160},{160,192},{192,224},{224... | collective-permute-start | bytes 417800 | tf_op jit(solution)/shard_map/ppermute | solution.py:363
  133.9 6.1 %collective-permute-start.12 = (bf16[544,128]{1,0:T(8,128)(2,1)S(1)}, bf16[544,128]{1,0:T(8,128)(2,1)S(1)}, u32[]{:S(2)}, u32[]{:S(2)}) collective-permute-start(bf16[544,128]{1,0:T(8,128)(2,1)S(1)} %collective-permute-done.10.refs_3_), channel_id=1, source_target_pairs={{32,0},{64,32},{96,64},{128,96},{160,128},{192,160},{224,192},{256... | collective-permute-start | bytes 417800 | tf_op jit(solution)/shard_map/ppermute | solution.py:364
  140.0 8.9 %collective-permute-start.13 = (bf16[544,128]{1,0:T(8,128)(2,1)S(1)}, bf16[544,128]{1,0:T(8,128)(2,1)S(1)}, u32[]{:S(2)}, u32[]{:S(2)}) collective-permute-start(bf16[544,128]{1,0:T(8,128)(2,1)S(1)} %collective-permute-done.11.refs_2_), channel_id=1, source_target_pairs={{0,32},{32,64},{64,96},{96,128},{128,160},{160,192},{192,224},{224... | collective-permute-start | bytes 417800 | tf_op jit(solution)/shard_map/ppermute | solution.py:363
  143.1 5.8 %collective-permute-start.14 = (bf16[544,128]{1,0:T(8,128)(2,1)S(1)}, bf16[544,128]{1,0:T(8,128)(2,1)S(1)}, u32[]{:S(2)}, u32[]{:S(2)}) collective-permute-start(bf16[544,128]{1,0:T(8,128)(2,1)S(1)} %collective-permute-done.12.refs_3_), channel_id=1, source_target_pairs={{32,0},{64,32},{96,64},{128,96},{160,128},{192,160},{224,192},{256... | collective-permute-start | bytes 417800 | tf_op jit(solution)/shard_map/ppermute | solution.py:364
  148.9 8.9 %collective-permute-start.15 = (bf16[544,128]{1,0:T(8,128)(2,1)S(1)}, bf16[544,128]{1,0:T(8,128)(2,1)S(1)}, u32[]{:S(2)}, u32[]{:S(2)}) collective-permute-start(bf16[544,128]{1,0:T(8,128)(2,1)S(1)} %collective-permute-done.13.refs_2_), channel_id=1, source_target_pairs={{0,32},{32,64},{64,96},{96,128},{128,160},{160,192},{192,224},{224... | collective-permute-start | bytes 417800 | tf_op jit(solution)/shard_map/ppermute | solution.py:363
  152.1 5.8 %collective-permute-start.16 = (bf16[544,128]{1,0:T(8,128)(2,1)S(1)}, bf16[544,128]{1,0:T(8,128)(2,1)S(1)}, u32[]{:S(2)}, u32[]{:S(2)}) collective-permute-start(bf16[544,128]{1,0:T(8,128)(2,1)S(1)} %collective-permute-done.14.refs_3_), channel_id=1, source_target_pairs={{32,0},{64,32},{96,64},{128,96},{160,128},{192,160},{224,192},{256... | collective-permute-start | bytes 417800 | tf_op jit(solution)/shard_map/ppermute | solution.py:364
  157.9 7.2 %collective-permute-start.17 = (bf16[544,128]{1,0:T(8,128)(2,1)S(1)}, bf16[544,128]{1,0:T(8,128)(2,1)S(1)}, u32[]{:S(2)}, u32[]{:S(2)}) collective-permute-start(bf16[544,128]{1,0:T(8,128)(2,1)S(1)} %collective-permute-done.15.refs_2_), channel_id=1, source_target_pairs={{0,32},{32,64},{64,96},{96,128},{128,160},{160,192},{192,224},{224... | collective-permute-start | bytes 417800 | tf_op jit(solution)/shard_map/ppermute | solution.py:363
  178.5 27.1 %copy-start.7 = (bf16[16,4096]{1,0:T(8,128)(2,1)S(1)}, bf16[16,4096]{1,0:T(8,128)(2,1)}, u32[]{:S(2)}) copy-start(bf16[16,4096]{1,0:T(8,128)(2,1)} %x_ref.1) | copy-start | bytes 393220
  178.5 13.2 %collective-permute-start.18 = (bf16[64,4096]{1,0:T(8,128)(2,1)S(1)}, bf16[64,4096]{1,0:T(8,128)(2,1)S(1)}, u32[]{:S(2)}, u32[]{:S(2)}) collective-permute-start(bf16[64,4096]{1,0:T(8,128)(2,1)S(1)} %get-tuple-element.178), channel_id=1, source_target_pairs={{0,1},{1,0},{2,3},{3,2},{4,5},{5,4},{6,7},{7,6},{8,9},{9,8},{10,11... | collective-permute-start | bytes 1572872 | tf_op jit(solution)/shard_map/ppermute | solution.py:380
  192.6 12.9 %all-to-all-start.4 = ((bf16[4,16,4096]{2,1,0:T(8,128)(2,1)}), bf16[4,16,4096]{2,1,0:T(8,128)(2,1)S(1)}, u32[]{:S(2)}, u32[]{:S(2)}) async-start(bf16[4,16,4096]{2,1,0:T(8,128)(2,1)} %bitcast.16), calls=%async_computation.4 | async-start | bytes 1048576 | tf_op jit(solution)/shard_map/all_to_all | solution.py:382

commit v4 on v3

--- a/solution.py
+++ b/solution.py
@@ -314,13 +314,13 @@
     inside = (half // own_rows) * (2 * own_rows) + core * own_rows + half % own_rows
     positions = lax.axis_index("sp") * block_rows + inside
     freq_count = hs // 4
-    inverse = 10000.0 ** (-jnp.arange(freq_count, dtype=jnp.float32) / freq_count)
-    grid_row = (positions // GRID_W).astype(jnp.float32)
-    grid_col = (positions % GRID_W).astype(jnp.float32)
-    angles = jnp.concatenate([grid_row[:, None] * inverse, grid_col[:, None] * inverse], axis=-1)
-    cos = jnp.tile(jnp.repeat(jnp.cos(angles), 2, axis=1), (1, 2))
-    sign = jnp.tile(jnp.array([-1.0, 1.0], jnp.float32), hs)
-    sin = jnp.tile(jnp.repeat(jnp.sin(angles), 2, axis=1), (1, 2)) * sign
+    lane = lax.broadcasted_iota(jnp.int32, (block_rows // 2, 2 * hs), 1)
+    pair = lane % hs // 2
+    inverse = 10000.0 ** (-(pair % freq_count).astype(jnp.float32) / freq_count)
+    along = jnp.where(pair < freq_count, positions[:, None] // GRID_W, positions[:, None] % GRID_W)
+    angles = along.astype(jnp.float32) * inverse
+    cos = jnp.cos(angles)
+    sin = jnp.where(lane % 2 == 0, -jnp.sin(angles), jnp.sin(angles))
     lift = jnp.broadcast_to(context_lift[:, None], (context_lift.shape[0], block_rows))
     q_gain = jnp.tile(query_gain, 2)[None]
     k_gain = key_gain[None]

time: 208 us -> 199 us (0.957)
  blocking collectives: 37.4 us -> 52.3 us
  local copies, waits for them, and re-layouts: 9.48 us -> 2.25 us
  starting transfers between devices: 95.9 us -> 90.4 us
  waiting for transfers between devices: 23.1 us -> 17.7 us
  other arithmetic: 6.55 us -> 4.31 us
    all_to_all x0 -> x1, blocking collectives: none -> 14.9 us  [local(): mod = lax.all_to_all(mod_copies, 'tp', 0, 0, tiled=True)]
    all_to_all x1 -> x0, starting transfers between devices: 7.81 us -> none  [local(): mod = lax.all_to_all(mod_copies, 'tp', 0, 0, tiled=True)]
    ppermute x7, starting transfers between devices: 28.3 us -> 35 us  [local(): nxt_b = lax.ppermute(bwd, 'sp', down) if step < n_sp // 2 else None]
    all_to_all x1 -> x0, waiting for transfers between devices: 5.79 us -> none  [local(): mod = lax.all_to_all(mod_copies, 'tp', 0, 0, tiled=True)]
    ppermute x8, starting transfers between devices: 21.5 us -> 17.2 us  [local(): nxt_f = lax.ppermute(fwd, 'sp', up)]
  transfers between devices with their start and end apart: 23 -> 22, of which waited for: 6 -> 5; matrix products, arithmetic and copies ran while one was open for 4% -> 1% of each run, Pallas kernels for 9% -> 9%
where the time goes in v4:
time: 199 us; the launch traced here: 198 us
  starting transfers between devices  90.4 us (45%)
  blocking collectives  52.3 us (26%)
  Pallas kernels  30.5 us (15%)
  waiting for transfers between devices  17.7 us (9%)
  other arithmetic  4.31 us (2%)
  local copies, waits for them, and re-layouts  2.25 us (1%)
    ppermute x7, starting transfers between devices, local(): nxt_b = lax.ppermute(bwd, 'sp', down) if step < n_sp // 2 else None  35 us
    pallas_call x9, Pallas kernels, flash(): pl.pallas_call(functools.partial(flash_body, len(blocks), first, last, la...  17.6 us
    ppermute x8, starting transfers between devices, local(): nxt_f = lax.ppermute(fwd, 'sp', up)  17.2 us
    psum x1, blocking collectives, local(): lax.psum(lax.psum(partial_mod, 'sp', axis_index_groups=near_z), 'sp', axi...  16.8 us
    all_to_all x1, blocking collectives, local(): mod = lax.all_to_all(mod_copies, 'tp', 0, 0, tiled=True)  14.9 us
    psum x1, blocking collectives, local(): lax.psum(partial_mod, 'sp', axis_index_groups=near_z)  11.4 us
    ppermute x1, starting transfers between devices, local(): lax.ppermute(send, 'tp', swap).astype(jnp.float32)  11.3 us
    all_to_all x1, blocking collectives, local(): lax.all_to_all(attended, 'tp', 0, 0, axis_index_groups=group_y, tiled=True)  9.09 us
  transfers between devices with their start and end apart: 22, of which 5 were waited for; matrix products, arithmetic and copies ran while one was open for 1% of the time, Pallas kernels for 9%

profile of v4, /device:TPU:1, one launch (start us, length us, event | category | flops | bytes accessed | tf_op | source)
XLA Modules:
  0.0 198.2 jit_solution(17903812906980582270)
XLA Ops:
  0.0 2.4 %repeated.1 = bf16[16,16,4096]{2,1,0:T(8,128)(2,1)} custom-call(bf16[16,4096]{1,0:T(8,128)(2,1)} %x_ref.1), custom_call_target="tpu_custom_call" | custom-call | bytes 2228224 | tf_op jit(solution)/shard_map/repeated/pallas_call | solution.py:66
  2.5 7.7 %all-to-all-start = ((bf16[16,16,4096]{2,1,0:T(8,128)(2,1)}), bf16[16,16,4096]{2,1,0:T(8,128)(2,1)S(1)}, u32[]{:S(2)}, u32[]{:S(2)}) async-start(bf16[16,16,4096]{2,1,0:T(8,128)(2,1)} %repeated.1), calls=%async_computation | async-start | bytes 4194304 | tf_op jit(solution)/shard_map/all_to_all | solution.py:310
  10.5 11.4 %psum.14 = f32[2,384]{1,0:T(2,128)S(1)} all-reduce(f32[2,384]{1,0:T(2,128)S(1)} %fusion.16), channel_id=1, replica_groups={{0,32,64,96},{128,160,192,224},{256,288,320,352},{384,416,448,480},{1,3..., use_global_device_ids=true, to_apply=%region_0.1 | all-reduce | flops 768 | bytes 6144 | tf_op jit(solution)/shard_map/psum | solution.py:333
  21.9 16.8 %psum.15 = f32[2,384]{1,0:T(2,128)S(1)} all-reduce(f32[2,384]{1,0:T(2,128)S(1)} %psum.14), channel_id=1, replica_groups={{0,128,256,384},{32,160,288,416},{64,192,320,448},{96,224,352,480},{1,1..., use_global_device_ids=true, to_apply=%region_1.2 | all-reduce | flops 768 | bytes 6144 | tf_op jit(solution)/shard_map/psum | solution.py:333
  38.8 1.2 negate_select_fusion
  40.1 1.3 pad_maximum_fusion.wkv_ref
  41.4 6.3 %collective-permute-start.1 = (bf16[128,4096]{1,0:T(8,128)(2,1)S(1)}, bf16[128,4096]{1,0:T(8,128)(2,1)S(1)}, u32[]{:S(2)}, u32[]{:S(2)}) collective-permute-start(bf16[128,4096]{1,0:T(8,128)(2,1)S(1)} %pad_maximum_fusion.wkv_ref), channel_id=1, source_target_pairs={{0,1},{1,0},{2,3},{3,2},{4,5},{5,4},{6,7},{7,6},{8,9},{9,8},{10,11... | collective-permute-start | bytes 3145736 | tf_op jit(solution)/shard_map/ppermute | solution.py:343
  47.7 1.9 collective-permute-start
  49.7 14.9 %all_to_all.25 = f32[32,2,384]{2,1,0:T(2,128)S(1)} all-to-all(f32[32,2,384]{2,1,0:T(2,128)S(1)} %broadcast_in_dim.35), channel_id=1, replica_groups=mesh['sp'=16,'tp'=32] {'tp'}, dimensions={0} | all-to-all | bytes 196608 | tf_op jit(solution)/shard_map/all_to_all | solution.py:348
  65.3 4.0 %qkv.1 = (bf16[256,256]{1,0:T(8,128)(2,1)S(1)}, bf16[256,256]{1,0:T(8,128)(2,1)}, bf16[32,128]{1,0:T(8,128)(2,1)S(1)}) custom-call(bf16[256,4096]{1,0:T(8,128)(2,1)S(1)} %bitcast.16, bf16[32,4096]{1,0:T(8,128)(2,1)S(1)} %copy-done.3, f32[2,4096]{1,0:T(2,128)S(1)} %get-tuple-element.180.gain_ref, f32[2,4096]{1,0:T(2,128)S(1)} %get-tuple-element.179.shift_ref, ...), custom_call_target="tpu_custom_call" | custom-call | flops 1073741824 | bytes 6291456 | tf_op jit(solution)/shard_map/qkv/pallas_call | solution.py:114
  70.0 2.3 %collective-permute-start.2 = (bf16[256,256]{1,0:T(8,128)(2,1)}, bf16[256,256]{1,0:T(8,128)(2,1)S(1)}, u32[]{:S(2)}, u32[]{:S(2)}) collective-permute-start(bf16[256,256]{1,0:T(8,128)(2,1)} %get-tuple-element.103), channel_id=1, source_target_pairs={{0,1},{1,0},{2,3},{3,2},{4,5},{5,4},{6,7},{7,6},{8,9},{9,8},{10,11... | collective-permute-start | bytes 393224 | tf_op jit(solution)/shard_map/ppermute | solution.py:354
  72.3 3.4 %spread.1 = bf16[4,8,4,128,128]{4,3,2,1,0:T(8,128)(2,1)} custom-call(bf16[4,8,128,128]{3,2,1,0:T(8,128)(2,1)} %bitcast.19), custom_call_target="tpu_custom_call" | custom-call | bytes 5242880 | tf_op jit(solution)/shard_map/spread/pallas_call | solution.py:46
  75.9 1.2 flash.9
  77.1 4.7 %all-to-all-start.2 = ((bf16[32,4,128,128]{3,2,1,0:T(8,128)(2,1)}), bf16[32,4,128,128]{3,2,1,0:T(8,128)(2,1)}, u32[]{:S(2)}, u32[]{:S(2)}) async-start(bf16[32,4,128,128]{3,2,1,0:T(8,128)(2,1)} %bitcast.18), calls=%async_computation.2 | async-start | bytes 8388608 | tf_op jit(solution)/shard_map/all_to_all | solution.py:368
  81.7 6.0 %collective-permute-start.4 = (bf16[544,128]{1,0:T(8,128)(2,1)S(1)}, bf16[544,128]{1,0:T(8,128)(2,1)S(1)}, u32[]{:S(2)}, u32[]{:S(2)}) collective-permute-start(bf16[544,128]{1,0:T(8,128)(2,1)S(1)} %get-tuple-element.107.refs_2_), channel_id=1, source_target_pairs={{32,0},{64,32},{96,64},{128,96},{160,128},{192,160},{224,192},{256... | collective-permute-start | bytes 417800 | tf_op jit(solution)/shard_map/ppermute | solution.py:364
  87.7 1.9 collective-permute-start.3
  89.6 0.8 collective-permute-done.4.refs_3_
  90.4 5.2 %collective-permute-done.3.refs_2_ = bf16[544,128]{1,0:T(8,128)(2,1)S(1)} collective-permute-done((bf16[544,128]{1,0:T(8,128)(2,1)S(1)}, bf16[544,128]{1,0:T(8,128)(2,1)S(1)}, u32[]{:S(2)}, u32[]{:S(2)}) %collective-permute-start.3) | collective-permute-done | bytes 139296 | tf_op jit(solution)/shard_map/ppermute | solution.py:363
  95.6 1.9 collective-permute-start.5
  97.5 4.6 %collective-permute-start.6 = (bf16[544,128]{1,0:T(8,128)(2,1)S(1)}, bf16[544,128]{1,0:T(8,128)(2,1)S(1)}, u32[]{:S(2)}, u32[]{:S(2)}) collective-permute-start(bf16[544,128]{1,0:T(8,128)(2,1)S(1)} %collective-permute-done.4.refs_3_), channel_id=1, source_target_pairs={{32,0},{64,32},{96,64},{128,96},{160,128},{192,160},{224,192},{256... | collective-permute-start | bytes 417800 | tf_op jit(solution)/shard_map/ppermute | solution.py:364
  102.1 2.1 %flash.10 = (f32[2,512]{1,0:T(2,128)S(1)}, f32[2,512]{1,0:T(2,128)S(1)}, f32[2,64,512]{2,1,0:T(8,128)S(1)}) custom-call(bf16[2,64,512]{2,1,0:T(8,128)(2,1)S(1)} %get-tuple-element.105.refs_0_, f32[2,512]{1,0:T(2,128)S(1)} %broadcast_in_dim.33.refs_1_, bf16[544,128]{1,0:T(8,128)(2,1)S(1)} %collective-permute-done.3.refs_2_, ...), custom_call_target="tpu_custom_call" | custom-call | flops 285212672 | bytes 1048576 | tf_op jit(solution)/shard_map/flash/pallas_call | solution.py:232
  104.2 1.9 collective-permute-start.7
  106.2 5.2 %collective-permute-start.8 = (bf16[544,128]{1,0:T(8,128)(2,1)S(1)}, bf16[544,128]{1,0:T(8,128)(2,1)S(1)}, u32[]{:S(2)}, u32[]{:S(2)}) collective-permute-start(bf16[544,128]{1,0:T(8,128)(2,1)S(1)} %collective-permute-done.6.refs_3_), channel_id=1, source_target_pairs={{32,0},{64,32},{96,64},{128,96},{160,128},{192,160},{224,192},{256... | collective-permute-start | bytes 417800 | tf_op jit(solution)/shard_map/ppermute | solution.py:364
  111.4 2.2 %flash.11 = (f32[2,512]{1,0:T(2,128)S(1)}, f32[2,512]{1,0:T(2,128)S(1)}, f32[2,64,512]{2,1,0:T(8,128)S(1)}) custom-call(bf16[2,64,512]{2,1,0:T(8,128)(2,1)S(1)} %get-tuple-element.105.refs_0_, f32[2,512]{1,0:T(2,128)S(1)} %broadcast_in_dim.33.refs_1_, bf16[544,128]{1,0:T(8,128)(2,1)S(1)} %collective-permute-done.5.refs_2_, ...), custom_call_target="tpu_custom_call" | custom-call | flops 285212672 | bytes 1048576 | tf_op jit(solution)/shard_map/flash/pallas_call | solution.py:232
  113.6 1.9 collective-permute-start.9
  115.5 5.4 %collective-permute-start.10 = (bf16[544,128]{1,0:T(8,128)(2,1)S(1)}, bf16[544,128]{1,0:T(8,128)(2,1)S(1)}, u32[]{:S(2)}, u32[]{:S(2)}) collective-permute-start(bf16[544,128]{1,0:T(8,128)(2,1)S(1)} %collective-permute-done.8.refs_3_), channel_id=1, source_target_pairs={{32,0},{64,32},{96,64},{128,96},{160,128},{192,160},{224,192},{256... | collective-permute-start | bytes 417800 | tf_op jit(solution)/shard_map/ppermute | solution.py:364
  120.9 2.1 %flash.12 = (f32[2,512]{1,0:T(2,128)S(1)}, f32[2,512]{1,0:T(2,128)S(1)}, f32[2,64,512]{2,1,0:T(8,128)S(1)}) custom-call(bf16[2,64,512]{2,1,0:T(8,128)(2,1)S(1)} %get-tuple-element.105.refs_0_, f32[2,512]{1,0:T(2,128)S(1)} %broadcast_in_dim.33.refs_1_, bf16[544,128]{1,0:T(8,128)(2,1)S(1)} %collective-permute-done.7.refs_2_, ...), custom_call_target="tpu_custom_call" | custom-call | flops 285212672 | bytes 1048576 | tf_op jit(solution)/shard_map/flash/pallas_call | solution.py:232
  123.1 1.9 collective-permute-start.11
  125.0 5.0 %collective-permute-start.12 = (bf16[544,128]{1,0:T(8,128)(2,1)S(1)}, bf16[544,128]{1,0:T(8,128)(2,1)S(1)}, u32[]{:S(2)}, u32[]{:S(2)}) collective-permute-start(bf16[544,128]{1,0:T(8,128)(2,1)S(1)} %collective-permute-done.10.refs_3_), channel_id=1, source_target_pairs={{32,0},{64,32},{96,64},{128,96},{160,128},{192,160},{224,192},{256... | collective-permute-start | bytes 417800 | tf_op jit(solution)/shard_map/ppermute | solution.py:364
  130.0 2.2 %flash.13 = (f32[2,512]{1,0:T(2,128)S(1)}, f32[2,512]{1,0:T(2,128)S(1)}, f32[2,64,512]{2,1,0:T(8,128)S(1)}) custom-call(bf16[2,64,512]{2,1,0:T(8,128)(2,1)S(1)} %get-tuple-element.105.refs_0_, f32[2,512]{1,0:T(2,128)S(1)} %broadcast_in_dim.33.refs_1_, bf16[544,128]{1,0:T(8,128)(2,1)S(1)} %collective-permute-done.9.refs_2_, ...), custom_call_target="tpu_custom_call" | custom-call | flops 285212672 | bytes 1048576 | tf_op jit(solution)/shard_map/flash/pallas_call | solution.py:232
  132.2 1.9 collective-permute-start.13
  134.2 4.8 %collective-permute-start.14 = (bf16[544,128]{1,0:T(8,128)(2,1)S(1)}, bf16[544,128]{1,0:T(8,128)(2,1)S(1)}, u32[]{:S(2)}, u32[]{:S(2)}) collective-permute-start(bf16[544,128]{1,0:T(8,128)(2,1)S(1)} %collective-permute-done.12.refs_3_), channel_id=1, source_target_pairs={{32,0},{64,32},{96,64},{128,96},{160,128},{192,160},{224,192},{256... | collective-permute-start | bytes 417800 | tf_op jit(solution)/shard_map/ppermute | solution.py:364
  139.0 2.2 %flash.14 = (f32[2,512]{1,0:T(2,128)S(1)}, f32[2,512]{1,0:T(2,128)S(1)}, f32[2,64,512]{2,1,0:T(8,128)S(1)}) custom-call(bf16[2,64,512]{2,1,0:T(8,128)(2,1)S(1)} %get-tuple-element.105.refs_0_, f32[2,512]{1,0:T(2,128)S(1)} %broadcast_in_dim.33.refs_1_, bf16[544,128]{1,0:T(8,128)(2,1)S(1)} %collective-permute-done.11.refs_2_, ...), custom_call_target="tpu_custom_call" | custom-call | flops 285212672 | bytes 1048576 | tf_op jit(solution)/shard_map/flash/pallas_call | solution.py:232
  141.1 2.7 %collective-permute-start.15 = (bf16[544,128]{1,0:T(8,128)(2,1)S(1)}, bf16[544,128]{1,0:T(8,128)(2,1)S(1)}, u32[]{:S(2)}, u32[]{:S(2)}) collective-permute-start(bf16[544,128]{1,0:T(8,128)(2,1)S(1)} %collective-permute-done.13.refs_2_), channel_id=1, source_target_pairs={{0,32},{32,64},{64,96},{96,128},{128,160},{160,192},{192,224},{224... | collective-permute-start | bytes 417800 | tf_op jit(solution)/shard_map/ppermute | solution.py:363
  143.9 4.0 %collective-permute-start.16 = (bf16[544,128]{1,0:T(8,128)(2,1)S(1)}, bf16[544,128]{1,0:T(8,128)(2,1)S(1)}, u32[]{:S(2)}, u32[]{:S(2)}) collective-permute-start(bf16[544,128]{1,0:T(8,128)(2,1)S(1)} %collective-permute-done.14.refs_3_), channel_id=1, source_target_pairs={{32,0},{64,32},{96,64},{128,96},{160,128},{192,160},{224,192},{256... | collective-permute-start | bytes 417800 | tf_op jit(solution)/shard_map/ppermute | solution.py:364
  147.9 2.2 %flash.15 = (f32[2,512]{1,0:T(2,128)S(1)}, f32[2,512]{1,0:T(2,128)S(1)}, f32[2,64,512]{2,1,0:T(8,128)S(1)}) custom-call(bf16[2,64,512]{2,1,0:T(8,128)(2,1)S(1)} %get-tuple-element.105.refs_0_, f32[2,512]{1,0:T(2,128)S(1)} %broadcast_in_dim.33.refs_1_, bf16[544,128]{1,0:T(8,128)(2,1)S(1)} %collective-permute-done.13.refs_2_, ...), custom_call_target="tpu_custom_call" | custom-call | flops 285212672 | bytes 1048576 | tf_op jit(solution)/shard_map/flash/pallas_call | solution.py:232
  150.1 3.0 %collective-permute-start.17 = (bf16[544,128]{1,0:T(8,128)(2,1)S(1)}, bf16[544,128]{1,0:T(8,128)(2,1)S(1)}, u32[]{:S(2)}, u32[]{:S(2)}) collective-permute-start(bf16[544,128]{1,0:T(8,128)(2,1)S(1)} %collective-permute-done.15.refs_2_), channel_id=1, source_target_pairs={{0,32},{32,64},{64,96},{96,128},{128,160},{160,192},{192,224},{224... | collective-permute-start | bytes 417800 | tf_op jit(solution)/shard_map/ppermute | solution.py:363
  153.1 2.2 %flash.16 = (f32[2,512]{1,0:T(2,128)S(1)}, f32[2,512]{1,0:T(2,128)S(1)}, f32[2,64,512]{2,1,0:T(8,128)S(1)}) custom-call(bf16[2,64,512]{2,1,0:T(8,128)(2,1)S(1)} %get-tuple-element.105.refs_0_, f32[2,512]{1,0:T(2,128)S(1)} %broadcast_in_dim.33.refs_1_, bf16[544,128]{1,0:T(8,128)(2,1)S(1)} %collective-permute-done.15.refs_2_, ...), custom_call_target="tpu_custom_call" | custom-call | flops 285212672 | bytes 1048576 | tf_op jit(solution)/shard_map/flash/pallas_call | solution.py:232
  155.2 2.1 %collective-permute-done.17.refs_2_ = bf16[544,128]{1,0:T(8,128)(2,1)S(1)} collective-permute-done((bf16[544,128]{1,0:T(8,128)(2,1)S(1)}, bf16[544,128]{1,0:T(8,128)(2,1)S(1)}, u32[]{:S(2)}, u32[]{:S(2)}) %collective-permute-start.17) | collective-permute-done | bytes 139296 | tf_op jit(solution)/shard_map/ppermute | solution.py:363
  157.3 1.4 flash.17
  158.7 9.1 %all_to_all.26.a_ref = bf16[4,128,128]{2,1,0:T(8,128)(2,1)S(1)} all-to-all(bf16[4,128,128]{2,1,0:T(8,128)(2,1)S(1)} %flash.17), channel_id=1, replica_groups={{0,8,16,24},{1,9,17,25},{2,10,18,26},{3,11,19,27},{4,12,20,28},{5,13,21..., dimensions={0} | all-to-all | bytes 262144 | tf_op jit(solution)/shard_map/all_to_all | solution.py:378
  167.8 2.9 %out_partial.1 = (bf16[64,4096]{1,0:T(8,128)(2,1)S(1)}, bf16[64,4096]{1,0:T(8,128)(2,1)S(1)}) custom-call(s32[1]{0:T(128)} %bitcast.7.core_ref, bf16[4,128,128]{2,1,0:T(8,128)(2,1)S(1)} %all_to_all.26.a_ref, bf16[4,8,4,128,128]{4,3,2,1,0:T(8,128)(2,1)} %bitcast.13.w_ref), custom_call_target="tpu_custom_call" | custom-call | flops 536870912 | bytes 4194304 | tf_op jit(solution)/shard_map/out_partial/pallas_call | solution.py:271
  170.7 11.3 %collective-permute-start.18 = (bf16[64,4096]{1,0:T(8,128)(2,1)S(1)}, bf16[64,4096]{1,0:T(8,128)(2,1)S(1)}, u32[]{:S(2)}, u32[]{:S(2)}) collective-permute-start(bf16[64,4096]{1,0:T(8,128)(2,1)S(1)} %get-tuple-element.178), channel_id=1, source_target_pairs={{0,1},{1,0},{2,3},{3,2},{4,5},{5,4},{6,7},{7,6},{8,9},{9,8},{10,11... | collective-permute-start | bytes 1572872 | tf_op jit(solution)/shard_map/ppermute | solution.py:380
  182.1 1.5 collective-permute-done.18
  183.6 0.9 add_convert_fusion
  184.5 4.0 %all-to-all-start.4 = ((bf16[4,16,4096]{2,1,0:T(8,128)(2,1)}), bf16[4,16,4096]{2,1,0:T(8,128)(2,1)S(1)}, u32[]{:S(2)}, u32[]{:S(2)}) async-start(bf16[4,16,4096]{2,1,0:T(8,128)(2,1)} %bitcast.14), calls=%async_computation.4 | async-start | bytes 1048576 | tf_op jit(solution)/shard_map/all_to_all | solution.py:382
  188.5 0.8 slice.12
  189.3 8.1 %all-to-all-done.4 = bf16[4,16,4096]{2,1,0:T(8,128)(2,1)S(1)} async-done(((bf16[4,16,4096]{2,1,0:T(8,128)(2,1)}), bf16[4,16,4096]{2,1,0:T(8,128)(2,1)S(1)}, u32[]{:S(2)}, u32[]{:S(2)}) %all-to-all-start.4) | async-done | bytes 524320 | tf_op jit(solution)/shard_map/all_to_all | solution.py:382
  (58 shorter events, 2.6 us)
Async XLA Ops:
  0.0 10.4 %copy-start = (bf16[256,384]{1,0:T(8,128)(2,1)S(1)}, bf16[256,384]{1,0:T(8,128)(2,1)}, u32[]{:S(2)}) copy-start(bf16[256,384]{1,0:T(8,128)(2,1)} %param.17) | copy-start | bytes 589828
  2.4 7.8 %copy-start.13 = (f32[64]{0:T(128)S(1)}, f32[64]{0:T(128)}, u32[]{:S(2)}) copy-start(f32[64]{0:T(128)} %param.23) | copy-start | bytes 772
  2.5 7.9 %copy-start.10 = (f32[256]{0:T(256)S(1)}, f32[256]{0:T(256)}, u32[]{:S(2)}) copy-start(f32[256]{0:T(256)} %param.16) | copy-start | bytes 3076
  2.5 7.9 %copy-start.11 = (f32[256]{0:T(256)S(1)}, f32[256]{0:T(256)}, u32[]{:S(2)}) copy-start(f32[256]{0:T(256)} %param.15) | copy-start | bytes 3076
  2.5 37.5 %copy-start.12 = (f32[2]{0:T(128)S(1)}, f32[2]{0:T(128)}, u32[]{:S(2)}) copy-start(f32[2]{0:T(128)} %param.25) | copy-start | bytes 28
  2.5 37.5 %all-to-all-start = ((bf16[16,16,4096]{2,1,0:T(8,128)(2,1)}), bf16[16,16,4096]{2,1,0:T(8,128)(2,1)S(1)}, u32[]{:S(2)}, u32[]{:S(2)}) async-start(bf16[16,16,4096]{2,1,0:T(8,128)(2,1)} %repeated.1), calls=%async_computation | async-start | bytes 4194304 | tf_op jit(solution)/shard_map/all_to_all | solution.py:310
  10.2 37.5 %copy-start.1 = (bf16[4096,128]{1,0:T(8,128)(2,1)S(1)}, bf16[4096,128]{1,0:T(8,128)(2,1)}, u32[]{:S(2)}) copy-start(bf16[4096,128]{1,0:T(8,128)(2,1)} %wq_ref) | copy-start | bytes 3145732
  10.2 54.4 %copy-start.9 = (f32[4096]{0:T(1024)S(1)}, f32[4096]{0:T(1024)}, u32[]{:S(2)}) copy-start(f32[4096]{0:T(1024)} %param.18) | copy-start | bytes 49156
  10.2 55.0 %copy-start.6 = (f32[64]{0:T(128)S(1)}, f32[64]{0:T(128)}, u32[]{:S(2)}) copy-start(f32[64]{0:T(128)} %param.24) | copy-start | bytes 772
  40.0 25.3 %copy-start.2 = (f32[256,128]{1,0:T(8,128)S(1)}, f32[256,128]{1,0:T(8,128)}, u32[]{:S(2)}) copy-start(f32[256,128]{1,0:T(8,128)} %get-tuple-element.100.cos_ref) | copy-start | bytes 393220
  40.0 25.3 %copy-start.3 = (bf16[32,4096]{1,0:T(8,128)(2,1)S(1)}, bf16[32,4096]{1,0:T(8,128)(2,1)}, u32[]{:S(2)}) copy-start(bf16[32,4096]{1,0:T(8,128)(2,1)} %ctx_ref.1) | copy-start | bytes 786436
  41.4 23.2 %collective-permute-start.1 = (bf16[128,4096]{1,0:T(8,128)(2,1)S(1)}, bf16[128,4096]{1,0:T(8,128)(2,1)S(1)}, u32[]{:S(2)}, u32[]{:S(2)}) collective-permute-start(bf16[128,4096]{1,0:T(8,128)(2,1)S(1)} %pad_maximum_fusion.wkv_ref), channel_id=1, source_target_pairs={{0,1},{1,0},{2,3},{3,2},{4,5},{5,4},{6,7},{7,6},{8,9},{9,8},{10,11... | collective-permute-start | bytes 3145736 | tf_op jit(solution)/shard_map/ppermute | solution.py:343
  47.7 17.0 %collective-permute-start = (bf16[4096,128]{1,0:T(8,128)(2,1)S(1)}, bf16[4096,128]{1,0:T(8,128)(2,1)S(1)}, u32[]{:S(2)}, u32[]{:S(2)}) collective-permute-start(bf16[4096,128]{1,0:T(8,128)(2,1)S(1)} %copy-done.1), channel_id=1, source_target_pairs={{0,1},{1,0},{2,3},{3,2},{4,5},{5,4},{6,7},{7,6},{8,9},{9,8},{10,11... | collective-permute-start | bytes 3145736 | tf_op jit(solution)/shard_map/ppermute | solution.py:342
  64.6 0.6 copy-start.8
  69.3 0.6 copy-start.4
  70.0 5.7 %collective-permute-start.2 = (bf16[256,256]{1,0:T(8,128)(2,1)}, bf16[256,256]{1,0:T(8,128)(2,1)S(1)}, u32[]{:S(2)}, u32[]{:S(2)}) collective-permute-start(bf16[256,256]{1,0:T(8,128)(2,1)} %get-tuple-element.103), channel_id=1, source_target_pairs={{0,1},{1,0},{2,3},{3,2},{4,5},{5,4},{6,7},{7,6},{8,9},{9,8},{10,11... | collective-permute-start | bytes 393224 | tf_op jit(solution)/shard_map/ppermute | solution.py:354
  72.3 3.5 %copy-start.5 = (bf16[256,256]{1,0:T(8,128)(2,1)S(1)}, bf16[256,256]{1,0:T(8,128)(2,1)}, u32[]{:S(2)}) copy-start(bf16[256,256]{1,0:T(8,128)(2,1)} %copy-done.4) | copy-start | bytes 393220
  77.1 73.0 %all-to-all-start.2 = ((bf16[32,4,128,128]{3,2,1,0:T(8,128)(2,1)}), bf16[32,4,128,128]{3,2,1,0:T(8,128)(2,1)}, u32[]{:S(2)}, u32[]{:S(2)}) async-start(bf16[32,4,128,128]{3,2,1,0:T(8,128)(2,1)} %bitcast.18), calls=%async_computation.2 | async-start | bytes 8388608 | tf_op jit(solution)/shard_map/all_to_all | solution.py:368
  81.7 8.7 %collective-permute-start.4 = (bf16[544,128]{1,0:T(8,128)(2,1)S(1)}, bf16[544,128]{1,0:T(8,128)(2,1)S(1)}, u32[]{:S(2)}, u32[]{:S(2)}) collective-permute-start(bf16[544,128]{1,0:T(8,128)(2,1)S(1)} %get-tuple-element.107.refs_2_), channel_id=1, source_target_pairs={{32,0},{64,32},{96,64},{128,96},{160,128},{192,160},{224,192},{256... | collective-permute-start | bytes 417800 | tf_op jit(solution)/shard_map/ppermute | solution.py:364
  87.7 7.8 %collective-permute-start.3 = (bf16[544,128]{1,0:T(8,128)(2,1)S(1)}, bf16[544,128]{1,0:T(8,128)(2,1)S(1)}, u32[]{:S(2)}, u32[]{:S(2)}) collective-permute-start(bf16[544,128]{1,0:T(8,128)(2,1)S(1)} %get-tuple-element.107.refs_2_), channel_id=1, source_target_pairs={{0,32},{32,64},{64,96},{96,128},{128,160},{160,192},{192,224},{224... | collective-permute-start | bytes 417800 | tf_op jit(solution)/shard_map/ppermute | solution.py:363
  95.6 8.7 %collective-permute-start.5 = (bf16[544,128]{1,0:T(8,128)(2,1)S(1)}, bf16[544,128]{1,0:T(8,128)(2,1)S(1)}, u32[]{:S(2)}, u32[]{:S(2)}) collective-permute-start(bf16[544,128]{1,0:T(8,128)(2,1)S(1)} %collective-permute-done.3.refs_2_), channel_id=1, source_target_pairs={{0,32},{32,64},{64,96},{96,128},{128,160},{160,192},{192,224},{224... | collective-permute-start | bytes 417800 | tf_op jit(solution)/shard_map/ppermute | solution.py:363
  97.5 6.8 %collective-permute-start.6 = (bf16[544,128]{1,0:T(8,128)(2,1)S(1)}, bf16[544,128]{1,0:T(8,128)(2,1)S(1)}, u32[]{:S(2)}, u32[]{:S(2)}) collective-permute-start(bf16[544,128]{1,0:T(8,128)(2,1)S(1)} %collective-permute-done.4.refs_3_), channel_id=1, source_target_pairs={{32,0},{64,32},{96,64},{128,96},{160,128},{192,160},{224,192},{256... | collective-permute-start | bytes 417800 | tf_op jit(solution)/shard_map/ppermute | solution.py:364
  104.2 9.3 %collective-permute-start.7 = (bf16[544,128]{1,0:T(8,128)(2,1)S(1)}, bf16[544,128]{1,0:T(8,128)(2,1)S(1)}, u32[]{:S(2)}, u32[]{:S(2)}) collective-permute-start(bf16[544,128]{1,0:T(8,128)(2,1)S(1)} %collective-permute-done.5.refs_2_), channel_id=1, source_target_pairs={{0,32},{32,64},{64,96},{96,128},{128,160},{160,192},{192,224},{224... | collective-permute-start | bytes 417800 | tf_op jit(solution)/shard_map/ppermute | solution.py:363
  106.2 7.4 %collective-permute-start.8 = (bf16[544,128]{1,0:T(8,128)(2,1)S(1)}, bf16[544,128]{1,0:T(8,128)(2,1)S(1)}, u32[]{:S(2)}, u32[]{:S(2)}) collective-permute-start(bf16[544,128]{1,0:T(8,128)(2,1)S(1)} %collective-permute-done.6.refs_3_), channel_id=1, source_target_pairs={{32,0},{64,32},{96,64},{128,96},{160,128},{192,160},{224,192},{256... | collective-permute-start | bytes 417800 | tf_op jit(solution)/shard_map/ppermute | solution.py:364
  113.6 9.5 %collective-permute-start.9 = (bf16[544,128]{1,0:T(8,128)(2,1)S(1)}, bf16[544,128]{1,0:T(8,128)(2,1)S(1)}, u32[]{:S(2)}, u32[]{:S(2)}) collective-permute-start(bf16[544,128]{1,0:T(8,128)(2,1)S(1)} %collective-permute-done.7.refs_2_), channel_id=1, source_target_pairs={{0,32},{32,64},{64,96},{96,128},{128,160},{160,192},{192,224},{224... | collective-permute-start | bytes 417800 | tf_op jit(solution)/shard_map/ppermute | solution.py:363
  115.5 7.6 %collective-permute-start.10 = (bf16[544,128]{1,0:T(8,128)(2,1)S(1)}, bf16[544,128]{1,0:T(8,128)(2,1)S(1)}, u32[]{:S(2)}, u32[]{:S(2)}) collective-permute-start(bf16[544,128]{1,0:T(8,128)(2,1)S(1)} %collective-permute-done.8.refs_3_), channel_id=1, source_target_pairs={{32,0},{64,32},{96,64},{128,96},{160,128},{192,160},{224,192},{256... | collective-permute-start | bytes 417800 | tf_op jit(solution)/shard_map/ppermute | solution.py:364
  123.1 9.1 %collective-permute-start.11 = (bf16[544,128]{1,0:T(8,128)(2,1)S(1)}, bf16[544,128]{1,0:T(8,128)(2,1)S(1)}, u32[]{:S(2)}, u32[]{:S(2)}) collective-permute-start(bf16[544,128]{1,0:T(8,128)(2,1)S(1)} %collective-permute-done.9.refs_2_), channel_id=1, source_target_pairs={{0,32},{32,64},{64,96},{96,128},{128,160},{160,192},{192,224},{224... | collective-permute-start | bytes 417800 | tf_op jit(solution)/shard_map/ppermute | solution.py:363
  125.0 7.2 %collective-permute-start.12 = (bf16[544,128]{1,0:T(8,128)(2,1)S(1)}, bf16[544,128]{1,0:T(8,128)(2,1)S(1)}, u32[]{:S(2)}, u32[]{:S(2)}) collective-permute-start(bf16[544,128]{1,0:T(8,128)(2,1)S(1)} %collective-permute-done.10.refs_3_), channel_id=1, source_target_pairs={{32,0},{64,32},{96,64},{128,96},{160,128},{192,160},{224,192},{256... | collective-permute-start | bytes 417800 | tf_op jit(solution)/shard_map/ppermute | solution.py:364
  132.2 8.9 %collective-permute-start.13 = (bf16[544,128]{1,0:T(8,128)(2,1)S(1)}, bf16[544,128]{1,0:T(8,128)(2,1)S(1)}, u32[]{:S(2)}, u32[]{:S(2)}) collective-permute-start(bf16[544,128]{1,0:T(8,128)(2,1)S(1)} %collective-permute-done.11.refs_2_), channel_id=1, source_target_pairs={{0,32},{32,64},{64,96},{96,128},{128,160},{160,192},{192,224},{224... | collective-permute-start | bytes 417800 | tf_op jit(solution)/shard_map/ppermute | solution.py:363
  134.2 7.0 %collective-permute-start.14 = (bf16[544,128]{1,0:T(8,128)(2,1)S(1)}, bf16[544,128]{1,0:T(8,128)(2,1)S(1)}, u32[]{:S(2)}, u32[]{:S(2)}) collective-permute-start(bf16[544,128]{1,0:T(8,128)(2,1)S(1)} %collective-permute-done.12.refs_3_), channel_id=1, source_target_pairs={{32,0},{64,32},{96,64},{128,96},{160,128},{192,160},{224,192},{256... | collective-permute-start | bytes 417800 | tf_op jit(solution)/shard_map/ppermute | solution.py:364
  141.1 8.9 %collective-permute-start.15 = (bf16[544,128]{1,0:T(8,128)(2,1)S(1)}, bf16[544,128]{1,0:T(8,128)(2,1)S(1)}, u32[]{:S(2)}, u32[]{:S(2)}) collective-permute-start(bf16[544,128]{1,0:T(8,128)(2,1)S(1)} %collective-permute-done.13.refs_2_), channel_id=1, source_target_pairs={{0,32},{32,64},{64,96},{96,128},{128,160},{160,192},{192,224},{224... | collective-permute-start | bytes 417800 | tf_op jit(solution)/shard_map/ppermute | solution.py:363
  143.9 6.2 %collective-permute-start.16 = (bf16[544,128]{1,0:T(8,128)(2,1)S(1)}, bf16[544,128]{1,0:T(8,128)(2,1)S(1)}, u32[]{:S(2)}, u32[]{:S(2)}) collective-permute-start(bf16[544,128]{1,0:T(8,128)(2,1)S(1)} %collective-permute-done.14.refs_3_), channel_id=1, source_target_pairs={{32,0},{64,32},{96,64},{128,96},{160,128},{192,160},{224,192},{256... | collective-permute-start | bytes 417800 | tf_op jit(solution)/shard_map/ppermute | solution.py:364
  150.1 7.2 %collective-permute-start.17 = (bf16[544,128]{1,0:T(8,128)(2,1)S(1)}, bf16[544,128]{1,0:T(8,128)(2,1)S(1)}, u32[]{:S(2)}, u32[]{:S(2)}) collective-permute-start(bf16[544,128]{1,0:T(8,128)(2,1)S(1)} %collective-permute-done.15.refs_2_), channel_id=1, source_target_pairs={{0,32},{32,64},{64,96},{96,128},{128,160},{160,192},{192,224},{224... | collective-permute-start | bytes 417800 | tf_op jit(solution)/shard_map/ppermute | solution.py:363
  170.7 26.8 %copy-start.7 = (bf16[16,4096]{1,0:T(8,128)(2,1)S(1)}, bf16[16,4096]{1,0:T(8,128)(2,1)}, u32[]{:S(2)}) copy-start(bf16[16,4096]{1,0:T(8,128)(2,1)} %x_ref.1) | copy-start | bytes 393220
  170.7 12.9 %collective-permute-start.18 = (bf16[64,4096]{1,0:T(8,128)(2,1)S(1)}, bf16[64,4096]{1,0:T(8,128)(2,1)S(1)}, u32[]{:S(2)}, u32[]{:S(2)}) collective-permute-start(bf16[64,4096]{1,0:T(8,128)(2,1)S(1)} %get-tuple-element.178), channel_id=1, source_target_pairs={{0,1},{1,0},{2,3},{3,2},{4,5},{5,4},{6,7},{7,6},{8,9},{9,8},{10,11... | collective-permute-start | bytes 1572872 | tf_op jit(solution)/shard_map/ppermute | solution.py:380
  184.5 12.9 %all-to-all-start.4 = ((bf16[4,16,4096]{2,1,0:T(8,128)(2,1)}), bf16[4,16,4096]{2,1,0:T(8,128)(2,1)S(1)}, u32[]{:S(2)}, u32[]{:S(2)}) async-start(bf16[4,16,4096]{2,1,0:T(8,128)(2,1)} %bitcast.14), calls=%async_computation.4 | async-start | bytes 1048576 | tf_op jit(solution)/shard_map/all_to_all | solution.py:382
